TPU v7x, 32 devices: a whole 2x2x4 slice. The times are simulated.
32 devices in a mesh: sp: 4 (over z), dp: 8 (over y, x, core).
Axes of the slice: x: 2, y: 2, z: 4, core: 2. Of those that a mesh axis runs over, the one named last changes fastest.
Arguments:
- inputs: bfloat16 [8, 512, 2048], P('dp', 'sp'), may hold values from -0.75 to 0.75
- queries: bfloat16 [8, 512, 1024], P('dp', 'sp'), may hold values from -18 to 18
- keys: bfloat16 [8, 512, 256], P('dp', 'sp'), may hold values from -18 to 18
- values: bfloat16 [8, 512, 256], P('dp', 'sp'), may hold values from -6 to 6
- out_grad: bfloat16 [8, 512, 1024], P('dp', 'sp'), may hold values from -144 to 144
- query_gain: float32 [64], replicated, may hold values from 0.4 to 6.5
- key_gain: float32 [64], replicated, may hold values from 0.4 to 6.5
- key_matrix: bfloat16 [2048, 256], P('dp'), may hold values from -0.125 to 0.125
- value_matrix: bfloat16 [2048, 256], P('dp'), may hold values from -0.125 to 0.125
Outputs:
- input_grad: bfloat16 [8, 512, 2048], P('dp', 'sp')
- query_grad: bfloat16 [8, 512, 1024], P('dp', 'sp')
- key_weight_grad: float32 [2048, 256], P('dp')
- value_weight_grad: float32 [2048, 256], P('dp')
All inputs are finite; a program needn't handle non-finite values.
Results may differ from a plain program's by a relative error of at most 0.024.
The roundings to bfloat16 on the way count: a program that leaves them out, or rounds other values in their place, can miss the bound.
Values may be sent and summed in bfloat16 or wider, within the bound.
No kernel may reach another device: no remote copies, remote signals or barrier semaphores. Data moves between devices by JAX's collectives and lax.ppermute only.
A program may use at most 64 MiB of HBM per device.

v0:
```python
import jax
import jax.numpy as jnp
from jax import lax
from jax.sharding import PartitionSpec as P

QUERY_HEADS = 16
KEY_VALUE_HEADS = 4
HEAD_CHANNELS = 64
GRID = 64


rope_base = 10000.0
norm_eps = 0.5
score_scale = 0.125


def product(pattern, first_op, second_op):
    return jnp.einsum(pattern, first_op, second_op, preferred_element_type=jnp.float32)


def rotary_tables(token_length):
    position = jnp.arange(token_length, dtype=jnp.int32)
    grid_row = (position // GRID).astype(jnp.float32)
    grid_col = (position % GRID).astype(jnp.float32)
    half_pairs = HEAD_CHANNELS // 4
    inv_freq = rope_base ** (-jnp.arange(half_pairs, dtype=jnp.float32) / half_pairs)
    angles = jnp.concatenate([grid_row[:, None] * inv_freq, grid_col[:, None] * inv_freq], axis=1)
    return (jnp.cos(angles), jnp.sin(angles))


def rotate(vector, cos_tab, sin_tab):
    even_part = vector[..., 0::2]
    odd_part = vector[..., 1::2]
    turned = jnp.stack(
        [even_part * cos_tab - odd_part * sin_tab, even_part * sin_tab + odd_part * cos_tab],
        axis=-1,
    )
    return turned.reshape(vector.shape)


def rotate_back(cotangent, cos_tab, sin_tab):
    even_part = cotangent[..., 0::2]
    odd_part = cotangent[..., 1::2]
    turned = jnp.stack(
        [even_part * cos_tab + odd_part * sin_tab, odd_part * cos_tab - even_part * sin_tab],
        axis=-1,
    )
    return turned.reshape(cotangent.shape)


def inverse_rms(vector):
    return lax.rsqrt(jnp.mean(vector * vector, axis=-1, keepdims=True) + norm_eps)


def norm_back(vector, inv_scale, cotangent, gain_vec):
    weighted = cotangent * gain_vec
    inner_mean = jnp.mean(weighted * vector, axis=-1, keepdims=True)
    return inv_scale * (weighted - vector * inv_scale * inv_scale * inner_mean)


def head_grads(
    query_in, key_input, value_input, grad_in, query_gain, key_gain, cos_tab, sin_tab, block_rows
):
    token_length, groups, per_group, head_dim = query_in.shape
    cos_four = cos_tab[:, None, None, :]
    sin_four = sin_tab[:, None, None, :]
    cos_three = cos_tab[:, None, :]
    sin_three = sin_tab[:, None, :]
    query_f = query_in.astype(jnp.float32)
    query_inv = inverse_rms(query_f)
    query_rot = rotate(query_f * query_inv * query_gain, cos_four, sin_four).astype(jnp.bfloat16)
    key_f = key_input.astype(jnp.float32)
    key_inv = inverse_rms(key_f)
    key_rot = rotate(key_f * key_inv * key_gain, cos_three, sin_three).astype(jnp.bfloat16)
    num_blocks = token_length // block_rows
    query_blocks = query_rot.reshape(num_blocks, block_rows, groups, per_group, head_dim)
    grad_blocks = grad_in.reshape(num_blocks, block_rows, groups, per_group, head_dim)

    def attend_block(carried, pieces):
        key_acc, value_acc = carried
        query_piece, grad_piece = pieces
        scores = product("qgrd,cgd->grqc", query_piece, key_rot) * score_scale
        row_max = jnp.max(scores, axis=-1, keepdims=True)
        shifted = jnp.exp(scores - row_max)
        attn_prob = shifted / jnp.sum(shifted, axis=-1, keepdims=True)
        prob_low = attn_prob.astype(jnp.bfloat16)
        prob_grad = product("qgrd,cgd->grqc", grad_piece, value_input)
        row_dot = jnp.sum(attn_prob * prob_grad, axis=-1, keepdims=True)
        score_grad = (attn_prob * (prob_grad - row_dot) * score_scale).astype(jnp.bfloat16)
        dq_piece = product("grqc,cgd->qgrd", score_grad, key_rot)
        key_acc = key_acc + product("grqc,qgrd->cgd", score_grad, query_piece)
        value_acc = value_acc + product("grqc,qgrd->cgd", prob_low, grad_piece)
        return ((key_acc, value_acc), dq_piece)

    empty_acc = jnp.zeros((token_length, groups, head_dim), jnp.float32)
    (key_rot_grad, value_acc), query_rot_grad = lax.scan(
        attend_block, (empty_acc, empty_acc), (query_blocks, grad_blocks)
    )
    query_rot_grad = query_rot_grad.reshape(token_length, groups, per_group, head_dim)
    query_grad = norm_back(
        query_f, query_inv, rotate_back(query_rot_grad, cos_four, sin_four), query_gain
    ).astype(jnp.bfloat16)
    key_portion = norm_back(
        key_f, key_inv, rotate_back(key_rot_grad, cos_three, sin_three), key_gain
    ).astype(jnp.bfloat16)
    return (query_grad, key_portion, value_acc.astype(jnp.bfloat16))


def on_device(
    inputs, queries, keys, values, out_grad, query_gain, key_gain, key_matrix, value_matrix
):
    sp_count = lax.axis_size("sp")
    dp_count = lax.axis_size("dp")
    token_row_block = inputs.shape[1]
    token_length = token_row_block * sp_count
    local_heads = QUERY_HEADS // sp_count
    portion_heads = min(local_heads, QUERY_HEADS // KEY_VALUE_HEADS)
    kv_here = local_heads // portion_heads
    group_copies = QUERY_HEADS // KEY_VALUE_HEADS // portion_heads
    key_value_width = KEY_VALUE_HEADS * HEAD_CHANNELS
    key_positions = jnp.repeat(
        keys[0].reshape(token_row_block, KEY_VALUE_HEADS, HEAD_CHANNELS), group_copies, axis=1
    ).reshape(token_row_block, key_value_width * group_copies)
    value_positions = jnp.repeat(
        values[0].reshape(token_row_block, KEY_VALUE_HEADS, HEAD_CHANNELS), group_copies, axis=1
    ).reshape(token_row_block, key_value_width * group_copies)
    grad_heads, query_heads, key_heads, value_heads = (
        lax.all_to_all(out_grad[0], "sp", split_axis=1, concat_axis=0, tiled=True),
        lax.all_to_all(queries[0], "sp", split_axis=1, concat_axis=0, tiled=True),
        lax.all_to_all(key_positions, "sp", split_axis=1, concat_axis=0, tiled=True),
        lax.all_to_all(value_positions, "sp", split_axis=1, concat_axis=0, tiled=True),
    )
    cos_tab, sin_tab = rotary_tables(token_length)
    query_part, key_portion, value_portion = head_grads(
        query_heads.reshape(token_length, kv_here, portion_heads, HEAD_CHANNELS),
        key_heads.reshape(token_length, kv_here, HEAD_CHANNELS),
        value_heads.reshape(token_length, kv_here, HEAD_CHANNELS),
        grad_heads.reshape(token_length, kv_here, portion_heads, HEAD_CHANNELS),
        query_gain,
        key_gain,
        cos_tab,
        sin_tab,
        min(512, token_length),
    )
    query_tokens, key_token_rows, value_token_rows = (
        lax.all_to_all(
            query_part.reshape(token_length, local_heads * HEAD_CHANNELS),
            "sp",
            split_axis=0,
            concat_axis=1,
            tiled=True,
        ),
        lax.all_to_all(
            key_portion.reshape(token_length, kv_here * HEAD_CHANNELS),
            "sp",
            split_axis=0,
            concat_axis=1,
            tiled=True,
        ),
        lax.all_to_all(
            value_portion.reshape(token_length, kv_here * HEAD_CHANNELS),
            "sp",
            split_axis=0,
            concat_axis=1,
            tiled=True,
        ),
    )
    key_gradient = (
        key_token_rows.reshape(token_row_block, KEY_VALUE_HEADS, group_copies, HEAD_CHANNELS)
        .astype(jnp.float32)
        .sum(axis=2)
        .astype(jnp.bfloat16)
    )
    value_gradient = (
        value_token_rows.reshape(token_row_block, KEY_VALUE_HEADS, group_copies, HEAD_CHANNELS)
        .astype(jnp.float32)
        .sum(axis=2)
        .astype(jnp.bfloat16)
    )
    projection_gradient = jnp.concatenate(
        [
            key_gradient.reshape(token_row_block, key_value_width),
            value_gradient.reshape(token_row_block, key_value_width),
        ],
        axis=1,
    )
    joined_weight = jnp.concatenate([key_matrix, value_matrix], axis=1)
    input_grad = lax.dot_general(
        projection_gradient,
        lax.all_gather(joined_weight, "dp", axis=0, tiled=True),
        (((1,), (1,)), ((), ())),
        preferred_element_type=jnp.float32,
    ).astype(jnp.bfloat16)
    token_in = inputs[0]
    width = inputs.shape[2]
    row_share = width // (sp_count * dp_count)
    permuted = (
        token_in.reshape(token_row_block, dp_count, sp_count, row_share)
        .transpose(0, 2, 1, 3)
        .reshape(token_row_block, width)
    )
    share_cols = lax.all_to_all(permuted, "sp", split_axis=1, concat_axis=0, tiled=True)
    all_grads = lax.all_gather(projection_gradient, "sp", axis=0, tiled=True)
    grad_piece = lax.psum_scatter(
        lax.dot_general(
            share_cols, all_grads, (((0,), (0,)), ((), ())), preferred_element_type=jnp.float32
        ).astype(jnp.bfloat16),
        "dp",
        scatter_dimension=0,
        tiled=True,
    ).astype(jnp.float32)
    weight_grad = lax.all_gather(grad_piece, "sp", axis=0, tiled=True)
    return (
        input_grad[None],
        query_tokens[None],
        weight_grad[:, :key_value_width],
        weight_grad[:, key_value_width:],
    )


def solution(mesh):
    return jax.shard_map(
        on_device,
        mesh=mesh,
        in_specs=(
            P("dp", "sp", None),
            P("dp", "sp", None),
            P("dp", "sp", None),
            P("dp", "sp", None),
            P("dp", "sp", None),
            P(),
            P(),
            P("dp", None),
            P("dp", None),
        ),
        out_specs=(P("dp", "sp", None), P("dp", "sp", None), P("dp", None), P("dp", None)),
        check_vma=False,
    )
```

profile of v0, /device:TPU:0, one launch (start us, length us, event | category | flops | bytes accessed | tf_op | source)
XLA Modules:
  0.0 183.9 jit_solution(14497211045874740525)
XLA Ops:
  7.2 1.6 copy.142
  8.8 6.3 %all-to-all-start = ((bf16[128,4,64]{0,2,1:T(8,128)(2,1)}), bf16[128,4,64]{0,2,1:T(8,128)(2,1)S(1)}, u32[]{:S(2)}, u32[]{:S(2)}) async-start(bf16[128,4,64]{0,2,1:T(8,128)(2,1)} %bitcast), calls=%async_computation | async-start | bytes 131072 | tf_op jit(solution)/shard_map/all_to_all | solution.py:130
  15.1 1.8 copy.143
  16.9 1.8 copy.150
  18.7 1.6 copy.148
  20.4 0.2 fusion.37
  20.6 0.2 all-to-all-done
  20.8 4.9 %all-to-all-start.2 = ((bf16[128,4,64]{0,2,1:T(8,128)(2,1)}), bf16[128,4,64]{0,2,1:T(8,128)(2,1)S(1)}, u32[]{:S(2)}, u32[]{:S(2)}) async-start(bf16[128,4,64]{0,2,1:T(8,128)(2,1)} %bitcast.21), calls=%async_computation.2 | async-start | bytes 131072 | tf_op jit(solution)/shard_map/all_to_all | solution.py:131
  25.8 0.6 add_rsqrt_fusion.1
  26.5 5.0 %all-to-all-done.2 = bf16[128,4,64]{0,2,1:T(8,128)(2,1)S(1)} async-done(((bf16[128,4,64]{0,2,1:T(8,128)(2,1)}), bf16[128,4,64]{0,2,1:T(8,128)(2,1)S(1)}, u32[]{:S(2)}, u32[]{:S(2)}) %all-to-all-start.2) | async-done | bytes 65568 | tf_op jit(solution)/shard_map/all_to_all | solution.py:131
  31.5 3.4 %all-to-all-start.1 = ((bf16[128,4,256]{0,2,1:T(8,128)(2,1)}), bf16[128,4,256]{0,2,1:T(8,128)(2,1)S(1)}, u32[]{:S(2)}, u32[]{:S(2)}) async-start(bf16[128,4,256]{0,2,1:T(8,128)(2,1)} %bitcast.2), calls=%async_computation.1 | async-start | bytes 524288 | tf_op jit(solution)/shard_map/all_to_all | solution.py:129
  34.9 0.7 multiply_multiply_fusion.2
  35.8 0.3 subtract_convert_fusion.1
  36.1 5.6 %all-to-all-done.1 = bf16[128,4,256]{0,2,1:T(8,128)(2,1)S(1)} async-done(((bf16[128,4,256]{0,2,1:T(8,128)(2,1)}), bf16[128,4,256]{0,2,1:T(8,128)(2,1)S(1)}, u32[]{:S(2)}, u32[]{:S(2)}) %all-to-all-start.1) | async-done | bytes 262176 | tf_op jit(solution)/shard_map/all_to_all | solution.py:129
  41.6 3.4 %all-to-all-start.3 = ((bf16[128,4,256]{0,2,1:T(8,128)(2,1)}), bf16[128,4,256]{0,2,1:T(8,128)(2,1)S(1)}, u32[]{:S(2)}, u32[]{:S(2)}) async-start(bf16[128,4,256]{0,2,1:T(8,128)(2,1)} %bitcast.23), calls=%async_computation.3 | async-start | bytes 524288 | tf_op jit(solution)/shard_map/all_to_all | solution.py:128
  45.1 0.3 copy.144
  45.4 0.2 reshape.715
  46.2 5.7 %all-to-all-done.3 = bf16[128,4,256]{0,2,1:T(8,128)(2,1)S(1)} async-done(((bf16[128,4,256]{0,2,1:T(8,128)(2,1)}), bf16[128,4,256]{0,2,1:T(8,128)(2,1)S(1)}, u32[]{:S(2)}, u32[]{:S(2)}) %all-to-all-start.3) | async-done | bytes 262176 | tf_op jit(solution)/shard_map/all_to_all | solution.py:128
  51.8 0.2 copy.151
  52.3 0.2 copy.145
  52.5 0.7 bitcast_reduce_fusion
  53.3 0.7 fusion.6
  54.0 1.3 fusion
  55.3 1.3 fusion.8
  56.6 0.7 convolution_bitcast_fusion.1
  57.4 0.3 add_bitcast_fusion.1
  58.0 0.8 multiply_reduce_fusion.1
  58.7 1.4 multiply_convert_fusion
  60.1 3.4 %all-to-all-start.4 = ((bf16[4,128,64]{1,2,0:T(8,128)(2,1)}), bf16[4,128,64]{1,2,0:T(8,128)(2,1)S(1)}, u32[]{:S(2)}, u32[]{:S(2)}) async-start(bf16[4,128,64]{1,2,0:T(8,128)(2,1)} %multiply_convert_fusion), calls=%async_computation.4 | async-start | bytes 131072 | tf_op jit(solution)/shard_map/all_to_all | solution.py:153
  63.6 3.2 %fusion.19 = bf16[512,1,64]{0,2,1:T(8,128)(2,1)S(1)} fusion(bf16[512,4,64]{0,2,1:T(8,128)(2,1)} %copy-done.5, f32[512,512,4,1]{1,0,3,2:T(8,128)} %copy-done, f32[4,512]{1,0:T(4,128)} %copy-done.6, f32[4,512]{1,0:T(4,128)S(1)} %get-tuple-element.74), kind=kOutput, calls=%fused_computation.24 | convolution fusion | flops 138444800 | bytes 4538368 | tf_op jit(solution)/shard_map/while/body/eval_jaxpr/grqc,qgrd->cgd/dot_general | solution.py:18
  66.8 0.6 copy.157
  67.4 1.9 %all-to-all-done.4 = bf16[4,128,64]{1,2,0:T(8,128)(2,1)S(1)} async-done(((bf16[4,128,64]{1,2,0:T(8,128)(2,1)}), bf16[4,128,64]{1,2,0:T(8,128)(2,1)S(1)}, u32[]{:S(2)}, u32[]{:S(2)}) %all-to-all-start.4) | async-done | bytes 65568 | tf_op jit(solution)/shard_map/all_to_all | solution.py:153
  69.3 0.6 copy-done.1
  69.9 3.9 %all-to-all-start.5 = ((bf16[4,128,64]{1,2,0:T(8,128)(2,1)}), bf16[4,128,64]{1,2,0:T(8,128)(2,1)}, u32[]{:S(2)}, u32[]{:S(2)}) async-start(bf16[4,128,64]{1,2,0:T(8,128)(2,1)} %copy.157), calls=%async_computation.5 | async-start | bytes 131072 | tf_op jit(solution)/shard_map/all_to_all | solution.py:160
  73.8 1.3 copy.169
  75.2 0.8 copy.170
  76.0 3.6 %all-to-all-done.5 = bf16[4,128,64]{1,2,0:T(8,128)(2,1)} async-done(((bf16[4,128,64]{1,2,0:T(8,128)(2,1)}), bf16[4,128,64]{1,2,0:T(8,128)(2,1)}, u32[]{:S(2)}, u32[]{:S(2)}) %all-to-all-start.5) | async-done | bytes 65568 | tf_op jit(solution)/shard_map/all_to_all | solution.py:160
  79.6 4.1 %all-to-all-start.7 = ((bf16[128,4,512]{0,2,1:T(8,128)(2,1)}), bf16[128,4,512]{0,2,1:T(8,128)(2,1)}, u32[]{:S(2)}, u32[]{:S(2)}) async-start(bf16[128,4,512]{0,2,1:T(8,128)(2,1)} %bitcast.56), calls=%async_computation.7 | async-start | bytes 1048576 | tf_op jit(solution)/shard_map/all_to_all | solution.py:202
  83.8 0.9 pad_maximum_fusion.4
  84.7 19.0 %all_gather.10 = bf16[512,512]{0,1:T(8,128)(2,1)S(1)} all-gather(bf16[128,512]{0,1:T(8,128)(2,1)S(1)} %pad_maximum_fusion.4), channel_id=1, replica_groups=mesh['sp'=4,'dp'=8] {'sp'}, dimensions={0}, use_global_device_ids=true | all-gather | bytes 655360 | tf_op jit(solution)/shard_map/all_gather | solution.py:203
  103.7 2.0 %copy.171 = bf16[4,128,512]{2,1,0:T(8,128)(2,1)} copy(bf16[4,128,512]{1,2,0:T(8,128)(2,1)} %bitcast.57) | data formatting | bytes 1048576 | tf_op jit(solution)/shard_map/all_to_all | solution.py:202
  105.8 2.3 %fusion.12 = bf16[512,512]{0,1:T(8,128)(2,1)} fusion(bf16[512,512]{0,1:T(8,128)(2,1)S(1)} %all_gather.10, bf16[512,512]{1,0:T(8,128)(2,1)} %bitcast.182), kind=kOutput, calls=%fused_computation.20 | convolution fusion | flops 268697600 | bytes 1572864 | tf_op jit(solution)/shard_map/dot_general | solution.py:205
  108.0 2.0 %copy.178 = bf16[512,512]{1,0:T(8,128)(2,1)} copy(bf16[512,512]{0,1:T(8,128)(2,1)} %fusion.12) | data formatting | bytes 1048576
  110.1 0.2 all-gather.2.cloned.1.call-start
  110.3 1.7 pad_maximum_fusion.2
  112.3 0.8 pad_maximum_fusion.7
  113.2 0.7 reshape.723
  113.9 1.3 convolution_bitcast_fusion
  115.2 0.1 slice.36
  115.5 0.4 reshape.717
  116.0 0.3 pad_maximum_fusion
  116.3 0.2 mul.460
  116.5 0.4 copy.160
  116.9 0.5 reshape.714
  117.5 0.2 mul.444
  117.7 0.2 fusion.25
  117.9 10.3 %all_to_all.113 = bf16[4,128,256]{1,2,0:T(8,128)(2,1)S(1)} all-to-all(bf16[4,128,256]{1,2,0:T(8,128)(2,1)S(1)} %fusion.25), channel_id=1, replica_groups=mesh['sp'=4,'dp'=8] {'sp'}, dimensions={0} | all-to-all | bytes 524288 | tf_op jit(solution)/shard_map/all_to_all | solution.py:146
  128.2 0.8 copy.173
  129.0 15.1 %reduce-scatter.4.cloned.1.call-done = bf16[64,512]{1,0:T(8,128)(2,1)} async-done(((bf16[512,512]{1,0:T(8,128)(2,1)}), bf16[64,512]{1,0:T(8,128)(2,1)}) %reduce-scatter.4.cloned.1.call-update) | async-done | bytes 65552 | tf_op jit(solution)/shard_map/reduce_scatter | solution.py:204
  144.1 0.8 convert_element_type.220
  145.0 15.2 %all_gather.11 = f32[256,512]{1,0:T(8,128)S(1)} all-gather(f32[64,512]{1,0:T(8,128)S(1)} %convert_element_type.220), channel_id=1, replica_groups=mesh['sp'=4,'dp'=8] {'sp'}, dimensions={0}, use_global_device_ids=true | all-gather | bytes 655360 | tf_op jit(solution)/shard_map/all_gather | solution.py:212
  160.2 0.8 fusion.52
  161.0 12.8 %all-gather.2.cloned.1.call-done = bf16[2048,512]{1,0:T(8,128)(2,1)} async-done(((bf16[256,512]{1,0:T(8,128)(2,1)}), bf16[2048,512]{1,0:T(8,128)(2,1)}) %all-gather.2.cloned.1.call-update) | async-done | bytes 2097168 | tf_op jit(solution)/shard_map/all_gather | solution.py:190
  173.9 3.2 %fusion.7 = bf16[1,128,2048]{2,1,0:T(8,128)(2,1)} fusion(bf16[2048,512]{1,0:T(8,128)(2,1)} %all-gather.2.cloned.1.call-done, bf16[128,256]{0,1:T(8,128)(2,1)} %bitcast.43, bf16[128,256]{0,1:T(8,128)(2,1)S(1)} %bitcast.192), kind=kOutput, calls=%fused_computation.13 | convolution fusion | flops 268959744 | bytes 2752512 | tf_op jit(solution)/shard_map/dot_general | solution.py:188
  (58 shorter events, 2.2 us)
Async XLA Ops:
  7.2 38.6 %copy-start.7 = (f32[64]{0:T(128)S(1)}, f32[64]{0:T(128)}, u32[]{:S(2)}) copy-start(f32[64]{0:T(128)} %param.14) | copy-start | bytes 772
  8.8 12.1 %all-to-all-start = ((bf16[128,4,64]{0,2,1:T(8,128)(2,1)}), bf16[128,4,64]{0,2,1:T(8,128)(2,1)S(1)}, u32[]{:S(2)}, u32[]{:S(2)}) async-start(bf16[128,4,64]{0,2,1:T(8,128)(2,1)} %bitcast), calls=%async_computation | async-start | bytes 131072 | tf_op jit(solution)/shard_map/all_to_all | solution.py:130
  20.8 10.6 %all-to-all-start.2 = ((bf16[128,4,64]{0,2,1:T(8,128)(2,1)}), bf16[128,4,64]{0,2,1:T(8,128)(2,1)S(1)}, u32[]{:S(2)}, u32[]{:S(2)}) async-start(bf16[128,4,64]{0,2,1:T(8,128)(2,1)} %bitcast.21), calls=%async_computation.2 | async-start | bytes 131072 | tf_op jit(solution)/shard_map/all_to_all | solution.py:131
  31.5 10.2 %all-to-all-start.1 = ((bf16[128,4,256]{0,2,1:T(8,128)(2,1)}), bf16[128,4,256]{0,2,1:T(8,128)(2,1)S(1)}, u32[]{:S(2)}, u32[]{:S(2)}) async-start(bf16[128,4,256]{0,2,1:T(8,128)(2,1)} %bitcast.2), calls=%async_computation.1 | async-start | bytes 524288 | tf_op jit(solution)/shard_map/all_to_all | solution.py:129
  36.0 16.5 %copy-start.3 = (bf16[512,1,32]{0,2,1:T(8,128)(2,1)}, bf16[512,1,32]{0,2,1:T(8,128)(2,1)S(1)}, u32[]{:S(2)}) copy-start(bf16[512,1,32]{0,2,1:T(8,128)(2,1)S(1)} %get-tuple-element.62) | copy-start | bytes 98308
  36.0 16.5 %copy-start.4 = (bf16[512,1,32]{0,2,1:T(8,128)(2,1)}, bf16[512,1,32]{0,2,1:T(8,128)(2,1)S(1)}, u32[]{:S(2)}) copy-start(bf16[512,1,32]{0,2,1:T(8,128)(2,1)S(1)} %get-tuple-element.63) | copy-start | bytes 98308
  41.6 10.2 %all-to-all-start.3 = ((bf16[128,4,256]{0,2,1:T(8,128)(2,1)}), bf16[128,4,256]{0,2,1:T(8,128)(2,1)S(1)}, u32[]{:S(2)}, u32[]{:S(2)}) async-start(bf16[128,4,256]{0,2,1:T(8,128)(2,1)} %bitcast.23), calls=%async_computation.3 | async-start | bytes 524288 | tf_op jit(solution)/shard_map/all_to_all | solution.py:128
  52.1 1.8 copy-start.5
  53.2 2.0 %copy-start = (f32[512,512,4,1]{1,0,3,2:T(8,128)}, f32[512,512,4,1]{1,0,3,2:T(8,128)S(1)}, u32[]{:S(2)}) copy-start(f32[512,512,4,1]{1,0,3,2:T(8,128)S(1)} %get-tuple-element.75) | copy-start | bytes 12582916
  54.0 1.3 copy-start.6
  60.1 9.2 %all-to-all-start.4 = ((bf16[4,128,64]{1,2,0:T(8,128)(2,1)}), bf16[4,128,64]{1,2,0:T(8,128)(2,1)S(1)}, u32[]{:S(2)}, u32[]{:S(2)}) async-start(bf16[4,128,64]{1,2,0:T(8,128)(2,1)} %multiply_convert_fusion), calls=%async_computation.4 | async-start | bytes 131072 | tf_op jit(solution)/shard_map/all_to_all | solution.py:153
  69.3 0.6 copy-start.1
  69.9 9.7 %all-to-all-start.5 = ((bf16[4,128,64]{1,2,0:T(8,128)(2,1)}), bf16[4,128,64]{1,2,0:T(8,128)(2,1)}, u32[]{:S(2)}, u32[]{:S(2)}) async-start(bf16[4,128,64]{1,2,0:T(8,128)(2,1)} %copy.157), calls=%async_computation.5 | async-start | bytes 131072 | tf_op jit(solution)/shard_map/all_to_all | solution.py:160
  75.1 36.9 %copy-start.8 = (f32[64]{0:T(128)S(1)}, f32[64]{0:T(128)}, u32[]{:S(2)}) copy-start(f32[64]{0:T(128)} %param.14) | copy-start | bytes 772
  79.6 24.1 %all-to-all-start.7 = ((bf16[128,4,512]{0,2,1:T(8,128)(2,1)}), bf16[128,4,512]{0,2,1:T(8,128)(2,1)}, u32[]{:S(2)}, u32[]{:S(2)}) async-start(bf16[128,4,512]{0,2,1:T(8,128)(2,1)} %bitcast.56), calls=%async_computation.7 | async-start | bytes 1048576 | tf_op jit(solution)/shard_map/all_to_all | solution.py:202
  83.8 60.3 %reduce-scatter.4.cloned.1.call-start = ((), (), s32[]{:S(2)}) async-start(), calls=%async_computation.10 | async-start | bytes 589824 | tf_op jit(solution)/shard_map/reduce_scatter | solution.py:204
  110.1 63.8 %all-gather.2.cloned.1.call-start = ((), (), s32[]{:S(2)}) async-start(), calls=%async_computation.9 | async-start | bytes 2359296 | tf_op jit(solution)/shard_map/all_gather | solution.py:190
  116.5 57.4 %copy-start.2 = (bf16[4,128,64]{1,2,0:T(8,128)(2,1)S(1)}, bf16[4,128,64]{1,2,0:T(8,128)(2,1)}, u32[]{:S(2)}) copy-start(bf16[4,128,64]{1,2,0:T(8,128)(2,1)} %copy-done.1) | copy-start | bytes 196612
Sparse Core Ops, SparseCore 0:
  110.2 33.8 reduce-scatter.3
  146.0 27.7 all-gather.1
where the time goes:
time: 185 us; the launch traced here: 184 us
  waiting for transfers between devices  49.9 us (27%)
  blocking collectives  44.5 us (24%)
  starting transfers between devices  29.8 us (16%)
  local copies, waits for them, and re-layouts  20.9 us (11%)
  between operations  14.5 us (8%)
  matrix products  12.8 us (7%)
  other arithmetic  11.5 us (6%)
    all_gather x1, blocking collectives, on_device(): all_grads = lax.all_gather(projection_gradient, 'sp', axis=0, tiled=True)  19 us
    all_gather x1, blocking collectives, on_device(): weight_grad = lax.all_gather(grad_piece, 'sp', axis=0, tiled=True)  15.2 us
    reduce_scatter x1, waiting for transfers between devices, on_device(): lax.psum_scatter(lax.dot_general(share_cols, all_grads, (((0,), (0,)), ((...  15.1 us
    all_gather x1, waiting for transfers between devices, on_device(): lax.all_gather(joined_weight, 'dp', axis=0, tiled=True)  12.8 us
    unnamed x25, local copies, waits for them, and re-layouts  11.6 us
    all_to_all x1, blocking collectives, on_device(): lax.all_to_all(query_part.reshape(token_length, local_heads * HEAD_CHANNE...  10.3 us
    dot_general x5, matrix products, product(): jnp.einsum(pattern, first_op, second_op, preferred_element_type=jnp.float32)  7.27 us
    all_to_all x1, starting transfers between devices, on_device(): lax.all_to_all(key_positions, 'sp', split_axis=1, concat_axis=0, tiled=True)  6.35 us
  transfers between devices with their start and end apart: 9, of which 8 were waited for; matrix products, arithmetic and copies ran while one was open for 14% of the time, Pallas kernels for 0%

commit v1 on v0

--- a/solution.py
+++ b/solution.py
@@ -1,6 +1,9 @@
 import jax
 import jax.numpy as jnp
+import numpy as np
 from jax import lax
+from jax.experimental import pallas as pl
+from jax.experimental.pallas import tpu as pltpu
 from jax.sharding import PartitionSpec as P
 
 QUERY_HEADS = 16
@@ -106,7 +109,7 @@
     return (query_grad, key_portion, value_acc.astype(jnp.bfloat16))
 
 
-def on_device(
+def generic_device(
     inputs, queries, keys, values, out_grad, query_gain, key_gain, key_matrix, value_matrix
 ):
     sp_count = lax.axis_size("sp")
@@ -218,9 +221,413 @@
     )
 
 
+bf16 = jnp.bfloat16
+f32 = jnp.float32
+
+
+def dot(first_op, second_op, first_dim, second_dim):
+    return lax.dot_general(
+        first_op, second_op, (((first_dim,), (second_dim,)), ((), ())), preferred_element_type=f32
+    )
+
+
+def kernel_call(body, out_shape, scratch, args, flops=0):
+    vmem = pl.BlockSpec(memory_space=pltpu.VMEM)
+    return pl.pallas_call(
+        body,
+        out_shape=out_shape,
+        in_specs=[vmem] * len(args),
+        out_specs=jax.tree.map(lambda _: vmem, out_shape),
+        scratch_shapes=scratch,
+        cost_estimate=pl.CostEstimate(flops=flops, bytes_accessed=0, transcendentals=0),
+        compiler_params=pltpu.CompilerParams(vmem_limit_bytes=58 * 1024 * 1024),
+    )(*args)
+
+
+def shape_of(shape, dtype=bf16):
+    return jax.ShapeDtypeStruct(shape, dtype)
+
+
+def swap_with(value, axis, k):
+    count = lax.axis_size(axis)
+    return lax.ppermute(value, axis, [(i, i ^ k) for i in range(count)])
+
+
+def pack_heads(queries, keys, values, out_grad):
+    rows, q_all = queries.shape
+    kv_half = keys.shape[1] // 2
+    q_half = q_all // 2
+    width = 2 * q_half + 2 * kv_half
+
+    def body(q_ref, g_ref, k_ref, v_ref, own, mate, far, far_mate, buf):
+        bit = lax.axis_index("sp") % 2
+        for d in range(2):
+            buf[d, :, :q_half] = q_ref[:, d * q_half : (d + 1) * q_half]
+            buf[d, :, q_half : 2 * q_half] = g_ref[:, d * q_half : (d + 1) * q_half]
+            parts = []
+            for h in range(kv_half // HEAD_CHANNELS):
+                lo = d * kv_half + h * HEAD_CHANNELS
+                parts += [k_ref[:, lo : lo + HEAD_CHANNELS], v_ref[:, lo : lo + HEAD_CHANNELS]]
+            buf[d, :, 2 * q_half :] = jnp.concatenate(parts, axis=1)
+        own[...] = buf[bit]
+        mate[...] = buf[1 - bit]
+        far[...] = buf[bit, :, 2 * q_half :]
+        far_mate[...] = buf[1 - bit, :, 2 * q_half :]
+
+    return kernel_call(
+        body,
+        [shape_of((rows, width))] * 2 + [shape_of((rows, 2 * kv_half))] * 2,
+        [pltpu.VMEM((2, rows, width), bf16)],
+        (queries, out_grad, keys, values),
+    )
+
+
+def join_weights(key_matrix, value_matrix):
+    rows, kv_width = key_matrix.shape
+
+    def body(wk_ref, wv_ref, out):
+        for h in range(kv_width // HEAD_CHANNELS):
+            cols = slice(h * HEAD_CHANNELS, (h + 1) * HEAD_CHANNELS)
+            out[:, 2 * h * HEAD_CHANNELS : 2 * (h + 1) * HEAD_CHANNELS] = jnp.concatenate(
+                [wk_ref[:, cols], wv_ref[:, cols]], axis=1
+            )
+
+    return kernel_call(body, shape_of((rows, 2 * kv_width)), [], (key_matrix, value_matrix))
+
+
+def turn_inputs(token_in):
+    def body(x_ref, out):
+        out[...] = x_ref[...].T
+
+    return kernel_call(body, shape_of(token_in.shape[::-1]), [], (token_in,))
+
+
+def angle_tables(token_length):
+    half_pairs = HEAD_CHANNELS // 4
+    inv_freq = rope_base ** (-np.arange(half_pairs, dtype=np.float64) / half_pairs)
+    inv_freq = inv_freq.astype(np.float32)
+    channel = np.arange(2 * HEAD_CHANNELS)
+    freq = inv_freq[(channel % HEAD_CHANNELS // 2) % half_pairs]
+    sign = np.where(channel % 2 == 0, -1.0, 1.0).astype(np.float32)
+    tables = []
+    for count in (token_length // GRID, GRID):
+        angles = (np.arange(count, dtype=np.float32)[:, None] * freq).astype(np.float64)
+        tables += [np.cos(angles).astype(np.float32), (np.sin(angles) * sign).astype(np.float32)]
+    return tables
+
+
+def attention(own, mate, far, far_mate, query_gain, key_gain):
+    rows, width = own.shape
+    kv_width = far.shape[1]
+    q_width = (width - kv_width) // 2
+    pair = 2 * HEAD_CHANNELS
+    heads = q_width // HEAD_CHANNELS
+    groups = kv_width // pair
+    per_group = heads // groups
+    q_chunks = q_width // pair
+    half = 2 * rows
+    tokens = 4 * rows
+    tables = angle_tables(tokens)
+
+    def body(*refs):
+        own_ref, mate_ref, far_ref, far_mate_ref, qg_ref, kg_ref = refs[:6]
+        row_cos, row_sin, col_cos, col_sin = refs[6:10]
+        dq_own, dq_mate, p_own, p_far = refs[10:14]
+        q_tok, kv_tok, qh, gh, kr, vv, q_inv, k_inv, dq_sc, dkv_sc, dq_out, p_sc = refs[14:]
+        me = lax.axis_index("sp")
+        bit = me % 2
+        upper = me // 2
+        q_own = pl.multiple_of(bit * rows, rows)
+        q_mate = pl.multiple_of((1 - bit) * rows, rows)
+        q_tok[pl.ds(q_own, rows), :] = own_ref[:, : 2 * q_width]
+        q_tok[pl.ds(q_mate, rows), :] = mate_ref[:, : 2 * q_width]
+        for k, block in enumerate(
+            (own_ref[:, 2 * q_width :], mate_ref[:, 2 * q_width :], far_ref[...], far_mate_ref[...])
+        ):
+            kv_tok[pl.ds(pl.multiple_of((me ^ k) * rows, rows), rows), :] = block
+        lane = lax.broadcasted_iota(jnp.int32, (GRID, pair), 1)
+        even = lane % 2 == 0
+        by_row = lane % HEAD_CHANNELS < HEAD_CHANNELS // 2
+        first_head = lane < HEAD_CHANNELS
+        seg_r = lax.broadcasted_iota(jnp.int32, (2 * pair, pair), 0) // HEAD_CHANNELS % 2
+        seg_c = lax.broadcasted_iota(jnp.int32, (2 * pair, pair), 1) // HEAD_CHANNELS
+        seg = jnp.where(seg_r == seg_c, 1.0 / HEAD_CHANNELS, 0.0).astype(bf16)
+        q_gain = jnp.concatenate([qg_ref[...], qg_ref[...]], axis=1)
+        k_gain = jnp.concatenate([kg_ref[...], kg_ref[...]], axis=1)
+
+        def head_mean(product_f):
+            high = product_f.astype(bf16)
+            low = (product_f - high.astype(f32)).astype(bf16)
+            return dot(jnp.concatenate([high, low], axis=1), seg, 1, 0)
+
+        def swap(value):
+            return jnp.where(even, pltpu.roll(value, pair - 1, 1), pltpu.roll(value, 1, 1))
+
+        def angles_of(r):
+            cos = jnp.where(by_row, row_cos[pl.ds(r, 1), :], col_cos[...])
+            sin = jnp.where(by_row, row_sin[pl.ds(r, 1), :], col_sin[...])
+            return cos, sin
+
+        def forward(value, gain, cos, sin):
+            inv = lax.rsqrt(head_mean(value * value) + norm_eps)
+            normed = value * inv * gain
+            return inv, (normed * cos + swap(normed) * sin).astype(bf16)
+
+        def backward(value, inv, grad, gain, cos, sin):
+            weighted = (grad * cos - swap(grad) * sin) * gain
+            inner = head_mean(weighted * value)
+            return inv * (weighted - value * inv * inv * inner)
+
+        q_rows = half // GRID
+        for r in range(tokens // GRID):
+            at = slice(r * GRID, (r + 1) * GRID)
+            cos, sin = angles_of(r)
+            for c in range(groups):
+                part = slice(c * pair, (c + 1) * pair)
+                raw = kv_tok[at, part]
+                inv, turned = forward(raw.astype(f32), k_gain, cos, sin)
+                k_inv[at, part] = inv
+                kr[c, at, :] = turned[:, :HEAD_CHANNELS]
+                vv[c, at, :] = raw[:, HEAD_CHANNELS:]
+        for r in range(q_rows):
+            at = slice(r * GRID, (r + 1) * GRID)
+            cos, sin = angles_of(upper * q_rows + r)
+            for c in range(q_chunks):
+                part = slice(c * pair, (c + 1) * pair)
+                inv, turned = forward(q_tok[at, part].astype(f32), q_gain, cos, sin)
+                q_inv[at, part] = inv
+                grad = q_tok[at, q_width + c * pair : q_width + (c + 1) * pair]
+                for u in range(2):
+                    lanes = slice(u * HEAD_CHANNELS, (u + 1) * HEAD_CHANNELS)
+                    qh[2 * c + u, at, :] = turned[:, lanes]
+                    gh[2 * c + u, at, :] = grad[:, lanes]
+
+        for g in range(groups):
+            key_rot = kr[g]
+            value_in = vv[g]
+            for h in range(g * per_group, (g + 1) * per_group):
+                query = qh[h]
+                grad = gh[h]
+                scores = dot(key_rot, query, 1, 1)
+                top = jnp.max(scores, axis=0, keepdims=True)
+                expo = jnp.exp((scores - top) * score_scale)
+                prob = expo * (1.0 / jnp.sum(expo, axis=0, keepdims=True))
+                prob_grad = dot(value_in, grad, 1, 1)
+                row_dot = jnp.sum(prob * prob_grad, axis=0, keepdims=True)
+                score_grad = (prob * (prob_grad - row_dot)).astype(bf16)
+                dv = dot(prob.astype(bf16), grad, 1, 0)
+                dk = dot(score_grad, query, 1, 0)
+                dq_t = dot(key_rot, score_grad, 0, 0)
+                dq_sc[:, h * HEAD_CHANNELS : (h + 1) * HEAD_CHANNELS] = dq_t.T * score_scale
+                first = h == g * per_group
+                key_acc = dk if first else key_acc + dk
+                value_acc = dv if first else value_acc + dv
+            dkv_sc[:, g * pair : (g + 1) * pair] = jnp.concatenate(
+                [key_acc * score_scale, value_acc], axis=1
+            )
+
+        for r in range(tokens // GRID):
+            at = slice(r * GRID, (r + 1) * GRID)
+            cos, sin = angles_of(r)
+            for c in range(groups):
+                part = slice(c * pair, (c + 1) * pair)
+                grad = dkv_sc[at, part]
+                value = kv_tok[at, part].astype(f32)
+                result = backward(value, k_inv[at, part], grad, k_gain, cos, sin)
+                p_sc[at, part] = jnp.where(first_head, result, grad)
+        p_own[...] = p_sc[pl.ds(pl.multiple_of(upper * half, half), half), :]
+        p_far[...] = p_sc[pl.ds(pl.multiple_of((1 - upper) * half, half), half), :].astype(bf16)
+        for r in range(q_rows):
+            at = slice(r * GRID, (r + 1) * GRID)
+            cos, sin = angles_of(upper * q_rows + r)
+            for c in range(q_chunks):
+                part = slice(c * pair, (c + 1) * pair)
+                value = q_tok[at, part].astype(f32)
+                result = backward(value, q_inv[at, part], dq_sc[at, part], q_gain, cos, sin)
+                dq_out[at, part] = result.astype(bf16)
+        dq_own[...] = dq_out[pl.ds(q_own, rows), :]
+        dq_mate[...] = dq_out[pl.ds(q_mate, rows), :]
+
+    return kernel_call(
+        body,
+        [shape_of((rows, q_width))] * 2
+        + [shape_of((half, kv_width), f32), shape_of((half, kv_width))],
+        [
+            pltpu.VMEM((half, 2 * q_width), bf16),
+            pltpu.VMEM((tokens, kv_width), bf16),
+            pltpu.VMEM((heads, half, HEAD_CHANNELS), bf16),
+            pltpu.VMEM((heads, half, HEAD_CHANNELS), bf16),
+            pltpu.VMEM((groups, tokens, HEAD_CHANNELS), bf16),
+            pltpu.VMEM((groups, tokens, HEAD_CHANNELS), bf16),
+            pltpu.VMEM((half, q_width), f32),
+            pltpu.VMEM((tokens, kv_width), f32),
+            pltpu.VMEM((half, q_width), f32),
+            pltpu.VMEM((tokens, kv_width), f32),
+            pltpu.VMEM((half, q_width), bf16),
+            pltpu.VMEM((tokens, kv_width), f32),
+        ],
+        (
+            own,
+            mate,
+            far,
+            far_mate,
+            query_gain[None],
+            key_gain[None],
+            *[jnp.asarray(t) for t in tables],
+        ),
+        flops=10 * heads * half * tokens * HEAD_CHANNELS,
+    )
+
+
+def weight_partials(turned_own, turned_mate, p_own, p_far, dp_count):
+    feats, rows = turned_own.shape
+    half, cols = p_own.shape
+    share = feats // dp_count
+
+    def body(xo_ref, xm_ref, po_ref, pf_ref, *rest):
+        mine_out, mate_out = rest[:2]
+        outs = rest[2 : 2 + dp_count]
+        x_all, p_sc, res = rest[2 + dp_count :]
+        bit = lax.axis_index("sp") % 2
+        mine = lax.axis_index("dp")
+        p_sc[...] = (po_ref[...] + pf_ref[...].astype(f32)).astype(bf16)
+        p_mine = p_sc[pl.ds(pl.multiple_of(bit * rows, rows), rows), :]
+        p_mate = p_sc[pl.ds(pl.multiple_of((1 - bit) * rows, rows), rows), :]
+        mine_out[...] = p_mine
+        mate_out[...] = p_mate
+        x_all[:, :rows] = xo_ref[...]
+        x_all[:, rows:] = xm_ref[...]
+        p_all = jnp.concatenate([p_mine, p_mate], axis=0)
+        res[...] = dot(x_all[...], p_all, 1, 0).astype(bf16)
+        for m, out in enumerate(outs):
+            out[...] = res[pl.ds(pl.multiple_of((mine ^ m) * share, share), share), :]
+
+    outs = kernel_call(
+        body,
+        [shape_of((rows, cols))] * 2 + [shape_of((share, cols))] * dp_count,
+        [
+            pltpu.VMEM((feats, half), bf16),
+            pltpu.VMEM((half, cols), bf16),
+            pltpu.VMEM((feats, cols), bf16),
+        ],
+        (turned_own, turned_mate, p_own, p_far),
+        flops=2 * feats * half * cols,
+    )
+    return outs[0], outs[1], outs[2:]
+
+
+def sum_pieces(pieces):
+    total = pieces[0].astype(f32)
+    for piece in pieces[1:]:
+        total = total + piece.astype(f32)
+    return total.astype(bf16)
+
+
+def join_weight_grads(own, mate, far, far_mate):
+    rows, cols = own.shape
+    pair = 2 * HEAD_CHANNELS
+    groups = cols // pair
+
+    def body(own_ref, mate_ref, far_ref, far_mate_ref, k_out, v_out, buf):
+        bit = lax.axis_index("sp") % 2
+        buf[bit] = own_ref[...].astype(f32) + far_ref[...].astype(f32)
+        buf[1 - bit] = mate_ref[...].astype(f32) + far_mate_ref[...].astype(f32)
+        parts = [buf[d, :, g * pair : (g + 1) * pair] for d in range(2) for g in range(groups)]
+        k_out[...] = jnp.concatenate([p[:, :HEAD_CHANNELS] for p in parts], axis=1)
+        v_out[...] = jnp.concatenate([p[:, HEAD_CHANNELS:] for p in parts], axis=1)
+
+    return kernel_call(
+        body,
+        [shape_of((rows, cols), f32)] * 2,
+        [pltpu.VMEM((2, rows, cols), f32)],
+        (own, mate, far, far_mate),
+    )
+
+
+def token_outputs(p_mine, p_from_mate, weight_pieces, dq_own, dq_from_mate):
+    rows, cols = p_mine.shape
+    q_half = dq_own.shape[1]
+    dp_count = len(weight_pieces)
+    w_rows = weight_pieces[0].shape[0]
+
+    def body(p_ref, pm_ref, dq_ref, dqm_ref, *rest):
+        w_refs = rest[:dp_count]
+        x_out, q_out, p_buf, out_buf, q_buf = rest[dp_count:]
+        bit = lax.axis_index("sp") % 2
+        mine = lax.axis_index("dp")
+        p_buf[bit] = p_ref[...]
+        p_buf[1 - bit] = pm_ref[...]
+        q_buf[bit] = dq_ref[...]
+        q_buf[1 - bit] = dqm_ref[...]
+        for d in range(2):
+            q_out[:, d * q_half : (d + 1) * q_half] = q_buf[d]
+        left = jnp.concatenate([p_buf[0], p_buf[1]], axis=1)
+        for m in range(dp_count):
+            out_buf[mine ^ m] = dot(left, w_refs[m][...], 1, 1).astype(bf16)
+        for j in range(dp_count):
+            x_out[:, j * w_rows : (j + 1) * w_rows] = out_buf[j]
+
+    return kernel_call(
+        body,
+        [shape_of((rows, dp_count * w_rows)), shape_of((rows, 2 * q_half))],
+        [
+            pltpu.VMEM((2, rows, cols), bf16),
+            pltpu.VMEM((dp_count, rows, w_rows), bf16),
+            pltpu.VMEM((2, rows, q_half), bf16),
+        ],
+        (p_mine, p_from_mate, dq_own, dq_from_mate, *weight_pieces),
+        flops=4 * rows * dp_count * w_rows * cols,
+    )
+
+
+def fast_device(
+    inputs, queries, keys, values, out_grad, query_gain, key_gain, key_matrix, value_matrix
+):
+    return fast_body(
+        inputs[0],
+        queries[0],
+        keys[0],
+        values[0],
+        out_grad[0],
+        query_gain,
+        key_gain,
+        key_matrix,
+        value_matrix,
+    )
+
+
+def fast_body(
+    inputs, queries, keys, values, out_grad, query_gain, key_gain, key_matrix, value_matrix
+):
+    others = range(1, lax.axis_size("dp"))
+    own, mate, far, far_mate = pack_heads(queries, keys, values, out_grad)
+    mate = swap_with(mate, "sp", 1)
+    far = swap_with(far, "sp", 2)
+    far_mate = swap_with(far_mate, "sp", 3)
+    joined_weight = join_weights(key_matrix, value_matrix)
+    weight_pieces = [joined_weight] + [swap_with(joined_weight, "dp", m) for m in others]
+    turned = turn_inputs(inputs)
+    turned_mate = swap_with(turned, "sp", 1)
+    dq_own, dq_mate, p_own, p_far = attention(own, mate, far, far_mate, query_gain, key_gain)
+    p_far = swap_with(p_far, "sp", 2)
+    dq_mate = swap_with(dq_mate, "sp", 1)
+    p_mine, p_mate, partials = weight_partials(
+        turned, turned_mate, p_own, p_far, lax.axis_size("dp")
+    )
+    p_mate = swap_with(p_mate, "sp", 1)
+    summed = sum_pieces([partials[0]] + [swap_with(partials[m], "dp", m) for m in others])
+    input_grad, query_grad = token_outputs(p_mine, p_mate, weight_pieces, dq_own, dq_mate)
+    key_weight, value_weight = join_weight_grads(
+        summed, *[swap_with(summed, "sp", k) for k in range(1, 4)]
+    )
+    return input_grad[None], query_grad[None], key_weight, value_weight
+
+
 def solution(mesh):
+    sp_count, dp_count = mesh.shape["sp"], mesh.shape["dp"]
+    fast = sp_count == 4 and dp_count & (dp_count - 1) == 0
     return jax.shard_map(
-        on_device,
+        fast_device if fast else generic_device,
         mesh=mesh,
         in_specs=(
             P("dp", "sp", None),

time: 185 us -> 106 us (0.57)
  blocking collectives: 44.5 us -> 0 us
  Pallas kernels: 0 us -> 22.6 us
  local copies, waits for them, and re-layouts: 20.9 us -> 3.53 us
  between operations: 14.5 us -> 0.8 us
  matrix products: 12.8 us -> 0 us
  other arithmetic: 11.5 us -> 1.09 us
    ppermute x0 -> x24, waiting for transfers between devices: none -> 49 us  [swap_with(): return lax.ppermute(value, axis, [(i, i ^ k) for i in range(count)])]
    all_gather x2 -> x0, blocking collectives: 34.2 us -> none  [the longest x1 19 us: on_device(): all_grads = lax.all_gather(projection_gradient, 'sp', axis=0, tiled=True)]
    all_to_all x7 -> x0, starting transfers between devices: 29.5 us -> none  [the longest x1 6.35 us: on_device(): lax.all_to_all(key_positions, 'sp', split_axis=1, concat_axis=0, tiled=True)]
    ppermute x0 -> x24, starting transfers between devices: none -> 29 us  [swap_with(): return lax.ppermute(value, axis, [(i, i ^ k) for i in range(count)])]
    pallas_call x0 -> x7, Pallas kernels: none -> 22.6 us  [kernel_call(): pl.pallas_call(body, out_shape=out_shape, in_specs=[vmem] * len(args), ou...]
    all_to_all x7 -> x0, waiting for transfers between devices: 21.9 us -> none  [the longest x1 5.66 us: on_device(): lax.all_to_all(out_grad[0], 'sp', split_axis=1, concat_axis=0, tiled=True)]
    reduce_scatter x1 -> x0, waiting for transfers between devices: 15.1 us -> none  [on_device(): lax.psum_scatter(lax.dot_general(share_cols, all_grads, (((0,), (0,)), ((...]
    all_gather x1 -> x0, waiting for transfers between devices: 12.8 us -> none  [on_device(): lax.all_gather(joined_weight, 'dp', axis=0, tiled=True)]
  transfers between devices with their start and end apart: 9 -> 24, of which waited for: 8 -> 10; matrix products, arithmetic and copies ran while one was open for 14% -> 1% of each run, Pallas kernels for 0% -> 17%
where the time goes in v1:
time: 106 us
  waiting for transfers between devices  49 us (46%)
  starting transfers between devices  29 us (27%)
  Pallas kernels  22.6 us (21%)
  local copies, waits for them, and re-layouts  3.53 us (3%)
  other arithmetic  1.09 us (1%)
    ppermute x24, waiting for transfers between devices, swap_with(): return lax.ppermute(value, axis, [(i, i ^ k) for i in range(count)])  49 us
    ppermute x24, starting transfers between devices, swap_with(): return lax.ppermute(value, axis, [(i, i ^ k) for i in range(count)])  29 us
    pallas_call x7, Pallas kernels, kernel_call(): pl.pallas_call(body, out_shape=out_shape, in_specs=[vmem] * len(args), ou...  22.6 us
    unnamed x42, local copies, waits for them, and re-layouts  3.53 us
  transfers between devices with their start and end apart: 24, of which 10 were waited for; matrix products, arithmetic and copies ran while one was open for 1% of the time, Pallas kernels for 17%

profile of v1, /device:TPU:0, one launch (start us, length us, event | category | flops | bytes accessed | tf_op | source)
XLA Modules:
  0.0 106.0 jit_solution(11831547720655652593)
XLA Ops:
  0.6 2.0 %shard_map.156.xo_ref = bf16[2048,128]{1,0:T(8,128)(2,1)} custom-call(bf16[128,2048]{1,0:T(8,128)(2,1)} %bitcast.9), custom_call_target="tpu_custom_call" | custom-call | tf_op jit(solution)/shard_map/pallas_call | solution.py:236
  2.7 3.1 %collective-permute-start = (bf16[2048,128]{1,0:T(8,128)(2,1)}, bf16[2048,128]{1,0:T(8,128)(2,1)S(1)}, u32[]{:S(2)}, u32[]{:S(2)}) collective-permute-start(bf16[2048,128]{1,0:T(8,128)(2,1)} %shard_map.156.xo_ref), channel_id=1, source_target_pairs={{0,8},{8,0},{16,24},{24,16},{1,9},{9,1},{17,25},{25,17},{2,10},{10... | collective-permute-start | bytes 1572872 | tf_op jit(solution)/shard_map/ppermute | solution.py:253
  5.7 2.0 %shard_map.157 = (bf16[128,1280]{1,0:T(8,128)(2,1)}, bf16[128,1280]{1,0:T(8,128)(2,1)}, bf16[128,256]{1,0:T(8,128)(2,1)}, bf16[128,256]{1,0:T(8,128)(2,1)}) custom-call(bf16[128,1024]{1,0:T(8,128)(2,1)} %bitcast.10, bf16[128,1024]{1,0:T(8,128)(2,1)} %bitcast.11, bf16[128,256]{1,0:T(8,128)(2,1)} %bitcast.12, bf16[128,256]{1,0:T(8,128)(2,1)} %bitcast.13), custom_call_target="tpu_custom_call" | custom-call | tf_op jit(solution)/shard_map/pallas_call | solution.py:236
  7.7 0.0 collective-permute-start.1
  7.7 3.0 %collective-permute-start.2 = (bf16[128,256]{1,0:T(8,128)(2,1)}, bf16[128,256]{1,0:T(8,128)(2,1)S(1)}, u32[]{:S(2)}, u32[]{:S(2)}) collective-permute-start(bf16[128,256]{1,0:T(8,128)(2,1)} %get-tuple-element.28), channel_id=1, source_target_pairs={{0,16},{8,24},{16,0},{24,8},{1,17},{9,25},{17,1},{25,9},{2,18},{10... | collective-permute-start | bytes 196616 | tf_op jit(solution)/shard_map/ppermute | solution.py:253
  10.8 1.3 %collective-permute-start.3 = (bf16[128,256]{1,0:T(8,128)(2,1)}, bf16[128,256]{1,0:T(8,128)(2,1)S(1)}, u32[]{:S(2)}, u32[]{:S(2)}) collective-permute-start(bf16[128,256]{1,0:T(8,128)(2,1)} %get-tuple-element.29), channel_id=1, source_target_pairs={{0,24},{8,16},{16,8},{24,0},{1,25},{9,17},{17,9},{25,1},{2,26},{10... | collective-permute-start | bytes 196616 | tf_op jit(solution)/shard_map/ppermute | solution.py:253
  12.1 14.2 %collective-permute-done.2.refs_2_ = bf16[128,256]{1,0:T(8,128)(2,1)S(1)} collective-permute-done((bf16[128,256]{1,0:T(8,128)(2,1)}, bf16[128,256]{1,0:T(8,128)(2,1)S(1)}, u32[]{:S(2)}, u32[]{:S(2)}) %collective-permute-start.2) | collective-permute-done | bytes 65568 | tf_op jit(solution)/shard_map/ppermute | solution.py:253
  26.3 3.5 %collective-permute-done.3.refs_3_ = bf16[128,256]{1,0:T(8,128)(2,1)S(1)} collective-permute-done((bf16[128,256]{1,0:T(8,128)(2,1)}, bf16[128,256]{1,0:T(8,128)(2,1)S(1)}, u32[]{:S(2)}, u32[]{:S(2)}) %collective-permute-start.3) | collective-permute-done | bytes 65568 | tf_op jit(solution)/shard_map/ppermute | solution.py:253
  29.9 0.0 collective-permute-done.1.refs_1_
  29.9 0.6 copy-done.20
  30.5 0.1 copy-done.16
  30.6 8.5 %shard_map.158 = (bf16[128,512]{1,0:T(8,128)(2,1)}, bf16[128,512]{1,0:T(8,128)(2,1)}, f32[256,256]{1,0:T(8,128)}, bf16[256,256]{1,0:T(8,128)(2,1)}) custom-call(bf16[128,1280]{1,0:T(8,128)(2,1)} %get-tuple-element.26.refs_0_, bf16[128,1280]{1,0:T(8,128)(2,1)} %copy-done.16, bf16[128,256]{1,0:T(8,128)(2,1)} %copy-done.19, bf16[128,256]{1,0:T(8,128)(2,1)} %copy-done.20, ...), custom_call_target="tpu_custom_call" | custom-call | flops 671088640 | tf_op jit(solution)/shard_map/pallas_call | solution.py:236
  39.1 0.0 collective-permute-start.4
  39.1 1.8 %shard_map.160.rest_0_ = bf16[256,512]{1,0:T(8,128)(2,1)} custom-call(bf16[256,256]{1,0:T(8,128)(2,1)} %wk_ref.1, bf16[256,256]{1,0:T(8,128)(2,1)} %wv_ref.1), custom_call_target="tpu_custom_call" | custom-call | tf_op jit(solution)/shard_map/pallas_call | solution.py:236
  40.9 1.5 %collective-permute-start.10 = (bf16[256,512]{1,0:T(8,128)(2,1)}, bf16[256,512]{1,0:T(8,128)(2,1)S(1)}, u32[]{:S(2)}, u32[]{:S(2)}) collective-permute-start(bf16[256,512]{1,0:T(8,128)(2,1)} %shard_map.160.rest_0_), channel_id=1, source_target_pairs={{0,4},{1,5},{2,6},{3,7},{4,0},{5,1},{6,2},{7,3},{8,12},{9,13},{10,... | collective-permute-start | bytes 786440 | tf_op jit(solution)/shard_map/ppermute | solution.py:253
  42.4 0.0 collective-permute-start.11
  42.4 1.4 %collective-permute-start.12 = (bf16[256,512]{1,0:T(8,128)(2,1)}, bf16[256,512]{1,0:T(8,128)(2,1)S(1)}, u32[]{:S(2)}, u32[]{:S(2)}) collective-permute-start(bf16[256,512]{1,0:T(8,128)(2,1)} %shard_map.160.rest_0_), channel_id=1, source_target_pairs={{0,6},{1,7},{2,4},{3,5},{4,2},{5,3},{6,0},{7,1},{8,14},{9,15},{10,... | collective-permute-start | bytes 786440 | tf_op jit(solution)/shard_map/ppermute | solution.py:253
  43.9 2.0 %collective-permute-done.4.pf_ref = bf16[256,256]{1,0:T(8,128)(2,1)S(1)} collective-permute-done((bf16[256,256]{1,0:T(8,128)(2,1)}, bf16[256,256]{1,0:T(8,128)(2,1)S(1)}, u32[]{:S(2)}, u32[]{:S(2)}) %collective-permute-start.4) | collective-permute-done | bytes 131104 | tf_op jit(solution)/shard_map/ppermute | solution.py:253
  45.9 0.0 collective-permute-done.xm_ref
  45.9 0.6 copy-done.14
  46.6 0.2 copy-done.2
  46.8 2.9 %shard_map.159 = (bf16[128,256]{1,0:T(8,128)(2,1)}, bf16[128,256]{1,0:T(8,128)(2,1)}, bf16[256,256]{1,0:T(8,128)(2,1)}, bf16[256,256]{1,0:T(8,128)(2,1)}, bf16[2...) custom-call(bf16[2048,128]{1,0:T(8,128)(2,1)} %shard_map.156.xo_ref,, ...), custom_call_target="tpu_custom_call" | custom-call | flops 268435456 | tf_op jit(solution)/shard_map/pallas_call | solution.py:236
  49.6 0.0 collective-permute-start.14
  49.6 1.5 %collective-permute-start.15 = (bf16[256,256]{1,0:T(8,128)(2,1)}, bf16[256,256]{1,0:T(8,128)(2,1)S(1)}, u32[]{:S(2)}, u32[]{:S(2)}) collective-permute-start(bf16[256,256]{1,0:T(8,128)(2,1)} %get-tuple-element.40), channel_id=1, source_target_pairs={{0,2},{1,3},{2,0},{3,1},{4,6},{5,7},{6,4},{7,5},{8,10},{9,11},{10,... | collective-permute-start | bytes 393224 | tf_op jit(solution)/shard_map/ppermute | solution.py:253
  51.1 4.8 %collective-permute-done.10.rest_4_ = bf16[256,512]{1,0:T(8,128)(2,1)S(1)} collective-permute-done((bf16[256,512]{1,0:T(8,128)(2,1)}, bf16[256,512]{1,0:T(8,128)(2,1)S(1)}, u32[]{:S(2)}, u32[]{:S(2)}) %collective-permute-start.10) | collective-permute-done | bytes 262176 | tf_op jit(solution)/shard_map/ppermute | solution.py:253
  55.9 0.0 collective-permute-start.16
  55.9 2.5 %collective-permute-done.11.rest_5_ = bf16[256,512]{1,0:T(8,128)(2,1)S(1)} collective-permute-done((bf16[256,512]{1,0:T(8,128)(2,1)}, bf16[256,512]{1,0:T(8,128)(2,1)S(1)}, u32[]{:S(2)}, u32[]{:S(2)}) %collective-permute-start.11) | collective-permute-done | bytes 262176 | tf_op jit(solution)/shard_map/ppermute | solution.py:253
  58.4 0.5 collective-permute-start.17
  58.9 0.0 collective-permute-done.12.rest_6_
  58.9 1.8 %collective-permute-start.18 = (bf16[256,256]{1,0:T(8,128)(2,1)}, bf16[256,256]{1,0:T(8,128)(2,1)S(1)}, u32[]{:S(2)}, u32[]{:S(2)}) collective-permute-start(bf16[256,256]{1,0:T(8,128)(2,1)} %get-tuple-element.43), channel_id=1, source_target_pairs={{0,5},{1,4},{2,7},{3,6},{4,1},{5,0},{6,3},{7,2},{8,13},{9,12},{10,... | collective-permute-start | bytes 393224 | tf_op jit(solution)/shard_map/ppermute | solution.py:253
  60.7 0.0 collective-permute-done.14
  60.7 2.4 %collective-permute-start.19 = (bf16[256,256]{1,0:T(8,128)(2,1)}, bf16[256,256]{1,0:T(8,128)(2,1)S(1)}, u32[]{:S(2)}, u32[]{:S(2)}) collective-permute-start(bf16[256,256]{1,0:T(8,128)(2,1)} %get-tuple-element.44), channel_id=1, source_target_pairs={{0,6},{1,7},{2,4},{3,5},{4,2},{5,3},{6,0},{7,1},{8,14},{9,15},{10,... | collective-permute-start | bytes 393224 | tf_op jit(solution)/shard_map/ppermute | solution.py:253
  63.2 0.0 collective-permute-done.15
  63.2 0.0 collective-permute-start.20
  63.2 0.0 collective-permute-done.16
  63.2 2.6 %collective-permute-start.13 = (bf16[256,512]{1,0:T(8,128)(2,1)S(1)}, bf16[256,512]{1,0:T(8,128)(2,1)S(1)}, u32[]{:S(2)}, u32[]{:S(2)}) collective-permute-start(bf16[256,512]{1,0:T(8,128)(2,1)S(1)} %copy-done), channel_id=1, source_target_pairs={{0,7},{1,6},{2,5},{3,4},{4,3},{5,2},{6,1},{7,0},{8,15},{9,14},{10,... | collective-permute-start | bytes 786440 | tf_op jit(solution)/shard_map/ppermute | solution.py:253
  65.8 10.4 %collective-permute-done.17 = bf16[256,256]{1,0:T(8,128)(2,1)S(1)} collective-permute-done((bf16[256,256]{1,0:T(8,128)(2,1)}, bf16[256,256]{1,0:T(8,128)(2,1)S(1)}, u32[]{:S(2)}, u32[]{:S(2)}) %collective-permute-start.17) | collective-permute-done | bytes 131104 | tf_op jit(solution)/shard_map/ppermute | solution.py:253
  76.2 0.1 collective-permute-start.7
  76.3 2.7 %collective-permute-done.18 = bf16[256,256]{1,0:T(8,128)(2,1)S(1)} collective-permute-done((bf16[256,256]{1,0:T(8,128)(2,1)}, bf16[256,256]{1,0:T(8,128)(2,1)S(1)}, u32[]{:S(2)}, u32[]{:S(2)}) %collective-permute-start.18) | collective-permute-done | bytes 131104 | tf_op jit(solution)/shard_map/ppermute | solution.py:253
  79.0 1.5 %collective-permute-start.8 = (bf16[256,512]{1,0:T(8,128)(2,1)S(1)}, bf16[256,512]{1,0:T(8,128)(2,1)S(1)}, u32[]{:S(2)}, u32[]{:S(2)}) collective-permute-start(bf16[256,512]{1,0:T(8,128)(2,1)S(1)} %copy-done), channel_id=1, source_target_pairs={{0,2},{1,3},{2,0},{3,1},{4,6},{5,7},{6,4},{7,5},{8,10},{9,11},{10,... | collective-permute-start | bytes 786440 | tf_op jit(solution)/shard_map/ppermute | solution.py:253
  80.5 0.0 collective-permute-done.19
  80.5 0.0 collective-permute-start.9
  80.5 0.0 collective-permute-done.20
  80.5 1.7 %collective-permute-start.6 = (bf16[128,512]{1,0:T(8,128)(2,1)S(1)}, bf16[128,512]{1,0:T(8,128)(2,1)S(1)}, u32[]{:S(2)}, u32[]{:S(2)}) collective-permute-start(bf16[128,512]{1,0:T(8,128)(2,1)S(1)} %copy-done.17), channel_id=1, source_target_pairs={{0,8},{8,0},{16,24},{24,16},{1,9},{9,1},{17,25},{25,17},{2,10},{10... | collective-permute-start | bytes 393224 | tf_op jit(solution)/shard_map/ppermute | solution.py:253
  82.2 1.1 %add_convert_fusion.own_ref = bf16[256,256]{1,0:T(8,128)(2,1)S(1)} fusion(bf16[256,256]{1,0:T(8,128)(2,1)S(1)} %collective-permute-done.20, bf16[256,256]{1,0:T(8,128)(2,1)S(1)} %collective-permute-done.19, bf16[256,256]{1,0:T(8,128)(2,1)S(1)} %collective-permute-done.18, bf16[256,256]{1,0:T(8,128)(2,1)S(1)} %collective-permute-done.17, ...), kind=kLoop, calls=%fused_computation | loop fusion | flops 1048576 | bytes 1179648 | tf_op jit(solution)/shard_map/convert_element_type | solution.py:523
  83.3 0.0 collective-permute-done.13.rest_7_
  83.4 0.5 collective-permute-start.21
  83.8 0.0 collective-permute-done.7.rest_1_
  83.8 2.6 %collective-permute-start.22 = (bf16[256,256]{1,0:T(8,128)(2,1)S(1)}, bf16[256,256]{1,0:T(8,128)(2,1)S(1)}, u32[]{:S(2)}, u32[]{:S(2)}) collective-permute-start(bf16[256,256]{1,0:T(8,128)(2,1)S(1)} %add_convert_fusion.own_ref), channel_id=1, source_target_pairs={{0,16},{8,24},{16,0},{24,8},{1,17},{9,25},{17,1},{25,9},{2,18},{10... | collective-permute-start | bytes 393224 | tf_op jit(solution)/shard_map/ppermute | solution.py:253
  86.5 1.7 %collective-permute-done.8.rest_2_ = bf16[256,512]{1,0:T(8,128)(2,1)S(1)} collective-permute-done((bf16[256,512]{1,0:T(8,128)(2,1)S(1)}, bf16[256,512]{1,0:T(8,128)(2,1)S(1)}, u32[]{:S(2)}, u32[]{:S(2)}) %collective-permute-start.8) | collective-permute-done | bytes 262176 | tf_op jit(solution)/shard_map/ppermute | solution.py:253
  88.2 1.7 %collective-permute-start.23 = (bf16[256,256]{1,0:T(8,128)(2,1)S(1)}, bf16[256,256]{1,0:T(8,128)(2,1)S(1)}, u32[]{:S(2)}, u32[]{:S(2)}) collective-permute-start(bf16[256,256]{1,0:T(8,128)(2,1)S(1)} %add_convert_fusion.own_ref), channel_id=1, source_target_pairs={{0,24},{8,16},{16,8},{24,0},{1,25},{9,17},{17,9},{25,1},{2,26},{10... | collective-permute-start | bytes 393224 | tf_op jit(solution)/shard_map/ppermute | solution.py:253
  89.9 2.2 %collective-permute-done.9.rest_3_ = bf16[256,512]{1,0:T(8,128)(2,1)S(1)} collective-permute-done((bf16[256,512]{1,0:T(8,128)(2,1)S(1)}, bf16[256,512]{1,0:T(8,128)(2,1)S(1)}, u32[]{:S(2)}, u32[]{:S(2)}) %collective-permute-start.9) | collective-permute-done | bytes 262176 | tf_op jit(solution)/shard_map/ppermute | solution.py:253
  92.1 1.6 %collective-permute-start.5 = (bf16[128,256]{1,0:T(8,128)(2,1)S(1)}, bf16[128,256]{1,0:T(8,128)(2,1)S(1)}, u32[]{:S(2)}, u32[]{:S(2)}) collective-permute-start(bf16[128,256]{1,0:T(8,128)(2,1)S(1)} %copy-done.18), channel_id=1, source_target_pairs={{0,8},{8,0},{16,24},{24,16},{1,9},{9,1},{17,25},{25,17},{2,10},{10... | collective-permute-start | bytes 196616 | tf_op jit(solution)/shard_map/ppermute | solution.py:253
  93.7 0.0 collective-permute-done.6.dqm_ref
  93.7 4.8 %collective-permute-done.5.pm_ref = bf16[128,256]{1,0:T(8,128)(2,1)S(1)} collective-permute-done((bf16[128,256]{1,0:T(8,128)(2,1)S(1)}, bf16[128,256]{1,0:T(8,128)(2,1)S(1)}, u32[]{:S(2)}, u32[]{:S(2)}) %collective-permute-start.5) | collective-permute-done | bytes 65568 | tf_op jit(solution)/shard_map/ppermute | solution.py:253
  98.6 0.6 copy-done.15
  99.2 3.3 %shard_map.161 = (bf16[128,2048]{1,0:T(8,128)(2,1)}, bf16[128,1024]{1,0:T(8,128)(2,1)}) custom-call(bf16[128,256]{1,0:T(8,128)(2,1)} %get-tuple-element.32.p_ref, bf16[128,256]{1,0:T(8,128)(2,1)} %copy-done.15, bf16[128,512]{1,0:T(8,128)(2,1)} %get-tuple-element.34.dq_ref, bf16[128,512]{1,0:T(8,128)(2,1)} %copy-done.10, ...), custom_call_target="tpu_custom_call" | custom-call | flops 268435456 | tf_op jit(solution)/shard_map/pallas_call | solution.py:236
  102.5 0.0 collective-permute-done.21.mate_ref
  102.6 0.0 collective-permute-done.22.far_ref
  102.6 0.0 collective-permute-done.23.far_mate_ref
  102.6 0.6 copy-done.11
  103.2 0.1 copy-done.12
  103.2 0.6 copy-done.13
  103.9 2.1 %shard_map.162 = (f32[256,256]{1,0:T(8,128)}, f32[256,256]{1,0:T(8,128)}) custom-call(bf16[256,256]{1,0:T(8,128)(2,1)} %copy-done.1, bf16[256,256]{1,0:T(8,128)(2,1)} %copy-done.11, bf16[256,256]{1,0:T(8,128)(2,1)} %copy-done.12, bf16[256,256]{1,0:T(8,128)(2,1)} %copy-done.13), custom_call_target="tpu_custom_call" | custom-call | tf_op jit(solution)/shard_map/pallas_call | solution.py:236
  (34 shorter events, 0.1 us)
Async XLA Ops:
  2.7 43.3 %collective-permute-start = (bf16[2048,128]{1,0:T(8,128)(2,1)}, bf16[2048,128]{1,0:T(8,128)(2,1)S(1)}, u32[]{:S(2)}, u32[]{:S(2)}) collective-permute-start(bf16[2048,128]{1,0:T(8,128)(2,1)} %shard_map.156.xo_ref), channel_id=1, source_target_pairs={{0,8},{8,0},{16,24},{24,16},{1,9},{9,1},{17,25},{25,17},{2,10},{10... | collective-permute-start | bytes 1572872 | tf_op jit(solution)/shard_map/ppermute | solution.py:253
  7.7 22.1 %collective-permute-start.1 = (bf16[128,1280]{1,0:T(8,128)(2,1)}, bf16[128,1280]{1,0:T(8,128)(2,1)S(1)}, u32[]{:S(2)}, u32[]{:S(2)}) collective-permute-start(bf16[128,1280]{1,0:T(8,128)(2,1)} %get-tuple-element.27), channel_id=1, source_target_pairs={{0,8},{8,0},{16,24},{24,16},{1,9},{9,1},{17,25},{25,17},{2,10},{10... | collective-permute-start | bytes 983048 | tf_op jit(solution)/shard_map/ppermute | solution.py:253
  7.7 18.6 %collective-permute-start.2 = (bf16[128,256]{1,0:T(8,128)(2,1)}, bf16[128,256]{1,0:T(8,128)(2,1)S(1)}, u32[]{:S(2)}, u32[]{:S(2)}) collective-permute-start(bf16[128,256]{1,0:T(8,128)(2,1)} %get-tuple-element.28), channel_id=1, source_target_pairs={{0,16},{8,24},{16,0},{24,8},{1,17},{9,25},{17,1},{25,9},{2,18},{10... | collective-permute-start | bytes 196616 | tf_op jit(solution)/shard_map/ppermute | solution.py:253
  10.8 19.1 %collective-permute-start.3 = (bf16[128,256]{1,0:T(8,128)(2,1)}, bf16[128,256]{1,0:T(8,128)(2,1)S(1)}, u32[]{:S(2)}, u32[]{:S(2)}) collective-permute-start(bf16[128,256]{1,0:T(8,128)(2,1)} %get-tuple-element.29), channel_id=1, source_target_pairs={{0,24},{8,16},{16,8},{24,0},{1,25},{9,17},{17,9},{25,1},{2,26},{10... | collective-permute-start | bytes 196616 | tf_op jit(solution)/shard_map/ppermute | solution.py:253
  26.3 3.5 %copy-start.19 = (bf16[128,256]{1,0:T(8,128)(2,1)}, bf16[128,256]{1,0:T(8,128)(2,1)S(1)}, u32[]{:S(2)}) copy-start(bf16[128,256]{1,0:T(8,128)(2,1)S(1)} %collective-permute-done.2.refs_2_) | copy-start | bytes 196612
  29.9 0.6 copy-start.20
  29.9 0.7 copy-start.16
  39.1 6.8 %collective-permute-start.4 = (bf16[256,256]{1,0:T(8,128)(2,1)}, bf16[256,256]{1,0:T(8,128)(2,1)S(1)}, u32[]{:S(2)}, u32[]{:S(2)}) collective-permute-start(bf16[256,256]{1,0:T(8,128)(2,1)} %get-tuple-element.31), channel_id=1, source_target_pairs={{0,16},{8,24},{16,0},{24,8},{1,17},{9,25},{17,1},{25,9},{2,18},{10... | collective-permute-start | bytes 393224 | tf_op jit(solution)/shard_map/ppermute | solution.py:253
  40.9 15.0 %collective-permute-start.10 = (bf16[256,512]{1,0:T(8,128)(2,1)}, bf16[256,512]{1,0:T(8,128)(2,1)S(1)}, u32[]{:S(2)}, u32[]{:S(2)}) collective-permute-start(bf16[256,512]{1,0:T(8,128)(2,1)} %shard_map.160.rest_0_), channel_id=1, source_target_pairs={{0,4},{1,5},{2,6},{3,7},{4,0},{5,1},{6,2},{7,3},{8,12},{9,13},{10,... | collective-permute-start | bytes 786440 | tf_op jit(solution)/shard_map/ppermute | solution.py:253
  42.4 16.0 %collective-permute-start.11 = (bf16[256,512]{1,0:T(8,128)(2,1)}, bf16[256,512]{1,0:T(8,128)(2,1)S(1)}, u32[]{:S(2)}, u32[]{:S(2)}) collective-permute-start(bf16[256,512]{1,0:T(8,128)(2,1)} %shard_map.160.rest_0_), channel_id=1, source_target_pairs={{0,5},{1,4},{2,7},{3,6},{4,1},{5,0},{6,3},{7,2},{8,13},{9,12},{10,... | collective-permute-start | bytes 786440 | tf_op jit(solution)/shard_map/ppermute | solution.py:253
  42.4 16.5 %collective-permute-start.12 = (bf16[256,512]{1,0:T(8,128)(2,1)}, bf16[256,512]{1,0:T(8,128)(2,1)S(1)}, u32[]{:S(2)}, u32[]{:S(2)}) collective-permute-start(bf16[256,512]{1,0:T(8,128)(2,1)} %shard_map.160.rest_0_), channel_id=1, source_target_pairs={{0,6},{1,7},{2,4},{3,5},{4,2},{5,3},{6,0},{7,1},{8,14},{9,15},{10,... | collective-permute-start | bytes 786440 | tf_op jit(solution)/shard_map/ppermute | solution.py:253
  45.9 0.7 copy-start.14
  45.9 0.8 copy-start.2
  46.8 16.4 %copy-start = (bf16[256,512]{1,0:T(8,128)(2,1)S(1)}, bf16[256,512]{1,0:T(8,128)(2,1)}, u32[]{:S(2)}) copy-start(bf16[256,512]{1,0:T(8,128)(2,1)} %shard_map.160.rest_0_) | copy-start | bytes 786436
  46.8 33.8 %copy-start.17 = (bf16[128,512]{1,0:T(8,128)(2,1)S(1)}, bf16[128,512]{1,0:T(8,128)(2,1)}, u32[]{:S(2)}) copy-start(bf16[128,512]{1,0:T(8,128)(2,1)} %get-tuple-element.35) | copy-start | bytes 393220
  49.6 11.1 %collective-permute-start.14 = (bf16[256,256]{1,0:T(8,128)(2,1)}, bf16[256,256]{1,0:T(8,128)(2,1)S(1)}, u32[]{:S(2)}, u32[]{:S(2)}) collective-permute-start(bf16[256,256]{1,0:T(8,128)(2,1)} %get-tuple-element.39), channel_id=1, source_target_pairs={{0,1},{1,0},{2,3},{3,2},{4,5},{5,4},{6,7},{7,6},{8,9},{9,8},{10,11... | collective-permute-start | bytes 393224 | tf_op jit(solution)/shard_map/ppermute | solution.py:253
  49.6 13.6 %collective-permute-start.15 = (bf16[256,256]{1,0:T(8,128)(2,1)}, bf16[256,256]{1,0:T(8,128)(2,1)S(1)}, u32[]{:S(2)}, u32[]{:S(2)}) collective-permute-start(bf16[256,256]{1,0:T(8,128)(2,1)} %get-tuple-element.40), channel_id=1, source_target_pairs={{0,2},{1,3},{2,0},{3,1},{4,6},{5,7},{6,4},{7,5},{8,10},{9,11},{10,... | collective-permute-start | bytes 393224 | tf_op jit(solution)/shard_map/ppermute | solution.py:253
  55.9 27.4 %copy-start.3 = (bf16[256,512]{1,0:T(8,128)(2,1)}, bf16[256,512]{1,0:T(8,128)(2,1)S(1)}, u32[]{:S(2)}) copy-start(bf16[256,512]{1,0:T(8,128)(2,1)S(1)} %collective-permute-done.10.rest_4_) | copy-start | bytes 786436
  55.9 7.3 %collective-permute-start.16 = (bf16[256,256]{1,0:T(8,128)(2,1)}, bf16[256,256]{1,0:T(8,128)(2,1)S(1)}, u32[]{:S(2)}, u32[]{:S(2)}) collective-permute-start(bf16[256,256]{1,0:T(8,128)(2,1)} %get-tuple-element.41), channel_id=1, source_target_pairs={{0,3},{1,2},{2,1},{3,0},{4,7},{5,6},{6,5},{7,4},{8,11},{9,10},{10,... | collective-permute-start | bytes 393224 | tf_op jit(solution)/shard_map/ppermute | solution.py:253
  58.4 24.9 %copy-start.4 = (bf16[256,512]{1,0:T(8,128)(2,1)}, bf16[256,512]{1,0:T(8,128)(2,1)S(1)}, u32[]{:S(2)}) copy-start(bf16[256,512]{1,0:T(8,128)(2,1)S(1)} %collective-permute-done.11.rest_5_) | copy-start | bytes 786436
  58.4 17.8 %collective-permute-start.17 = (bf16[256,256]{1,0:T(8,128)(2,1)}, bf16[256,256]{1,0:T(8,128)(2,1)S(1)}, u32[]{:S(2)}, u32[]{:S(2)}) collective-permute-start(bf16[256,256]{1,0:T(8,128)(2,1)} %get-tuple-element.42), channel_id=1, source_target_pairs={{0,4},{1,5},{2,6},{3,7},{4,0},{5,1},{6,2},{7,3},{8,12},{9,13},{10,... | collective-permute-start | bytes 393224 | tf_op jit(solution)/shard_map/ppermute | solution.py:253
  58.9 24.4 %copy-start.5 = (bf16[256,512]{1,0:T(8,128)(2,1)}, bf16[256,512]{1,0:T(8,128)(2,1)S(1)}, u32[]{:S(2)}) copy-start(bf16[256,512]{1,0:T(8,128)(2,1)S(1)} %collective-permute-done.12.rest_6_) | copy-start | bytes 786436
  58.9 20.1 %collective-permute-start.18 = (bf16[256,256]{1,0:T(8,128)(2,1)}, bf16[256,256]{1,0:T(8,128)(2,1)S(1)}, u32[]{:S(2)}, u32[]{:S(2)}) collective-permute-start(bf16[256,256]{1,0:T(8,128)(2,1)} %get-tuple-element.43), channel_id=1, source_target_pairs={{0,5},{1,4},{2,7},{3,6},{4,1},{5,0},{6,3},{7,2},{8,13},{9,12},{10,... | collective-permute-start | bytes 393224 | tf_op jit(solution)/shard_map/ppermute | solution.py:253
  60.7 19.8 %collective-permute-start.19 = (bf16[256,256]{1,0:T(8,128)(2,1)}, bf16[256,256]{1,0:T(8,128)(2,1)S(1)}, u32[]{:S(2)}, u32[]{:S(2)}) collective-permute-start(bf16[256,256]{1,0:T(8,128)(2,1)} %get-tuple-element.44), channel_id=1, source_target_pairs={{0,6},{1,7},{2,4},{3,5},{4,2},{5,3},{6,0},{7,1},{8,14},{9,15},{10,... | collective-permute-start | bytes 393224 | tf_op jit(solution)/shard_map/ppermute | solution.py:253
  63.2 17.3 %collective-permute-start.20 = (bf16[256,256]{1,0:T(8,128)(2,1)}, bf16[256,256]{1,0:T(8,128)(2,1)S(1)}, u32[]{:S(2)}, u32[]{:S(2)}) collective-permute-start(bf16[256,256]{1,0:T(8,128)(2,1)} %get-tuple-element.45), channel_id=1, source_target_pairs={{0,7},{1,6},{2,5},{3,4},{4,3},{5,2},{6,1},{7,0},{8,15},{9,14},{10,... | collective-permute-start | bytes 393224 | tf_op jit(solution)/shard_map/ppermute | solution.py:253
  63.2 20.1 %collective-permute-start.13 = (bf16[256,512]{1,0:T(8,128)(2,1)S(1)}, bf16[256,512]{1,0:T(8,128)(2,1)S(1)}, u32[]{:S(2)}, u32[]{:S(2)}) collective-permute-start(bf16[256,512]{1,0:T(8,128)(2,1)S(1)} %copy-done), channel_id=1, source_target_pairs={{0,7},{1,6},{2,5},{3,4},{4,3},{5,2},{6,1},{7,0},{8,15},{9,14},{10,... | collective-permute-start | bytes 786440 | tf_op jit(solution)/shard_map/ppermute | solution.py:253
  76.2 7.6 %collective-permute-start.7 = (bf16[256,512]{1,0:T(8,128)(2,1)S(1)}, bf16[256,512]{1,0:T(8,128)(2,1)S(1)}, u32[]{:S(2)}, u32[]{:S(2)}) collective-permute-start(bf16[256,512]{1,0:T(8,128)(2,1)S(1)} %copy-done), channel_id=1, source_target_pairs={{0,1},{1,0},{2,3},{3,2},{4,5},{5,4},{6,7},{7,6},{8,9},{9,8},{10,11... | collective-permute-start | bytes 786440 | tf_op jit(solution)/shard_map/ppermute | solution.py:253
  79.0 9.2 %collective-permute-start.8 = (bf16[256,512]{1,0:T(8,128)(2,1)S(1)}, bf16[256,512]{1,0:T(8,128)(2,1)S(1)}, u32[]{:S(2)}, u32[]{:S(2)}) collective-permute-start(bf16[256,512]{1,0:T(8,128)(2,1)S(1)} %copy-done), channel_id=1, source_target_pairs={{0,2},{1,3},{2,0},{3,1},{4,6},{5,7},{6,4},{7,5},{8,10},{9,11},{10,... | collective-permute-start | bytes 786440 | tf_op jit(solution)/shard_map/ppermute | solution.py:253
  80.5 11.6 %collective-permute-start.9 = (bf16[256,512]{1,0:T(8,128)(2,1)S(1)}, bf16[256,512]{1,0:T(8,128)(2,1)S(1)}, u32[]{:S(2)}, u32[]{:S(2)}) collective-permute-start(bf16[256,512]{1,0:T(8,128)(2,1)S(1)} %copy-done), channel_id=1, source_target_pairs={{0,3},{1,2},{2,1},{3,0},{4,7},{5,6},{6,5},{7,4},{8,11},{9,10},{10,... | collective-permute-start | bytes 786440 | tf_op jit(solution)/shard_map/ppermute | solution.py:253
  80.5 13.2 %collective-permute-start.6 = (bf16[128,512]{1,0:T(8,128)(2,1)S(1)}, bf16[128,512]{1,0:T(8,128)(2,1)S(1)}, u32[]{:S(2)}, u32[]{:S(2)}) collective-permute-start(bf16[128,512]{1,0:T(8,128)(2,1)S(1)} %copy-done.17), channel_id=1, source_target_pairs={{0,8},{8,0},{16,24},{24,16},{1,9},{9,1},{17,25},{25,17},{2,10},{10... | collective-permute-start | bytes 393224 | tf_op jit(solution)/shard_map/ppermute | solution.py:253
  82.2 9.9 %copy-start.18 = (bf16[128,256]{1,0:T(8,128)(2,1)S(1)}, bf16[128,256]{1,0:T(8,128)(2,1)}, u32[]{:S(2)}) copy-start(bf16[128,256]{1,0:T(8,128)(2,1)} %get-tuple-element.33) | copy-start | bytes 196612
  83.3 19.2 %copy-start.1 = (bf16[256,256]{1,0:T(8,128)(2,1)}, bf16[256,256]{1,0:T(8,128)(2,1)S(1)}, u32[]{:S(2)}) copy-start(bf16[256,256]{1,0:T(8,128)(2,1)S(1)} %add_convert_fusion.own_ref) | copy-start | bytes 393220
  83.4 15.2 %copy-start.6 = (bf16[256,512]{1,0:T(8,128)(2,1)}, bf16[256,512]{1,0:T(8,128)(2,1)S(1)}, u32[]{:S(2)}) copy-start(bf16[256,512]{1,0:T(8,128)(2,1)S(1)} %collective-permute-done.13.rest_7_) | copy-start | bytes 786436
  83.4 19.2 %collective-permute-start.21 = (bf16[256,256]{1,0:T(8,128)(2,1)S(1)}, bf16[256,256]{1,0:T(8,128)(2,1)S(1)}, u32[]{:S(2)}, u32[]{:S(2)}) collective-permute-start(bf16[256,256]{1,0:T(8,128)(2,1)S(1)} %add_convert_fusion.own_ref), channel_id=1, source_target_pairs={{0,8},{8,0},{16,24},{24,16},{1,9},{9,1},{17,25},{25,17},{2,10},{10... | collective-permute-start | bytes 393224 | tf_op jit(solution)/shard_map/ppermute | solution.py:253
  83.8 14.7 %copy-start.7 = (bf16[256,512]{1,0:T(8,128)(2,1)}, bf16[256,512]{1,0:T(8,128)(2,1)S(1)}, u32[]{:S(2)}) copy-start(bf16[256,512]{1,0:T(8,128)(2,1)S(1)} %collective-permute-done.7.rest_1_) | copy-start | bytes 786436
  83.8 18.7 %collective-permute-start.22 = (bf16[256,256]{1,0:T(8,128)(2,1)S(1)}, bf16[256,256]{1,0:T(8,128)(2,1)S(1)}, u32[]{:S(2)}, u32[]{:S(2)}) collective-permute-start(bf16[256,256]{1,0:T(8,128)(2,1)S(1)} %add_convert_fusion.own_ref), channel_id=1, source_target_pairs={{0,16},{8,24},{16,0},{24,8},{1,17},{9,25},{17,1},{25,9},{2,18},{10... | collective-permute-start | bytes 393224 | tf_op jit(solution)/shard_map/ppermute | solution.py:253
  88.2 10.4 %copy-start.8 = (bf16[256,512]{1,0:T(8,128)(2,1)}, bf16[256,512]{1,0:T(8,128)(2,1)S(1)}, u32[]{:S(2)}) copy-start(bf16[256,512]{1,0:T(8,128)(2,1)S(1)} %collective-permute-done.8.rest_2_) | copy-start | bytes 786436
  88.2 14.4 %collective-permute-start.23 = (bf16[256,256]{1,0:T(8,128)(2,1)S(1)}, bf16[256,256]{1,0:T(8,128)(2,1)S(1)}, u32[]{:S(2)}, u32[]{:S(2)}) collective-permute-start(bf16[256,256]{1,0:T(8,128)(2,1)S(1)} %add_convert_fusion.own_ref), channel_id=1, source_target_pairs={{0,24},{8,16},{16,8},{24,0},{1,25},{9,17},{17,9},{25,1},{2,26},{10... | collective-permute-start | bytes 393224 | tf_op jit(solution)/shard_map/ppermute | solution.py:253
  92.1 6.5 %copy-start.9 = (bf16[256,512]{1,0:T(8,128)(2,1)}, bf16[256,512]{1,0:T(8,128)(2,1)S(1)}, u32[]{:S(2)}) copy-start(bf16[256,512]{1,0:T(8,128)(2,1)S(1)} %collective-permute-done.9.rest_3_) | copy-start | bytes 786436
  92.1 6.5 %collective-permute-start.5 = (bf16[128,256]{1,0:T(8,128)(2,1)S(1)}, bf16[128,256]{1,0:T(8,128)(2,1)S(1)}, u32[]{:S(2)}, u32[]{:S(2)}) collective-permute-start(bf16[128,256]{1,0:T(8,128)(2,1)S(1)} %copy-done.18), channel_id=1, source_target_pairs={{0,8},{8,0},{16,24},{24,16},{1,9},{9,1},{17,25},{25,17},{2,10},{10... | collective-permute-start | bytes 196616 | tf_op jit(solution)/shard_map/ppermute | solution.py:253
  93.7 4.9 %copy-start.10 = (bf16[128,512]{1,0:T(8,128)(2,1)}, bf16[128,512]{1,0:T(8,128)(2,1)S(1)}, u32[]{:S(2)}) copy-start(bf16[128,512]{1,0:T(8,128)(2,1)S(1)} %collective-permute-done.6.dqm_ref) | copy-start | bytes 393220
  98.6 0.6 copy-start.15
  102.5 0.7 copy-start.11
  102.6 0.7 copy-start.12
  103.2 0.6 copy-start.13

commit v2 on v1

--- a/solution.py
+++ b/solution.py
@@ -253,53 +253,82 @@
     return lax.ppermute(value, axis, [(i, i ^ k) for i in range(count)])
 
 
+def copy_call(body, out_shape, count, args):
+    anywhere = pl.BlockSpec(memory_space=pl.ANY)
+    vmem = pl.BlockSpec(memory_space=pltpu.VMEM)
+
+    def run(*refs):
+        sems = refs[-1]
+        copies = [
+            pltpu.make_async_copy(source, target, sems.at[i])
+            for i, (source, target) in enumerate(body(*refs[:-1]))
+        ]
+        for copy in copies:
+            copy.start()
+        for copy in copies:
+            copy.wait()
+
+    return pl.pallas_call(
+        run,
+        out_shape=out_shape,
+        in_specs=[anywhere] * len(args),
+        out_specs=jax.tree.map(lambda _: vmem, out_shape),
+        scratch_shapes=[pltpu.SemaphoreType.DMA((count,))],
+    )(*args)
+
+
+def lanes_of(half, width):
+    return pl.ds(pl.multiple_of(half * width, 128), width)
+
+
 def pack_heads(queries, keys, values, out_grad):
     rows, q_all = queries.shape
-    kv_half = keys.shape[1] // 2
-    q_half = q_all // 2
+    q_half, kv_half = q_all // 2, keys.shape[1] // 2
     width = 2 * q_half + 2 * kv_half
 
-    def body(q_ref, g_ref, k_ref, v_ref, own, mate, far, far_mate, buf):
+    def body(q_ref, g_ref, k_ref, v_ref, mate, far, far_mate):
         bit = lax.axis_index("sp") % 2
-        for d in range(2):
-            buf[d, :, :q_half] = q_ref[:, d * q_half : (d + 1) * q_half]
-            buf[d, :, q_half : 2 * q_half] = g_ref[:, d * q_half : (d + 1) * q_half]
-            parts = []
-            for h in range(kv_half // HEAD_CHANNELS):
-                lo = d * kv_half + h * HEAD_CHANNELS
-                parts += [k_ref[:, lo : lo + HEAD_CHANNELS], v_ref[:, lo : lo + HEAD_CHANNELS]]
-            buf[d, :, 2 * q_half :] = jnp.concatenate(parts, axis=1)
-        own[...] = buf[bit]
-        mate[...] = buf[1 - bit]
-        far[...] = buf[bit, :, 2 * q_half :]
-        far_mate[...] = buf[1 - bit, :, 2 * q_half :]
-
-    return kernel_call(
+        pairs = [
+            (q_ref.at[:, lanes_of(1 - bit, q_half)], mate.at[:, :q_half]),
+            (g_ref.at[:, lanes_of(1 - bit, q_half)], mate.at[:, q_half : 2 * q_half]),
+        ]
+        for out, half, lo in ((mate, 1 - bit, 2 * q_half), (far, bit, 0), (far_mate, 1 - bit, 0)):
+            lanes = lanes_of(half, kv_half)
+            pairs.append((k_ref.at[:, lanes], out.at[:, lo : lo + kv_half]))
+            pairs.append((v_ref.at[:, lanes], out.at[:, lo + kv_half : lo + 2 * kv_half]))
+        return pairs
+
+    return copy_call(
         body,
-        [shape_of((rows, width))] * 2 + [shape_of((rows, 2 * kv_half))] * 2,
-        [pltpu.VMEM((2, rows, width), bf16)],
+        [shape_of((rows, width))] + [shape_of((rows, 2 * kv_half))] * 2,
+        8,
         (queries, out_grad, keys, values),
     )
 
 
 def join_weights(key_matrix, value_matrix):
     rows, kv_width = key_matrix.shape
+    half = kv_width // 2
 
     def body(wk_ref, wv_ref, out):
-        for h in range(kv_width // HEAD_CHANNELS):
-            cols = slice(h * HEAD_CHANNELS, (h + 1) * HEAD_CHANNELS)
-            out[:, 2 * h * HEAD_CHANNELS : 2 * (h + 1) * HEAD_CHANNELS] = jnp.concatenate(
-                [wk_ref[:, cols], wv_ref[:, cols]], axis=1
-            )
-
-    return kernel_call(body, shape_of((rows, 2 * kv_width)), [], (key_matrix, value_matrix))
-
-
-def turn_inputs(token_in):
-    def body(x_ref, out):
-        out[...] = x_ref[...].T
-
-    return kernel_call(body, shape_of(token_in.shape[::-1]), [], (token_in,))
+        pairs = []
+        for d in range(2):
+            cols = slice(d * half, (d + 1) * half)
+            pairs.append((wk_ref.at[:, cols], out.at[:, 2 * d * half : (2 * d + 1) * half]))
+            pairs.append((wv_ref.at[:, cols], out.at[:, (2 * d + 1) * half : (2 * d + 2) * half]))
+        return pairs
+
+    return copy_call(body, shape_of((rows, 2 * kv_width)), 4, (key_matrix, value_matrix))
+
+
+def turn_inputs(own, mate):
+    rows, width = own.shape
+
+    def body(own_ref, mate_ref, out):
+        out[:, :rows] = own_ref[...].T
+        out[:, rows:] = mate_ref[...].T
+
+    return kernel_call(body, shape_of((width, 2 * rows)), [], (own, mate))
 
 
 def angle_tables(token_length):
@@ -316,39 +345,51 @@
     return tables
 
 
-def attention(own, mate, far, far_mate, query_gain, key_gain):
-    rows, width = own.shape
-    kv_width = far.shape[1]
-    q_width = (width - kv_width) // 2
+def attention(queries, out_grad, keys, values, mate, far, far_mate, query_gain, key_gain):
+    rows = queries.shape[0]
+    q_width = queries.shape[1] // 2
+    k_width = keys.shape[1] // 2
     pair = 2 * HEAD_CHANNELS
     heads = q_width // HEAD_CHANNELS
-    groups = kv_width // pair
+    groups = k_width // HEAD_CHANNELS
     per_group = heads // groups
-    q_chunks = q_width // pair
     half = 2 * rows
     tokens = 4 * rows
     tables = angle_tables(tokens)
 
     def body(*refs):
-        own_ref, mate_ref, far_ref, far_mate_ref, qg_ref, kg_ref = refs[:6]
-        row_cos, row_sin, col_cos, col_sin = refs[6:10]
-        dq_own, dq_mate, p_own, p_far = refs[10:14]
-        q_tok, kv_tok, qh, gh, kr, vv, q_inv, k_inv, dq_sc, dkv_sc, dq_out, p_sc = refs[14:]
+        q_ref, g_ref, k_ref, v_ref, mate_ref, far_ref, far_mate_ref = refs[:7]
+        qg_ref, kg_ref, row_cos, row_sin, col_cos, col_sin = refs[7:13]
+        dq_own, dq_mate, p_own, p_far = refs[13:17]
+        q_tok, kv_tok, qh, gh, kr, vv, q_inv, k_inv, dq_sc, dk_sc, dq_out, p_sc, sems = refs[17:]
         me = lax.axis_index("sp")
         bit = me % 2
         upper = me // 2
         q_own = pl.multiple_of(bit * rows, rows)
         q_mate = pl.multiple_of((1 - bit) * rows, rows)
-        q_tok[pl.ds(q_own, rows), :] = own_ref[:, : 2 * q_width]
-        q_tok[pl.ds(q_mate, rows), :] = mate_ref[:, : 2 * q_width]
-        for k, block in enumerate(
-            (own_ref[:, 2 * q_width :], mate_ref[:, 2 * q_width :], far_ref[...], far_mate_ref[...])
-        ):
-            kv_tok[pl.ds(pl.multiple_of((me ^ k) * rows, rows), rows), :] = block
+
+        def kv_rows(k):
+            return pl.ds(pl.multiple_of((me ^ k) * rows, rows), rows)
+
+        pairs = [
+            (far_ref, kv_tok.at[kv_rows(2), :]),
+            (far_mate_ref, kv_tok.at[kv_rows(3), :]),
+            (mate_ref.at[:, 2 * q_width :], kv_tok.at[kv_rows(1), :]),
+            (k_ref.at[:, lanes_of(bit, k_width)], kv_tok.at[kv_rows(0), :k_width]),
+            (v_ref.at[:, lanes_of(bit, k_width)], kv_tok.at[kv_rows(0), k_width:]),
+            (q_ref.at[:, lanes_of(bit, q_width)], q_tok.at[pl.ds(q_own, rows), :q_width]),
+            (g_ref.at[:, lanes_of(bit, q_width)], q_tok.at[pl.ds(q_own, rows), q_width:]),
+            (mate_ref.at[:, : 2 * q_width], q_tok.at[pl.ds(q_mate, rows), :]),
+        ]
+        copies = [
+            pltpu.make_async_copy(source, target, sems.at[i])
+            for i, (source, target) in enumerate(pairs)
+        ]
+        for copy in copies:
+            copy.start()
         lane = lax.broadcasted_iota(jnp.int32, (GRID, pair), 1)
         even = lane % 2 == 0
         by_row = lane % HEAD_CHANNELS < HEAD_CHANNELS // 2
-        first_head = lane < HEAD_CHANNELS
         seg_r = lax.broadcasted_iota(jnp.int32, (2 * pair, pair), 0) // HEAD_CHANNELS % 2
         seg_c = lax.broadcasted_iota(jnp.int32, (2 * pair, pair), 1) // HEAD_CHANNELS
         seg = jnp.where(seg_r == seg_c, 1.0 / HEAD_CHANNELS, 0.0).astype(bf16)
@@ -379,28 +420,32 @@
             return inv * (weighted - value * inv * inv * inner)
 
         q_rows = half // GRID
+        for copy in copies:
+            copy.wait()
         for r in range(tokens // GRID):
             at = slice(r * GRID, (r + 1) * GRID)
             cos, sin = angles_of(r)
-            for c in range(groups):
-                part = slice(c * pair, (c + 1) * pair)
-                raw = kv_tok[at, part]
-                inv, turned = forward(raw.astype(f32), k_gain, cos, sin)
+            for lo in range(0, k_width, pair):
+                part = slice(lo, lo + pair)
+                inv, turned = forward(kv_tok[at, part].astype(f32), k_gain, cos, sin)
                 k_inv[at, part] = inv
-                kr[c, at, :] = turned[:, :HEAD_CHANNELS]
-                vv[c, at, :] = raw[:, HEAD_CHANNELS:]
+                for u in range(2):
+                    g = lo // HEAD_CHANNELS + u
+                    kr[g, at, :] = turned[:, u * HEAD_CHANNELS : (u + 1) * HEAD_CHANNELS]
+                    begin = k_width + g * HEAD_CHANNELS
+                    vv[g, at, :] = kv_tok[at, begin : begin + HEAD_CHANNELS]
         for r in range(q_rows):
             at = slice(r * GRID, (r + 1) * GRID)
             cos, sin = angles_of(upper * q_rows + r)
-            for c in range(q_chunks):
-                part = slice(c * pair, (c + 1) * pair)
+            for lo in range(0, q_width, pair):
+                part = slice(lo, lo + pair)
                 inv, turned = forward(q_tok[at, part].astype(f32), q_gain, cos, sin)
                 q_inv[at, part] = inv
-                grad = q_tok[at, q_width + c * pair : q_width + (c + 1) * pair]
+                grad = q_tok[at, q_width + lo : q_width + lo + pair]
                 for u in range(2):
                     lanes = slice(u * HEAD_CHANNELS, (u + 1) * HEAD_CHANNELS)
-                    qh[2 * c + u, at, :] = turned[:, lanes]
-                    gh[2 * c + u, at, :] = grad[:, lanes]
+                    qh[lo // HEAD_CHANNELS + u, at, :] = turned[:, lanes]
+                    gh[lo // HEAD_CHANNELS + u, at, :] = grad[:, lanes]
 
         for g in range(groups):
             key_rot = kr[g]
@@ -422,72 +467,69 @@
                 first = h == g * per_group
                 key_acc = dk if first else key_acc + dk
                 value_acc = dv if first else value_acc + dv
-            dkv_sc[:, g * pair : (g + 1) * pair] = jnp.concatenate(
-                [key_acc * score_scale, value_acc], axis=1
-            )
+            lo = g * HEAD_CHANNELS
+            dk_sc[:, lo : lo + HEAD_CHANNELS] = key_acc * score_scale
+            p_sc[:, k_width + lo : k_width + lo + HEAD_CHANNELS] = value_acc
 
         for r in range(tokens // GRID):
             at = slice(r * GRID, (r + 1) * GRID)
             cos, sin = angles_of(r)
-            for c in range(groups):
-                part = slice(c * pair, (c + 1) * pair)
-                grad = dkv_sc[at, part]
+            for lo in range(0, k_width, pair):
+                part = slice(lo, lo + pair)
                 value = kv_tok[at, part].astype(f32)
-                result = backward(value, k_inv[at, part], grad, k_gain, cos, sin)
-                p_sc[at, part] = jnp.where(first_head, result, grad)
+                p_sc[at, part] = backward(value, k_inv[at, part], dk_sc[at, part], k_gain, cos, sin)
         p_own[...] = p_sc[pl.ds(pl.multiple_of(upper * half, half), half), :]
         p_far[...] = p_sc[pl.ds(pl.multiple_of((1 - upper) * half, half), half), :].astype(bf16)
         for r in range(q_rows):
             at = slice(r * GRID, (r + 1) * GRID)
             cos, sin = angles_of(upper * q_rows + r)
-            for c in range(q_chunks):
-                part = slice(c * pair, (c + 1) * pair)
+            for lo in range(0, q_width, pair):
+                part = slice(lo, lo + pair)
                 value = q_tok[at, part].astype(f32)
                 result = backward(value, q_inv[at, part], dq_sc[at, part], q_gain, cos, sin)
                 dq_out[at, part] = result.astype(bf16)
         dq_own[...] = dq_out[pl.ds(q_own, rows), :]
         dq_mate[...] = dq_out[pl.ds(q_mate, rows), :]
 
-    return kernel_call(
+    vmem = pl.BlockSpec(memory_space=pltpu.VMEM)
+    args = (queries, out_grad, keys, values, mate, far, far_mate)
+    small = (query_gain[None], key_gain[None], *[jnp.asarray(t) for t in tables])
+    return pl.pallas_call(
         body,
-        [shape_of((rows, q_width))] * 2
-        + [shape_of((half, kv_width), f32), shape_of((half, kv_width))],
-        [
+        out_shape=[shape_of((rows, q_width))] * 2
+        + [shape_of((half, 2 * k_width), f32), shape_of((half, 2 * k_width))],
+        in_specs=[pl.BlockSpec(memory_space=pl.ANY)] * len(args) + [vmem] * len(small),
+        out_specs=[vmem] * 4,
+        scratch_shapes=[
             pltpu.VMEM((half, 2 * q_width), bf16),
-            pltpu.VMEM((tokens, kv_width), bf16),
+            pltpu.VMEM((tokens, 2 * k_width), bf16),
             pltpu.VMEM((heads, half, HEAD_CHANNELS), bf16),
             pltpu.VMEM((heads, half, HEAD_CHANNELS), bf16),
             pltpu.VMEM((groups, tokens, HEAD_CHANNELS), bf16),
             pltpu.VMEM((groups, tokens, HEAD_CHANNELS), bf16),
             pltpu.VMEM((half, q_width), f32),
-            pltpu.VMEM((tokens, kv_width), f32),
+            pltpu.VMEM((tokens, k_width), f32),
             pltpu.VMEM((half, q_width), f32),
-            pltpu.VMEM((tokens, kv_width), f32),
+            pltpu.VMEM((tokens, k_width), f32),
             pltpu.VMEM((half, q_width), bf16),
-            pltpu.VMEM((tokens, kv_width), f32),
+            pltpu.VMEM((tokens, 2 * k_width), f32),
+            pltpu.SemaphoreType.DMA((8,)),
         ],
-        (
-            own,
-            mate,
-            far,
-            far_mate,
-            query_gain[None],
-            key_gain[None],
-            *[jnp.asarray(t) for t in tables],
+        cost_estimate=pl.CostEstimate(
+            flops=10 * heads * half * tokens * HEAD_CHANNELS, bytes_accessed=0, transcendentals=0
         ),
-        flops=10 * heads * half * tokens * HEAD_CHANNELS,
-    )
-
-
-def weight_partials(turned_own, turned_mate, p_own, p_far, dp_count):
-    feats, rows = turned_own.shape
-    half, cols = p_own.shape
+        compiler_params=pltpu.CompilerParams(vmem_limit_bytes=58 * 1024 * 1024),
+        name="attention",
+    )(*args, *small)
+
+
+def weight_partials(turned, p_own, p_far, dp_count):
+    feats, half = turned.shape
+    rows, cols = half // 2, p_own.shape[1]
     share = feats // dp_count
-
-    def body(xo_ref, xm_ref, po_ref, pf_ref, *rest):
-        mine_out, mate_out = rest[:2]
-        outs = rest[2 : 2 + dp_count]
-        x_all, p_sc, res = rest[2 + dp_count :]
+    chips = dp_count // 2
+
+    def body(x_ref, po_ref, pf_ref, mine_out, mate_out, own_out, send_out, p_sc):
         bit = lax.axis_index("sp") % 2
         mine = lax.axis_index("dp")
         p_sc[...] = (po_ref[...] + pf_ref[...].astype(f32)).astype(bf16)
@@ -495,52 +537,41 @@
         p_mate = p_sc[pl.ds(pl.multiple_of((1 - bit) * rows, rows), rows), :]
         mine_out[...] = p_mine
         mate_out[...] = p_mate
-        x_all[:, :rows] = xo_ref[...]
-        x_all[:, rows:] = xm_ref[...]
         p_all = jnp.concatenate([p_mine, p_mate], axis=0)
-        res[...] = dot(x_all[...], p_all, 1, 0).astype(bf16)
-        for m, out in enumerate(outs):
-            out[...] = res[pl.ds(pl.multiple_of((mine ^ m) * share, share), share), :]
-
-    outs = kernel_call(
-        body,
-        [shape_of((rows, cols))] * 2 + [shape_of((share, cols))] * dp_count,
-        [
-            pltpu.VMEM((feats, half), bf16),
-            pltpu.VMEM((half, cols), bf16),
-            pltpu.VMEM((feats, cols), bf16),
-        ],
-        (turned_own, turned_mate, p_own, p_far),
-        flops=2 * feats * half * cols,
-    )
-    return outs[0], outs[1], outs[2:]
-
-
-def sum_pieces(pieces):
-    total = pieces[0].astype(f32)
-    for piece in pieces[1:]:
-        total = total + piece.astype(f32)
-    return total.astype(bf16)
-
-
-def join_weight_grads(own, mate, far, far_mate):
-    rows, cols = own.shape
-    pair = 2 * HEAD_CHANNELS
-    groups = cols // pair
-
-    def body(own_ref, mate_ref, far_ref, far_mate_ref, k_out, v_out, buf):
-        bit = lax.axis_index("sp") % 2
-        buf[bit] = own_ref[...].astype(f32) + far_ref[...].astype(f32)
-        buf[1 - bit] = mate_ref[...].astype(f32) + far_mate_ref[...].astype(f32)
-        parts = [buf[d, :, g * pair : (g + 1) * pair] for d in range(2) for g in range(groups)]
-        k_out[...] = jnp.concatenate([p[:, :HEAD_CHANNELS] for p in parts], axis=1)
-        v_out[...] = jnp.concatenate([p[:, HEAD_CHANNELS:] for p in parts], axis=1)
+        for out, flip in ((send_out, 1), (own_out, 0)):
+            for m in range(chips):
+                start = pl.multiple_of((mine ^ (2 * m + flip)) * share, share)
+                out[m] = dot(x_ref[pl.ds(start, share), :], p_all, 1, 0).astype(bf16)
 
     return kernel_call(
         body,
-        [shape_of((rows, cols), f32)] * 2,
-        [pltpu.VMEM((2, rows, cols), f32)],
-        (own, mate, far, far_mate),
+        [shape_of((rows, cols))] * 2 + [shape_of((chips, share, cols))] * 2,
+        [pltpu.VMEM((half, cols), bf16)],
+        (turned, p_own, p_far),
+        flops=2 * feats * half * cols,
+    )
+
+
+def sum_over_devices(own, sent):
+    received = swap_with(sent, "dp", 1)
+    chips = own.shape[0]
+    paired = [own[m].astype(f32) + received[m].astype(f32) for m in range(chips)]
+    total = paired[0]
+    for m in range(1, chips):
+        total = total + swap_with(paired[m].astype(bf16), "dp", 2 * m).astype(f32)
+    return total.astype(bf16)
+
+
+def join_weight_grads(own, mate, far, far_mate):
+    half = own.shape[1] // 2
+    here = own.astype(f32) + far.astype(f32)
+    there = mate.astype(f32) + far_mate.astype(f32)
+    even = lax.axis_index("sp") % 2 == 0
+    first = jnp.where(even, here, there)
+    second = jnp.where(even, there, here)
+    return (
+        jnp.concatenate([first[:, :half], second[:, :half]], axis=1),
+        jnp.concatenate([first[:, half:], second[:, half:]], axis=1),
     )
 
 
@@ -599,23 +630,25 @@
 def fast_body(
     inputs, queries, keys, values, out_grad, query_gain, key_gain, key_matrix, value_matrix
 ):
-    others = range(1, lax.axis_size("dp"))
-    own, mate, far, far_mate = pack_heads(queries, keys, values, out_grad)
+    dp_count = lax.axis_size("dp")
+    mate, far, far_mate = pack_heads(queries, keys, values, out_grad)
     mate = swap_with(mate, "sp", 1)
     far = swap_with(far, "sp", 2)
     far_mate = swap_with(far_mate, "sp", 3)
     joined_weight = join_weights(key_matrix, value_matrix)
-    weight_pieces = [joined_weight] + [swap_with(joined_weight, "dp", m) for m in others]
-    turned = turn_inputs(inputs)
-    turned_mate = swap_with(turned, "sp", 1)
-    dq_own, dq_mate, p_own, p_far = attention(own, mate, far, far_mate, query_gain, key_gain)
+    weight_pieces = [joined_weight] + [
+        swap_with(joined_weight, "dp", m) for m in range(1, dp_count)
+    ]
+    mate_inputs = swap_with(inputs, "sp", 1)
+    dq_own, dq_mate, p_own, p_far = attention(
+        queries, out_grad, keys, values, mate, far, far_mate, query_gain, key_gain
+    )
     p_far = swap_with(p_far, "sp", 2)
     dq_mate = swap_with(dq_mate, "sp", 1)
-    p_mine, p_mate, partials = weight_partials(
-        turned, turned_mate, p_own, p_far, lax.axis_size("dp")
-    )
+    turned = turn_inputs(inputs, mate_inputs)
+    p_mine, p_mate, own, sent = weight_partials(turned, p_own, p_far, dp_count)
+    summed = sum_over_devices(own, sent)
     p_mate = swap_with(p_mate, "sp", 1)
-    summed = sum_pieces([partials[0]] + [swap_with(partials[m], "dp", m) for m in others])
     input_grad, query_grad = token_outputs(p_mine, p_mate, weight_pieces, dq_own, dq_mate)
     key_weight, value_weight = join_weight_grads(
         summed, *[swap_with(summed, "sp", k) for k in range(1, 4)]

time: 106 us -> 103 us (0.972)
  starting transfers between devices: 29 us -> 25.4 us
  waiting for transfers between devices: 49 us -> 50.6 us
  Pallas kernels: 22.6 us -> 21.4 us
    pallas_call x7 -> x3, Pallas kernels: 22.6 us -> 8.47 us  [kernel_call(): pl.pallas_call(body, out_shape=out_shape, in_specs=[vmem] * len(args), ou...]
    pallas_call x0 -> x3, Pallas kernels: none -> 12.9 us  [the longest x1 9.39 us: attention(): pl.pallas_call(body, out_shape=[shape_of((rows, q_width))] * 2 + [shape_o...]
    ppermute x24 -> x21, starting transfers between devices: 29 us -> 25.4 us  [swap_with(): return lax.ppermute(value, axis, [(i, i ^ k) for i in range(count)])]
    ppermute x24 -> x21, waiting for transfers between devices: 49 us -> 50.6 us  [swap_with(): return lax.ppermute(value, axis, [(i, i ^ k) for i in range(count)])]
    concatenate x0 -> x2, other arithmetic: none -> 1.44 us  [the longest x1 0.72 us: join_weight_grads(): jnp.concatenate([first[:, half:], second[:, half:]], axis=1)]
    unnamed x42 -> x34, local copies, waits for them, and re-layouts: 3.53 us -> 2.82 us
  transfers between devices with their start and end apart: 24 -> 21, of which waited for: 10 -> 9; matrix products, arithmetic and copies ran while one was open for 1% -> 0% of each run, Pallas kernels for 17% -> 18%
where the time goes in v2:
time: 103 us
  waiting for transfers between devices  50.6 us (49%)
  starting transfers between devices  25.4 us (25%)
  Pallas kernels  21.4 us (21%)
  local copies, waits for them, and re-layouts  2.85 us (3%)
  other arithmetic  1.7 us (2%)
    ppermute x21, waiting for transfers between devices, swap_with(): return lax.ppermute(value, axis, [(i, i ^ k) for i in range(count)])  50.6 us
    ppermute x21, starting transfers between devices, swap_with(): return lax.ppermute(value, axis, [(i, i ^ k) for i in range(count)])  25.4 us
    pallas_call x1, Pallas kernels, attention(): pl.pallas_call(body, out_shape=[shape_of((rows, q_width))] * 2 + [shape_o...  9.39 us
    pallas_call x3, Pallas kernels, kernel_call(): pl.pallas_call(body, out_shape=out_shape, in_specs=[vmem] * len(args), ou...  8.47 us
    pallas_call x2, Pallas kernels, copy_call(): pl.pallas_call(run, out_shape=out_shape, in_specs=[anywhere] * len(args),...  3.53 us
    unnamed x34, local copies, waits for them, and re-layouts  2.82 us
  transfers between devices with their start and end apart: 21, of which 9 were waited for; matrix products, arithmetic and copies ran while one was open for 0% of the time, Pallas kernels for 18%

profile of v2, /device:TPU:0, one launch (start us, length us, event | category | flops | bytes accessed | tf_op | source)
XLA Modules:
  0.0 102.8 jit_solution(8012883071047934114)
XLA Ops:
  0.6 3.1 %collective-permute-start = (bf16[128,2048]{1,0:T(8,128)(2,1)}, bf16[128,2048]{1,0:T(8,128)(2,1)S(1)}, u32[]{:S(2)}, u32[]{:S(2)}) collective-permute-start(bf16[128,2048]{1,0:T(8,128)(2,1)} %bitcast.23), channel_id=1, source_target_pairs={{0,8},{8,0},{16,24},{24,16},{1,9},{9,1},{17,25},{25,17},{2,10},{10... | collective-permute-start | bytes 1572872 | tf_op jit(solution)/shard_map/ppermute | solution.py:253
  3.7 1.8 %shard_map.157 = (bf16[128,1280]{1,0:T(8,128)(2,1)}, bf16[128,256]{1,0:T(8,128)(2,1)}, bf16[128,256]{1,0:T(8,128)(2,1)}) custom-call(bf16[128,1024]{1,0:T(8,128)(2,1)} %bitcast.25, bf16[128,1024]{1,0:T(8,128)(2,1)} %bitcast.27, bf16[128,256]{1,0:T(8,128)(2,1)} %bitcast.29, bf16[128,256]{1,0:T(8,128)(2,1)} %bitcast.31), custom_call_target="tpu_custom_call" | custom-call | tf_op jit(solution)/shard_map/pallas_call | solution.py:271
  5.6 0.1 collective-permute-start.1
  5.7 3.0 %collective-permute-start.2 = (bf16[128,256]{1,0:T(8,128)(2,1)}, bf16[128,256]{1,0:T(8,128)(2,1)S(1)}, u32[]{:S(2)}, u32[]{:S(2)}) collective-permute-start(bf16[128,256]{1,0:T(8,128)(2,1)} %get-tuple-element.18), channel_id=1, source_target_pairs={{0,16},{8,24},{16,0},{24,8},{1,17},{9,25},{17,1},{25,9},{2,18},{10... | collective-permute-start | bytes 196616 | tf_op jit(solution)/shard_map/ppermute | solution.py:253
  8.7 1.3 %collective-permute-start.3 = (bf16[128,256]{1,0:T(8,128)(2,1)}, bf16[128,256]{1,0:T(8,128)(2,1)S(1)}, u32[]{:S(2)}, u32[]{:S(2)}) collective-permute-start(bf16[128,256]{1,0:T(8,128)(2,1)} %get-tuple-element.19), channel_id=1, source_target_pairs={{0,24},{8,16},{16,8},{24,0},{1,25},{9,17},{17,9},{25,1},{2,26},{10... | collective-permute-start | bytes 196616 | tf_op jit(solution)/shard_map/ppermute | solution.py:253
  10.0 14.4 %collective-permute-done.2.refs_5_ = bf16[128,256]{1,0:T(8,128)(2,1)S(1)} collective-permute-done((bf16[128,256]{1,0:T(8,128)(2,1)}, bf16[128,256]{1,0:T(8,128)(2,1)S(1)}, u32[]{:S(2)}, u32[]{:S(2)}) %collective-permute-start.2) | collective-permute-done | bytes 65568 | tf_op jit(solution)/shard_map/ppermute | solution.py:253
  24.4 3.5 %collective-permute-done.3.refs_6_ = bf16[128,256]{1,0:T(8,128)(2,1)S(1)} collective-permute-done((bf16[128,256]{1,0:T(8,128)(2,1)}, bf16[128,256]{1,0:T(8,128)(2,1)S(1)}, u32[]{:S(2)}, u32[]{:S(2)}) %collective-permute-start.3) | collective-permute-done | bytes 65568 | tf_op jit(solution)/shard_map/ppermute | solution.py:253
  27.9 0.0 collective-permute-done.1.refs_4_
  27.9 0.6 copy-done.16
  28.5 0.1 copy-done.13
  28.6 9.4 %attention.1 = (bf16[128,512]{1,0:T(8,128)(2,1)}, bf16[128,512]{1,0:T(8,128)(2,1)}, f32[256,256]{1,0:T(8,128)}, bf16[256,256]{1,0:T(8,128)(2,1)}) custom-call(bf16[128,1024]{1,0:T(8,128)(2,1)} %bitcast.26, bf16[128,1024]{1,0:T(8,128)(2,1)} %bitcast.28, bf16[128,256]{1,0:T(8,128)(2,1)} %bitcast.30, bf16[128,256]{1,0:T(8,128)(2,1)} %bitcast.32, ...), custom_call_target="tpu_custom_call" | custom-call | flops 671088640 | tf_op jit(solution)/shard_map/attention/pallas_call | solution.py:497
  38.0 0.1 collective-permute-start.4
  38.1 0.0 collective-permute-done.mate_ref
  38.1 0.0 copy-start.2
  38.2 0.8 copy-done.2
  38.9 2.5 %shard_map.156.x_ref = bf16[2048,256]{1,0:T(8,128)(2,1)} custom-call(bf16[128,2048]{1,0:T(8,128)(2,1)} %bitcast.24, bf16[128,2048]{1,0:T(8,128)(2,1)} %copy-done.2), custom_call_target="tpu_custom_call" | custom-call | tf_op jit(solution)/shard_map/pallas_call | solution.py:236
  41.4 3.5 %collective-permute-done.4.pf_ref = bf16[256,256]{1,0:T(8,128)(2,1)S(1)} collective-permute-done((bf16[256,256]{1,0:T(8,128)(2,1)}, bf16[256,256]{1,0:T(8,128)(2,1)S(1)}, u32[]{:S(2)}, u32[]{:S(2)}) %collective-permute-start.4) | collective-permute-done | bytes 131104 | tf_op jit(solution)/shard_map/ppermute | solution.py:253
  44.9 0.7 copy-done.11
  45.6 2.6 %shard_map.158 = (bf16[128,256]{1,0:T(8,128)(2,1)}, bf16[128,256]{1,0:T(8,128)(2,1)}, bf16[4,256,256]{2,1,0:T(8,128)(2,1)}, bf16[4,256,256]{2,1,0:T(8,128)(2,1)}) custom-call(bf16[2048,256]{1,0:T(8,128)(2,1)} %shard_map.156.x_ref, f32[256,256]{1,0:T(8,128)} %get-tuple-element.20.po_ref, bf16[256,256]{1,0:T(8,128)(2,1)} %copy-done.11), custom_call_target="tpu_custom_call" | custom-call | flops 268435456 | tf_op jit(solution)/shard_map/pallas_call | solution.py:236
  48.2 0.0 collective-permute-start.14
  48.2 1.7 %shard_map.159.rest_0_ = bf16[256,512]{1,0:T(8,128)(2,1)} custom-call(bf16[256,256]{1,0:T(8,128)(2,1)} %refs_0_.1, bf16[256,256]{1,0:T(8,128)(2,1)} %refs_1_.1), custom_call_target="tpu_custom_call" | custom-call | tf_op jit(solution)/shard_map/pallas_call | solution.py:271
  49.9 1.6 %collective-permute-start.10 = (bf16[256,512]{1,0:T(8,128)(2,1)}, bf16[256,512]{1,0:T(8,128)(2,1)S(1)}, u32[]{:S(2)}, u32[]{:S(2)}) collective-permute-start(bf16[256,512]{1,0:T(8,128)(2,1)} %shard_map.159.rest_0_), channel_id=1, source_target_pairs={{0,4},{1,5},{2,6},{3,7},{4,0},{5,1},{6,2},{7,3},{8,12},{9,13},{10,... | collective-permute-start | bytes 786440 | tf_op jit(solution)/shard_map/ppermute | solution.py:253
  51.5 0.3 collective-permute-start.11
  51.8 2.5 %collective-permute-start.12 = (bf16[256,512]{1,0:T(8,128)(2,1)}, bf16[256,512]{1,0:T(8,128)(2,1)S(1)}, u32[]{:S(2)}, u32[]{:S(2)}) collective-permute-start(bf16[256,512]{1,0:T(8,128)(2,1)} %shard_map.159.rest_0_), channel_id=1, source_target_pairs={{0,6},{1,7},{2,4},{3,5},{4,2},{5,3},{6,0},{7,1},{8,14},{9,15},{10,... | collective-permute-start | bytes 786440 | tf_op jit(solution)/shard_map/ppermute | solution.py:253
  54.3 0.0 collective-permute-done.14
  54.3 0.1 fusion.5
  54.4 0.6 collective-permute-start.15
  55.0 0.5 collective-permute-start.16
  55.5 9.5 %collective-permute-done.10.rest_4_ = bf16[256,512]{1,0:T(8,128)(2,1)S(1)} collective-permute-done((bf16[256,512]{1,0:T(8,128)(2,1)}, bf16[256,512]{1,0:T(8,128)(2,1)S(1)}, u32[]{:S(2)}, u32[]{:S(2)}) %collective-permute-start.10) | collective-permute-done | bytes 262176 | tf_op jit(solution)/shard_map/ppermute | solution.py:253
  65.0 2.5 %collective-permute-start.17 = (bf16[256,256]{1,0:T(8,128)(2,1)S(1)}, bf16[256,256]{1,0:T(8,128)(2,1)S(1)}, u32[]{:S(2)}, u32[]{:S(2)}) collective-permute-start(bf16[256,256]{1,0:T(8,128)(2,1)S(1)} %get-tuple-element.31), channel_id=1, source_target_pairs={{0,6},{1,7},{2,4},{3,5},{4,2},{5,3},{6,0},{7,1},{8,14},{9,15},{10,... | collective-permute-start | bytes 393224 | tf_op jit(solution)/shard_map/ppermute | solution.py:253
  67.5 5.1 %collective-permute-done.11.rest_5_ = bf16[256,512]{1,0:T(8,128)(2,1)S(1)} collective-permute-done((bf16[256,512]{1,0:T(8,128)(2,1)}, bf16[256,512]{1,0:T(8,128)(2,1)S(1)}, u32[]{:S(2)}, u32[]{:S(2)}) %collective-permute-start.11) | collective-permute-done | bytes 262176 | tf_op jit(solution)/shard_map/ppermute | solution.py:253
  72.6 2.7 %collective-permute-start.13 = (bf16[256,512]{1,0:T(8,128)(2,1)S(1)}, bf16[256,512]{1,0:T(8,128)(2,1)S(1)}, u32[]{:S(2)}, u32[]{:S(2)}) collective-permute-start(bf16[256,512]{1,0:T(8,128)(2,1)S(1)} %copy-done), channel_id=1, source_target_pairs={{0,7},{1,6},{2,5},{3,4},{4,3},{5,2},{6,1},{7,0},{8,15},{9,14},{10,... | collective-permute-start | bytes 786440 | tf_op jit(solution)/shard_map/ppermute | solution.py:253
  75.3 0.0 collective-permute-done.12.rest_6_
  75.3 0.0 collective-permute-start.7
  75.3 0.0 collective-permute-done.15
  75.3 0.6 collective-permute-start.8
  75.9 0.0 collective-permute-done.16
  75.9 1.3 %collective-permute-start.9 = (bf16[256,512]{1,0:T(8,128)(2,1)S(1)}, bf16[256,512]{1,0:T(8,128)(2,1)S(1)}, u32[]{:S(2)}, u32[]{:S(2)}) collective-permute-start(bf16[256,512]{1,0:T(8,128)(2,1)S(1)} %copy-done), channel_id=1, source_target_pairs={{0,3},{1,2},{2,1},{3,0},{4,7},{5,6},{6,5},{7,4},{8,11},{9,10},{10,... | collective-permute-start | bytes 786440 | tf_op jit(solution)/shard_map/ppermute | solution.py:253
  77.2 0.0 collective-permute-done.17
  77.2 0.0 collective-permute-start.6
  77.2 0.1 fusion.2
  77.3 0.0 copy-done.3
  77.3 0.0 copy-done.4
  77.3 0.0 copy-done.5
  77.3 4.7 %collective-permute-done.13.rest_7_ = bf16[256,512]{1,0:T(8,128)(2,1)S(1)} collective-permute-done((bf16[256,512]{1,0:T(8,128)(2,1)S(1)}, bf16[256,512]{1,0:T(8,128)(2,1)S(1)}, u32[]{:S(2)}, u32[]{:S(2)}) %collective-permute-start.13) | collective-permute-done | bytes 262176 | tf_op jit(solution)/shard_map/ppermute | solution.py:253
  82.0 0.0 collective-permute-start.18
  82.0 0.0 collective-permute-done.7.rest_1_
  82.0 2.9 %collective-permute-start.19 = (bf16[256,256]{1,0:T(8,128)(2,1)S(1)}, bf16[256,256]{1,0:T(8,128)(2,1)S(1)}, u32[]{:S(2)}, u32[]{:S(2)}) collective-permute-start(bf16[256,256]{1,0:T(8,128)(2,1)S(1)} %fusion.2), channel_id=1, source_target_pairs={{0,8},{8,0},{16,24},{24,16},{1,9},{9,1},{17,25},{25,17},{2,10},{10... | collective-permute-start | bytes 393224 | tf_op jit(solution)/shard_map/ppermute | solution.py:253
  85.0 3.6 %collective-permute-done.8.rest_2_ = bf16[256,512]{1,0:T(8,128)(2,1)S(1)} collective-permute-done((bf16[256,512]{1,0:T(8,128)(2,1)S(1)}, bf16[256,512]{1,0:T(8,128)(2,1)S(1)}, u32[]{:S(2)}, u32[]{:S(2)}) %collective-permute-start.8) | collective-permute-done | bytes 262176 | tf_op jit(solution)/shard_map/ppermute | solution.py:253
  88.6 2.4 %collective-permute-start.20 = (bf16[256,256]{1,0:T(8,128)(2,1)S(1)}, bf16[256,256]{1,0:T(8,128)(2,1)S(1)}, u32[]{:S(2)}, u32[]{:S(2)}) collective-permute-start(bf16[256,256]{1,0:T(8,128)(2,1)S(1)} %fusion.2), channel_id=1, source_target_pairs={{0,24},{8,16},{16,8},{24,0},{1,25},{9,17},{17,9},{25,1},{2,26},{10... | collective-permute-start | bytes 393224 | tf_op jit(solution)/shard_map/ppermute | solution.py:253
  91.0 1.2 %collective-permute-done.9.rest_3_ = bf16[256,512]{1,0:T(8,128)(2,1)S(1)} collective-permute-done((bf16[256,512]{1,0:T(8,128)(2,1)S(1)}, bf16[256,512]{1,0:T(8,128)(2,1)S(1)}, u32[]{:S(2)}, u32[]{:S(2)}) %collective-permute-start.9) | collective-permute-done | bytes 262176 | tf_op jit(solution)/shard_map/ppermute | solution.py:253
  92.2 0.0 collective-permute-start.5
  92.2 0.0 collective-permute-done.6.dqm_ref
  92.2 5.0 %collective-permute-done.5.pm_ref = bf16[128,256]{1,0:T(8,128)(2,1)S(1)} collective-permute-done((bf16[128,256]{1,0:T(8,128)(2,1)}, bf16[128,256]{1,0:T(8,128)(2,1)S(1)}, u32[]{:S(2)}, u32[]{:S(2)}) %collective-permute-start.5) | collective-permute-done | bytes 65568 | tf_op jit(solution)/shard_map/ppermute | solution.py:253
  97.3 0.0 copy-done.7
  97.3 0.0 copy-done.9
  97.3 0.6 copy-done.12
  97.9 3.3 %shard_map.160 = (bf16[128,2048]{1,0:T(8,128)(2,1)}, bf16[128,1024]{1,0:T(8,128)(2,1)}) custom-call(bf16[128,256]{1,0:T(8,128)(2,1)} %get-tuple-element.22.p_ref, bf16[128,256]{1,0:T(8,128)(2,1)} %copy-done.12, bf16[128,512]{1,0:T(8,128)(2,1)} %get-tuple-element.24.dq_ref, bf16[128,512]{1,0:T(8,128)(2,1)} %copy-done.10, ...), custom_call_target="tpu_custom_call" | custom-call | flops 268435456 | tf_op jit(solution)/shard_map/pallas_call | solution.py:236
  101.2 0.0 collective-permute-done.18
  101.2 0.0 collective-permute-done.19
  101.2 0.0 collective-permute-done.20
  101.2 0.1 fusion.4
  101.4 0.7 pad_maximum_fusion.1
  102.1 0.7 pad_maximum_fusion
  (24 shorter events, 0.1 us)
Async XLA Ops:
  0.6 37.5 %collective-permute-start = (bf16[128,2048]{1,0:T(8,128)(2,1)}, bf16[128,2048]{1,0:T(8,128)(2,1)S(1)}, u32[]{:S(2)}, u32[]{:S(2)}) collective-permute-start(bf16[128,2048]{1,0:T(8,128)(2,1)} %bitcast.23), channel_id=1, source_target_pairs={{0,8},{8,0},{16,24},{24,16},{1,9},{9,1},{17,25},{25,17},{2,10},{10... | collective-permute-start | bytes 1572872 | tf_op jit(solution)/shard_map/ppermute | solution.py:253
  5.6 22.3 %collective-permute-start.1 = (bf16[128,1280]{1,0:T(8,128)(2,1)}, bf16[128,1280]{1,0:T(8,128)(2,1)S(1)}, u32[]{:S(2)}, u32[]{:S(2)}) collective-permute-start(bf16[128,1280]{1,0:T(8,128)(2,1)} %get-tuple-element.17), channel_id=1, source_target_pairs={{0,8},{8,0},{16,24},{24,16},{1,9},{9,1},{17,25},{25,17},{2,10},{10... | collective-permute-start | bytes 983048 | tf_op jit(solution)/shard_map/ppermute | solution.py:253
  5.7 18.7 %collective-permute-start.2 = (bf16[128,256]{1,0:T(8,128)(2,1)}, bf16[128,256]{1,0:T(8,128)(2,1)S(1)}, u32[]{:S(2)}, u32[]{:S(2)}) collective-permute-start(bf16[128,256]{1,0:T(8,128)(2,1)} %get-tuple-element.18), channel_id=1, source_target_pairs={{0,16},{8,24},{16,0},{24,8},{1,17},{9,25},{17,1},{25,9},{2,18},{10... | collective-permute-start | bytes 196616 | tf_op jit(solution)/shard_map/ppermute | solution.py:253
  8.7 19.2 %collective-permute-start.3 = (bf16[128,256]{1,0:T(8,128)(2,1)}, bf16[128,256]{1,0:T(8,128)(2,1)S(1)}, u32[]{:S(2)}, u32[]{:S(2)}) collective-permute-start(bf16[128,256]{1,0:T(8,128)(2,1)} %get-tuple-element.19), channel_id=1, source_target_pairs={{0,24},{8,16},{16,8},{24,0},{1,25},{9,17},{17,9},{25,1},{2,26},{10... | collective-permute-start | bytes 196616 | tf_op jit(solution)/shard_map/ppermute | solution.py:253
  24.4 3.5 %copy-start.15 = (bf16[128,256]{1,0:T(8,128)(2,1)}, bf16[128,256]{1,0:T(8,128)(2,1)S(1)}, u32[]{:S(2)}) copy-start(bf16[128,256]{1,0:T(8,128)(2,1)S(1)} %collective-permute-done.2.refs_5_) | copy-start | bytes 196612
  27.9 0.6 copy-start.16
  27.9 0.7 copy-start.13
  38.0 6.9 %collective-permute-start.4 = (bf16[256,256]{1,0:T(8,128)(2,1)}, bf16[256,256]{1,0:T(8,128)(2,1)S(1)}, u32[]{:S(2)}, u32[]{:S(2)}) collective-permute-start(bf16[256,256]{1,0:T(8,128)(2,1)} %get-tuple-element.21), channel_id=1, source_target_pairs={{0,16},{8,24},{16,0},{24,8},{1,17},{9,25},{17,1},{25,9},{2,18},{10... | collective-permute-start | bytes 393224 | tf_op jit(solution)/shard_map/ppermute | solution.py:253
  38.1 0.8 copy-start.2
  44.9 0.7 copy-start.11
  48.2 6.1 %copy-start.1 = (bf16[4,256,256]{2,1,0:T(8,128)(2,1)S(1)}, bf16[4,256,256]{2,1,0:T(8,128)(2,1)}, u32[]{:S(2)}) copy-start(bf16[4,256,256]{2,1,0:T(8,128)(2,1)} %get-tuple-element.28) | copy-start | bytes 1572868
  48.2 6.1 %collective-permute-start.14 = (bf16[4,256,256]{2,1,0:T(8,128)(2,1)}, bf16[4,256,256]{2,1,0:T(8,128)(2,1)S(1)}, u32[]{:S(2)}, u32[]{:S(2)}) collective-permute-start(bf16[4,256,256]{2,1,0:T(8,128)(2,1)} %get-tuple-element.29), channel_id=1, source_target_pairs={{0,1},{1,0},{2,3},{3,2},{4,5},{5,4},{6,7},{7,6},{8,9},{9,8},{10,11... | collective-permute-start | bytes 1572872 | tf_op jit(solution)/shard_map/ppermute | solution.py:253
  49.9 15.1 %collective-permute-start.10 = (bf16[256,512]{1,0:T(8,128)(2,1)}, bf16[256,512]{1,0:T(8,128)(2,1)S(1)}, u32[]{:S(2)}, u32[]{:S(2)}) collective-permute-start(bf16[256,512]{1,0:T(8,128)(2,1)} %shard_map.159.rest_0_), channel_id=1, source_target_pairs={{0,4},{1,5},{2,6},{3,7},{4,0},{5,1},{6,2},{7,3},{8,12},{9,13},{10,... | collective-permute-start | bytes 786440 | tf_op jit(solution)/shard_map/ppermute | solution.py:253
  51.5 21.1 %collective-permute-start.11 = (bf16[256,512]{1,0:T(8,128)(2,1)}, bf16[256,512]{1,0:T(8,128)(2,1)S(1)}, u32[]{:S(2)}, u32[]{:S(2)}) collective-permute-start(bf16[256,512]{1,0:T(8,128)(2,1)} %shard_map.159.rest_0_), channel_id=1, source_target_pairs={{0,5},{1,4},{2,7},{3,6},{4,1},{5,0},{6,3},{7,2},{8,13},{9,12},{10,... | collective-permute-start | bytes 786440 | tf_op jit(solution)/shard_map/ppermute | solution.py:253
  51.8 23.5 %collective-permute-start.12 = (bf16[256,512]{1,0:T(8,128)(2,1)}, bf16[256,512]{1,0:T(8,128)(2,1)S(1)}, u32[]{:S(2)}, u32[]{:S(2)}) collective-permute-start(bf16[256,512]{1,0:T(8,128)(2,1)} %shard_map.159.rest_0_), channel_id=1, source_target_pairs={{0,6},{1,7},{2,4},{3,5},{4,2},{5,3},{6,0},{7,1},{8,14},{9,15},{10,... | collective-permute-start | bytes 786440 | tf_op jit(solution)/shard_map/ppermute | solution.py:253
  54.3 18.3 %copy-start = (bf16[256,512]{1,0:T(8,128)(2,1)S(1)}, bf16[256,512]{1,0:T(8,128)(2,1)}, u32[]{:S(2)}) copy-start(bf16[256,512]{1,0:T(8,128)(2,1)} %shard_map.159.rest_0_) | copy-start | bytes 786436
  54.3 22.9 %copy-start.14 = (bf16[128,512]{1,0:T(8,128)(2,1)S(1)}, bf16[128,512]{1,0:T(8,128)(2,1)}, u32[]{:S(2)}) copy-start(bf16[128,512]{1,0:T(8,128)(2,1)} %get-tuple-element.25) | copy-start | bytes 393220
  54.4 21.0 %collective-permute-start.15 = (bf16[256,256]{1,0:T(8,128)(2,1)S(1)}, bf16[256,256]{1,0:T(8,128)(2,1)S(1)}, u32[]{:S(2)}, u32[]{:S(2)}) collective-permute-start(bf16[256,256]{1,0:T(8,128)(2,1)S(1)} %get-tuple-element.30), channel_id=1, source_target_pairs={{0,2},{1,3},{2,0},{3,1},{4,6},{5,7},{6,4},{7,5},{8,10},{9,11},{10,... | collective-permute-start | bytes 393224 | tf_op jit(solution)/shard_map/ppermute | solution.py:253
  55.0 21.0 %collective-permute-start.16 = (bf16[256,256]{1,0:T(8,128)(2,1)S(1)}, bf16[256,256]{1,0:T(8,128)(2,1)S(1)}, u32[]{:S(2)}, u32[]{:S(2)}) collective-permute-start(bf16[256,256]{1,0:T(8,128)(2,1)S(1)} %get-tuple-element.32), channel_id=1, source_target_pairs={{0,4},{1,5},{2,6},{3,7},{4,0},{5,1},{6,2},{7,3},{8,12},{9,13},{10,... | collective-permute-start | bytes 393224 | tf_op jit(solution)/shard_map/ppermute | solution.py:253
  65.0 12.3 %copy-start.3 = (bf16[256,512]{1,0:T(8,128)(2,1)}, bf16[256,512]{1,0:T(8,128)(2,1)S(1)}, u32[]{:S(2)}) copy-start(bf16[256,512]{1,0:T(8,128)(2,1)S(1)} %collective-permute-done.10.rest_4_) | copy-start | bytes 786436
  65.0 12.2 %collective-permute-start.17 = (bf16[256,256]{1,0:T(8,128)(2,1)S(1)}, bf16[256,256]{1,0:T(8,128)(2,1)S(1)}, u32[]{:S(2)}, u32[]{:S(2)}) collective-permute-start(bf16[256,256]{1,0:T(8,128)(2,1)S(1)} %get-tuple-element.31), channel_id=1, source_target_pairs={{0,6},{1,7},{2,4},{3,5},{4,2},{5,3},{6,0},{7,1},{8,14},{9,15},{10,... | collective-permute-start | bytes 393224 | tf_op jit(solution)/shard_map/ppermute | solution.py:253
  72.6 4.7 %copy-start.4 = (bf16[256,512]{1,0:T(8,128)(2,1)}, bf16[256,512]{1,0:T(8,128)(2,1)S(1)}, u32[]{:S(2)}) copy-start(bf16[256,512]{1,0:T(8,128)(2,1)S(1)} %collective-permute-done.11.rest_5_) | copy-start | bytes 786436
  72.6 9.4 %collective-permute-start.13 = (bf16[256,512]{1,0:T(8,128)(2,1)S(1)}, bf16[256,512]{1,0:T(8,128)(2,1)S(1)}, u32[]{:S(2)}, u32[]{:S(2)}) collective-permute-start(bf16[256,512]{1,0:T(8,128)(2,1)S(1)} %copy-done), channel_id=1, source_target_pairs={{0,7},{1,6},{2,5},{3,4},{4,3},{5,2},{6,1},{7,0},{8,15},{9,14},{10,... | collective-permute-start | bytes 786440 | tf_op jit(solution)/shard_map/ppermute | solution.py:253
  75.3 2.0 %copy-start.5 = (bf16[256,512]{1,0:T(8,128)(2,1)}, bf16[256,512]{1,0:T(8,128)(2,1)S(1)}, u32[]{:S(2)}) copy-start(bf16[256,512]{1,0:T(8,128)(2,1)S(1)} %collective-permute-done.12.rest_6_) | copy-start | bytes 786436
  75.3 6.7 %collective-permute-start.7 = (bf16[256,512]{1,0:T(8,128)(2,1)S(1)}, bf16[256,512]{1,0:T(8,128)(2,1)S(1)}, u32[]{:S(2)}, u32[]{:S(2)}) collective-permute-start(bf16[256,512]{1,0:T(8,128)(2,1)S(1)} %copy-done), channel_id=1, source_target_pairs={{0,1},{1,0},{2,3},{3,2},{4,5},{5,4},{6,7},{7,6},{8,9},{9,8},{10,11... | collective-permute-start | bytes 786440 | tf_op jit(solution)/shard_map/ppermute | solution.py:253
  75.3 13.3 %collective-permute-start.8 = (bf16[256,512]{1,0:T(8,128)(2,1)S(1)}, bf16[256,512]{1,0:T(8,128)(2,1)S(1)}, u32[]{:S(2)}, u32[]{:S(2)}) collective-permute-start(bf16[256,512]{1,0:T(8,128)(2,1)S(1)} %copy-done), channel_id=1, source_target_pairs={{0,2},{1,3},{2,0},{3,1},{4,6},{5,7},{6,4},{7,5},{8,10},{9,11},{10,... | collective-permute-start | bytes 786440 | tf_op jit(solution)/shard_map/ppermute | solution.py:253
  75.9 16.3 %collective-permute-start.9 = (bf16[256,512]{1,0:T(8,128)(2,1)S(1)}, bf16[256,512]{1,0:T(8,128)(2,1)S(1)}, u32[]{:S(2)}, u32[]{:S(2)}) collective-permute-start(bf16[256,512]{1,0:T(8,128)(2,1)S(1)} %copy-done), channel_id=1, source_target_pairs={{0,3},{1,2},{2,1},{3,0},{4,7},{5,6},{6,5},{7,4},{8,11},{9,10},{10,... | collective-permute-start | bytes 786440 | tf_op jit(solution)/shard_map/ppermute | solution.py:253
  77.2 15.0 %collective-permute-start.6 = (bf16[128,512]{1,0:T(8,128)(2,1)S(1)}, bf16[128,512]{1,0:T(8,128)(2,1)S(1)}, u32[]{:S(2)}, u32[]{:S(2)}) collective-permute-start(bf16[128,512]{1,0:T(8,128)(2,1)S(1)} %copy-done.14), channel_id=1, source_target_pairs={{0,8},{8,0},{16,24},{24,16},{1,9},{9,1},{17,25},{25,17},{2,10},{10... | collective-permute-start | bytes 393224 | tf_op jit(solution)/shard_map/ppermute | solution.py:253
  82.0 15.2 %copy-start.6 = (bf16[256,512]{1,0:T(8,128)(2,1)}, bf16[256,512]{1,0:T(8,128)(2,1)S(1)}, u32[]{:S(2)}) copy-start(bf16[256,512]{1,0:T(8,128)(2,1)S(1)} %collective-permute-done.13.rest_7_) | copy-start | bytes 786436
  82.0 19.2 %collective-permute-start.18 = (bf16[256,256]{1,0:T(8,128)(2,1)S(1)}, bf16[256,256]{1,0:T(8,128)(2,1)S(1)}, u32[]{:S(2)}, u32[]{:S(2)}) collective-permute-start(bf16[256,256]{1,0:T(8,128)(2,1)S(1)} %fusion.2), channel_id=1, source_target_pairs={{0,16},{8,24},{16,0},{24,8},{1,17},{9,25},{17,1},{25,9},{2,18},{10... | collective-permute-start | bytes 393224 | tf_op jit(solution)/shard_map/ppermute | solution.py:253
  82.0 15.2 %copy-start.7 = (bf16[256,512]{1,0:T(8,128)(2,1)}, bf16[256,512]{1,0:T(8,128)(2,1)S(1)}, u32[]{:S(2)}) copy-start(bf16[256,512]{1,0:T(8,128)(2,1)S(1)} %collective-permute-done.7.rest_1_) | copy-start | bytes 786436
  82.0 19.2 %collective-permute-start.19 = (bf16[256,256]{1,0:T(8,128)(2,1)S(1)}, bf16[256,256]{1,0:T(8,128)(2,1)S(1)}, u32[]{:S(2)}, u32[]{:S(2)}) collective-permute-start(bf16[256,256]{1,0:T(8,128)(2,1)S(1)} %fusion.2), channel_id=1, source_target_pairs={{0,8},{8,0},{16,24},{24,16},{1,9},{9,1},{17,25},{25,17},{2,10},{10... | collective-permute-start | bytes 393224 | tf_op jit(solution)/shard_map/ppermute | solution.py:253
  88.6 8.6 %copy-start.8 = (bf16[256,512]{1,0:T(8,128)(2,1)}, bf16[256,512]{1,0:T(8,128)(2,1)S(1)}, u32[]{:S(2)}) copy-start(bf16[256,512]{1,0:T(8,128)(2,1)S(1)} %collective-permute-done.8.rest_2_) | copy-start | bytes 786436
  88.6 12.6 %collective-permute-start.20 = (bf16[256,256]{1,0:T(8,128)(2,1)S(1)}, bf16[256,256]{1,0:T(8,128)(2,1)S(1)}, u32[]{:S(2)}, u32[]{:S(2)}) collective-permute-start(bf16[256,256]{1,0:T(8,128)(2,1)S(1)} %fusion.2), channel_id=1, source_target_pairs={{0,24},{8,16},{16,8},{24,0},{1,25},{9,17},{17,9},{25,1},{2,26},{10... | collective-permute-start | bytes 393224 | tf_op jit(solution)/shard_map/ppermute | solution.py:253
  92.2 5.1 %copy-start.9 = (bf16[256,512]{1,0:T(8,128)(2,1)}, bf16[256,512]{1,0:T(8,128)(2,1)S(1)}, u32[]{:S(2)}) copy-start(bf16[256,512]{1,0:T(8,128)(2,1)S(1)} %collective-permute-done.9.rest_3_) | copy-start | bytes 786436
  92.2 5.0 %collective-permute-start.5 = (bf16[128,256]{1,0:T(8,128)(2,1)}, bf16[128,256]{1,0:T(8,128)(2,1)S(1)}, u32[]{:S(2)}, u32[]{:S(2)}) collective-permute-start(bf16[128,256]{1,0:T(8,128)(2,1)} %get-tuple-element.23), channel_id=1, source_target_pairs={{0,8},{8,0},{16,24},{24,16},{1,9},{9,1},{17,25},{25,17},{2,10},{10... | collective-permute-start | bytes 196616 | tf_op jit(solution)/shard_map/ppermute | solution.py:253
  92.2 5.1 %copy-start.10 = (bf16[128,512]{1,0:T(8,128)(2,1)}, bf16[128,512]{1,0:T(8,128)(2,1)S(1)}, u32[]{:S(2)}) copy-start(bf16[128,512]{1,0:T(8,128)(2,1)S(1)} %collective-permute-done.6.dqm_ref) | copy-start | bytes 393220
  97.3 0.6 copy-start.12

commit v3 on v2

--- a/solution.py
+++ b/solution.py
@@ -231,17 +231,28 @@
     )
 
 
-def kernel_call(body, out_shape, scratch, args, flops=0):
+MIB = 1024 * 1024
+
+
+def in_vmem(value):
+    return pltpu.with_memory_space_constraint(value, pltpu.VMEM)
+
+
+def kernel_call(body, out_shape, scratch, args, flops=0, limit=12 * MIB):
     vmem = pl.BlockSpec(memory_space=pltpu.VMEM)
     return pl.pallas_call(
         body,
         out_shape=out_shape,
         in_specs=[vmem] * len(args),
-        out_specs=jax.tree.map(lambda _: vmem, out_shape),
+        out_specs=[vmem] * len(out_shape),
         scratch_shapes=scratch,
         cost_estimate=pl.CostEstimate(flops=flops, bytes_accessed=0, transcendentals=0),
-        compiler_params=pltpu.CompilerParams(vmem_limit_bytes=58 * 1024 * 1024),
-    )(*args)
+        compiler_params=pltpu.CompilerParams(vmem_limit_bytes=limit),
+    )(*[in_vmem(arg) for arg in args])
+
+
+def held(shape, dtype=bf16):
+    return pltpu.VMEM(shape, dtype)
 
 
 def shape_of(shape, dtype=bf16):
@@ -254,9 +265,6 @@
 
 
 def copy_call(body, out_shape, count, args):
-    anywhere = pl.BlockSpec(memory_space=pl.ANY)
-    vmem = pl.BlockSpec(memory_space=pltpu.VMEM)
-
     def run(*refs):
         sems = refs[-1]
         copies = [
@@ -271,54 +279,67 @@
     return pl.pallas_call(
         run,
         out_shape=out_shape,
-        in_specs=[anywhere] * len(args),
-        out_specs=jax.tree.map(lambda _: vmem, out_shape),
+        in_specs=[pl.BlockSpec(memory_space=pltpu.HBM)] * len(args),
+        out_specs=[pl.BlockSpec(memory_space=pltpu.VMEM)] * len(out_shape),
         scratch_shapes=[pltpu.SemaphoreType.DMA((count,))],
-    )(*args)
+        compiler_params=pltpu.CompilerParams(vmem_limit_bytes=4 * MIB),
+    )(*[pltpu.with_memory_space_constraint(arg, pltpu.HBM) for arg in args])
 
 
 def lanes_of(half, width):
     return pl.ds(pl.multiple_of(half * width, 128), width)
+
+
+def head_copies(refs, out, half, q_half, kv_half):
+    pairs = []
+    lo = 0
+    for ref, width in zip(refs, (q_half, q_half, kv_half, kv_half)):
+        pairs.append((ref.at[:, lanes_of(half, width)], out.at[:, lo : lo + width]))
+        lo += width
+    return pairs
 
 
 def pack_heads(queries, keys, values, out_grad):
     rows, q_all = queries.shape
     q_half, kv_half = q_all // 2, keys.shape[1] // 2
-    width = 2 * q_half + 2 * kv_half
 
     def body(q_ref, g_ref, k_ref, v_ref, mate, far, far_mate):
         bit = lax.axis_index("sp") % 2
-        pairs = [
-            (q_ref.at[:, lanes_of(1 - bit, q_half)], mate.at[:, :q_half]),
-            (g_ref.at[:, lanes_of(1 - bit, q_half)], mate.at[:, q_half : 2 * q_half]),
-        ]
-        for out, half, lo in ((mate, 1 - bit, 2 * q_half), (far, bit, 0), (far_mate, 1 - bit, 0)):
+        pairs = head_copies((q_ref, g_ref, k_ref, v_ref), mate, 1 - bit, q_half, kv_half)
+        for out, half in ((far, bit), (far_mate, 1 - bit)):
             lanes = lanes_of(half, kv_half)
-            pairs.append((k_ref.at[:, lanes], out.at[:, lo : lo + kv_half]))
-            pairs.append((v_ref.at[:, lanes], out.at[:, lo + kv_half : lo + 2 * kv_half]))
+            pairs.append((k_ref.at[:, lanes], out.at[:, :kv_half]))
+            pairs.append((v_ref.at[:, lanes], out.at[:, kv_half:]))
         return pairs
 
     return copy_call(
         body,
-        [shape_of((rows, width))] + [shape_of((rows, 2 * kv_half))] * 2,
+        [held((rows, 2 * q_half + 2 * kv_half))] + [held((rows, 2 * kv_half))] * 2,
         8,
         (queries, out_grad, keys, values),
     )
 
 
-def join_weights(key_matrix, value_matrix):
-    rows, kv_width = key_matrix.shape
-    half = kv_width // 2
-
-    def body(wk_ref, wv_ref, out):
-        pairs = []
+def pack_own(queries, keys, values, out_grad, key_matrix, value_matrix, query_gain, key_gain):
+    rows, q_all = queries.shape
+    q_half, kv_half = q_all // 2, keys.shape[1] // 2
+
+    def body(q_ref, g_ref, k_ref, v_ref, wk_ref, wv_ref, qg_ref, kg_ref, own, weight, qg_out, kg_out):
+        bit = lax.axis_index("sp") % 2
+        pairs = head_copies((q_ref, g_ref, k_ref, v_ref), own, bit, q_half, kv_half)
         for d in range(2):
-            cols = slice(d * half, (d + 1) * half)
-            pairs.append((wk_ref.at[:, cols], out.at[:, 2 * d * half : (2 * d + 1) * half]))
-            pairs.append((wv_ref.at[:, cols], out.at[:, (2 * d + 1) * half : (2 * d + 2) * half]))
-        return pairs
-
-    return copy_call(body, shape_of((rows, 2 * kv_width)), 4, (key_matrix, value_matrix))
+            cols = slice(d * kv_half, (d + 1) * kv_half)
+            for ref, at in ((wk_ref, 2 * d), (wv_ref, 2 * d + 1)):
+                pairs.append((ref.at[:, cols], weight.at[:, at * kv_half : (at + 1) * kv_half]))
+        return pairs + [(qg_ref, qg_out), (kg_ref, kg_out)]
+
+    return copy_call(
+        body,
+        [held((rows, 2 * q_half + 2 * kv_half)), held((key_matrix.shape[0], 4 * kv_half))]
+        + [held((1, HEAD_CHANNELS), f32)] * 2,
+        10,
+        (queries, out_grad, keys, values, key_matrix, value_matrix, query_gain[None], key_gain[None]),
+    )
 
 
 def turn_inputs(own, mate):
@@ -328,7 +349,7 @@
         out[:, :rows] = own_ref[...].T
         out[:, rows:] = mate_ref[...].T
 
-    return kernel_call(body, shape_of((width, 2 * rows)), [], (own, mate))
+    return kernel_call(body, [held((width, 2 * rows))], [], (own, mate))[0]
 
 
 def angle_tables(token_length):
@@ -345,10 +366,10 @@
     return tables
 
 
-def attention(queries, out_grad, keys, values, mate, far, far_mate, query_gain, key_gain):
-    rows = queries.shape[0]
-    q_width = queries.shape[1] // 2
-    k_width = keys.shape[1] // 2
+def attention(own, mate, far, far_mate, query_gain, key_gain):
+    rows, width = own.shape
+    k_width = far.shape[1] // 2
+    q_width = width // 2 - k_width
     pair = 2 * HEAD_CHANNELS
     heads = q_width // HEAD_CHANNELS
     groups = k_width // HEAD_CHANNELS
@@ -358,35 +379,22 @@
     tables = angle_tables(tokens)
 
     def body(*refs):
-        q_ref, g_ref, k_ref, v_ref, mate_ref, far_ref, far_mate_ref = refs[:7]
-        qg_ref, kg_ref, row_cos, row_sin, col_cos, col_sin = refs[7:13]
-        dq_own, dq_mate, p_own, p_far = refs[13:17]
-        q_tok, kv_tok, qh, gh, kr, vv, q_inv, k_inv, dq_sc, dk_sc, dq_out, p_sc, sems = refs[17:]
+        own_ref, mate_ref, far_ref, far_mate_ref = refs[:4]
+        qg_ref, kg_ref, row_cos, row_sin, col_cos, col_sin = refs[4:10]
+        dq_own, dq_mate, p_own, p_far = refs[10:14]
+        q_tok, kv_tok, qh, gh, kr, vv, q_inv, k_inv, dq_sc, dk_sc, dq_out, p_sc = refs[14:]
         me = lax.axis_index("sp")
         bit = me % 2
         upper = me // 2
         q_own = pl.multiple_of(bit * rows, rows)
         q_mate = pl.multiple_of((1 - bit) * rows, rows)
 
-        def kv_rows(k):
-            return pl.ds(pl.multiple_of((me ^ k) * rows, rows), rows)
-
-        pairs = [
-            (far_ref, kv_tok.at[kv_rows(2), :]),
-            (far_mate_ref, kv_tok.at[kv_rows(3), :]),
-            (mate_ref.at[:, 2 * q_width :], kv_tok.at[kv_rows(1), :]),
-            (k_ref.at[:, lanes_of(bit, k_width)], kv_tok.at[kv_rows(0), :k_width]),
-            (v_ref.at[:, lanes_of(bit, k_width)], kv_tok.at[kv_rows(0), k_width:]),
-            (q_ref.at[:, lanes_of(bit, q_width)], q_tok.at[pl.ds(q_own, rows), :q_width]),
-            (g_ref.at[:, lanes_of(bit, q_width)], q_tok.at[pl.ds(q_own, rows), q_width:]),
-            (mate_ref.at[:, : 2 * q_width], q_tok.at[pl.ds(q_mate, rows), :]),
-        ]
-        copies = [
-            pltpu.make_async_copy(source, target, sems.at[i])
-            for i, (source, target) in enumerate(pairs)
-        ]
-        for copy in copies:
-            copy.start()
+        q_tok[pl.ds(q_own, rows), :] = own_ref[:, : 2 * q_width]
+        q_tok[pl.ds(q_mate, rows), :] = mate_ref[:, : 2 * q_width]
+        for k, block in enumerate(
+            (own_ref[:, 2 * q_width :], mate_ref[:, 2 * q_width :], far_ref[...], far_mate_ref[...])
+        ):
+            kv_tok[pl.ds(pl.multiple_of((me ^ k) * rows, rows), rows), :] = block
         lane = lax.broadcasted_iota(jnp.int32, (GRID, pair), 1)
         even = lane % 2 == 0
         by_row = lane % HEAD_CHANNELS < HEAD_CHANNELS // 2
@@ -420,8 +428,6 @@
             return inv * (weighted - value * inv * inv * inner)
 
         q_rows = half // GRID
-        for copy in copies:
-            copy.wait()
         for r in range(tokens // GRID):
             at = slice(r * GRID, (r + 1) * GRID)
             cos, sin = angles_of(r)
@@ -491,16 +497,10 @@
         dq_own[...] = dq_out[pl.ds(q_own, rows), :]
         dq_mate[...] = dq_out[pl.ds(q_mate, rows), :]
 
-    vmem = pl.BlockSpec(memory_space=pltpu.VMEM)
-    args = (queries, out_grad, keys, values, mate, far, far_mate)
-    small = (query_gain[None], key_gain[None], *[jnp.asarray(t) for t in tables])
-    return pl.pallas_call(
+    return kernel_call(
         body,
-        out_shape=[shape_of((rows, q_width))] * 2
-        + [shape_of((half, 2 * k_width), f32), shape_of((half, 2 * k_width))],
-        in_specs=[pl.BlockSpec(memory_space=pl.ANY)] * len(args) + [vmem] * len(small),
-        out_specs=[vmem] * 4,
-        scratch_shapes=[
+        [held((rows, q_width))] * 2 + [held((half, 2 * k_width), f32), held((half, 2 * k_width))],
+        [
             pltpu.VMEM((half, 2 * q_width), bf16),
             pltpu.VMEM((tokens, 2 * k_width), bf16),
             pltpu.VMEM((heads, half, HEAD_CHANNELS), bf16),
@@ -513,14 +513,19 @@
             pltpu.VMEM((tokens, k_width), f32),
             pltpu.VMEM((half, q_width), bf16),
             pltpu.VMEM((tokens, 2 * k_width), f32),
-            pltpu.SemaphoreType.DMA((8,)),
         ],
-        cost_estimate=pl.CostEstimate(
-            flops=10 * heads * half * tokens * HEAD_CHANNELS, bytes_accessed=0, transcendentals=0
+        (
+            own,
+            mate,
+            far,
+            far_mate,
+            query_gain,
+            key_gain,
+            *[jnp.asarray(table) for table in tables],
         ),
-        compiler_params=pltpu.CompilerParams(vmem_limit_bytes=58 * 1024 * 1024),
-        name="attention",
-    )(*args, *small)
+        flops=10 * heads * half * tokens * HEAD_CHANNELS,
+        limit=32 * MIB,
+    )
 
 
 def weight_partials(turned, p_own, p_far, dp_count):
@@ -545,7 +550,7 @@
 
     return kernel_call(
         body,
-        [shape_of((rows, cols))] * 2 + [shape_of((chips, share, cols))] * 2,
+        [held((rows, cols))] * 2 + [held((chips, share, cols))] * 2,
         [pltpu.VMEM((half, cols), bf16)],
         (turned, p_own, p_far),
         flops=2 * feats * half * cols,
@@ -563,16 +568,34 @@
 
 
 def join_weight_grads(own, mate, far, far_mate):
-    half = own.shape[1] // 2
-    here = own.astype(f32) + far.astype(f32)
-    there = mate.astype(f32) + far_mate.astype(f32)
-    even = lax.axis_index("sp") % 2 == 0
-    first = jnp.where(even, here, there)
-    second = jnp.where(even, there, here)
-    return (
-        jnp.concatenate([first[:, :half], second[:, :half]], axis=1),
-        jnp.concatenate([first[:, half:], second[:, half:]], axis=1),
-    )
+    rows, cols = own.shape
+    half = cols // 2
+
+    def body(own_ref, mate_ref, far_ref, far_mate_ref, k_out, v_out, k_sc, v_sc, sems):
+        even = lax.axis_index("sp") % 2 == 0
+        here = own_ref[...].astype(f32) + far_ref[...].astype(f32)
+        there = mate_ref[...].astype(f32) + far_mate_ref[...].astype(f32)
+        copies = []
+        for i, (scratch, out, lanes) in enumerate(
+            ((k_sc, k_out, slice(0, half)), (v_sc, v_out, slice(half, cols)))
+        ):
+            scratch[:, :half] = jnp.where(even, here[:, lanes], there[:, lanes])
+            scratch[:, half:] = jnp.where(even, there[:, lanes], here[:, lanes])
+            copy = pltpu.make_async_copy(scratch, out, sems.at[i])
+            copy.start()
+            copies.append(copy)
+        for copy in copies:
+            copy.wait()
+
+    return pl.pallas_call(
+        body,
+        out_shape=[shape_of((rows, cols), f32)] * 2,
+        in_specs=[pl.BlockSpec(memory_space=pltpu.VMEM)] * 4,
+        out_specs=[pl.BlockSpec(memory_space=pltpu.HBM)] * 2,
+        scratch_shapes=[pltpu.VMEM((rows, cols), f32)] * 2 + [pltpu.SemaphoreType.DMA((2,))],
+        compiler_params=pltpu.CompilerParams(vmem_limit_bytes=4 * MIB),
+        name="join_weight_grads",
+    )(*[in_vmem(piece) for piece in (own, mate, far, far_mate)])
 
 
 def token_outputs(p_mine, p_from_mate, weight_pieces, dq_own, dq_from_mate):
@@ -635,14 +658,14 @@
     mate = swap_with(mate, "sp", 1)
     far = swap_with(far, "sp", 2)
     far_mate = swap_with(far_mate, "sp", 3)
-    joined_weight = join_weights(key_matrix, value_matrix)
+    own, joined_weight, query_gain, key_gain = pack_own(
+        queries, keys, values, out_grad, key_matrix, value_matrix, query_gain, key_gain
+    )
     weight_pieces = [joined_weight] + [
         swap_with(joined_weight, "dp", m) for m in range(1, dp_count)
     ]
     mate_inputs = swap_with(inputs, "sp", 1)
-    dq_own, dq_mate, p_own, p_far = attention(
-        queries, out_grad, keys, values, mate, far, far_mate, query_gain, key_gain
-    )
+    dq_own, dq_mate, p_own, p_far = attention(own, mate, far, far_mate, query_gain, key_gain)
     p_far = swap_with(p_far, "sp", 2)
     dq_mate = swap_with(dq_mate, "sp", 1)
     turned = turn_inputs(inputs, mate_inputs)

time: 103 us -> 91.3 us (0.89)
  Pallas kernels: 21.4 us -> 12.1 us
  local copies, waits for them, and re-layouts: 2.85 us -> 0.02 us
  waiting for transfers between devices: 50.6 us -> 52.4 us
  other arithmetic: 1.7 us -> 0.18 us
    pallas_call x3, Pallas kernels: 12.9 us -> 3.1 us  [the longest x2 2.24 us: copy_call(): pl.pallas_call(run, out_shape=out_shape, in_specs=[pl.BlockSpec(memory_sp...]
    unnamed x34 -> x10, local copies, waits for them, and re-layouts: 2.82 us -> 0.02 us
    ppermute x21, waiting for transfers between devices: 50.6 us -> 52.4 us  [swap_with(): return lax.ppermute(value, axis, [(i, i ^ k) for i in range(count)])]
    concatenate x2 -> x0, other arithmetic: 1.44 us -> none  [the longest x1 0.72 us: join_weight_grads(): jnp.concatenate([first[:, half:], second[:, half:]], axis=1)]
    pallas_call x3 -> x4, Pallas kernels: 8.47 us -> 9.03 us  [kernel_call(): pl.pallas_call(body, out_shape=out_shape, in_specs=[vmem] * len(args), ou...]
  transfers between devices with their start and end apart: 21 -> 21, of which waited for: 9 -> 9; matrix products, arithmetic and copies ran while one was open for 0% -> 0% of each run, Pallas kernels for 18% -> 12%
where the time goes in v3:
time: 91.3 us; the launch traced here: 91.1 us
  waiting for transfers between devices  52.4 us (57%)
  starting transfers between devices  25.6 us (28%)
  Pallas kernels  12.1 us (13%)
    ppermute x21, waiting for transfers between devices, swap_with(): return lax.ppermute(value, axis, [(i, i ^ k) for i in range(count)])  52.4 us
    ppermute x21, starting transfers between devices, swap_with(): return lax.ppermute(value, axis, [(i, i ^ k) for i in range(count)])  25.6 us
    pallas_call x4, Pallas kernels, kernel_call(): pl.pallas_call(body, out_shape=out_shape, in_specs=[vmem] * len(args), ou...  9.03 us
    pallas_call x2, Pallas kernels, copy_call(): pl.pallas_call(run, out_shape=out_shape, in_specs=[pl.BlockSpec(memory_sp...  2.24 us
  transfers between devices with their start and end apart: 21, of which 9 were waited for; matrix products, arithmetic and copies ran while one was open for 0% of the time, Pallas kernels for 12%

profile of v3, /device:TPU:0, one launch (start us, length us, event | category | flops | bytes accessed | tf_op | source)
XLA Modules:
  0.0 91.1 jit_solution(13317905180447095868)
XLA Ops:
  0.6 3.1 %collective-permute-start = (bf16[128,2048]{1,0:T(8,128)(2,1)}, bf16[128,2048]{1,0:T(8,128)(2,1)S(1)}, u32[]{:S(2)}, u32[]{:S(2)}) collective-permute-start(bf16[128,2048]{1,0:T(8,128)(2,1)} %bitcast.23), channel_id=1, source_target_pairs={{0,8},{8,0},{16,24},{24,16},{1,9},{9,1},{17,25},{25,17},{2,10},{10... | collective-permute-start | bytes 1572872 | tf_op jit(solution)/shard_map/ppermute | solution.py:264
  3.7 1.0 %shard_map.158 = (bf16[128,1280]{1,0:T(8,128)(2,1)S(1)}, bf16[128,256]{1,0:T(8,128)(2,1)S(1)}, bf16[128,256]{1,0:T(8,128)(2,1)S(1)}) custom-call(bf16[128,1024]{1,0:T(8,128)(2,1)} %bitcast.25, bf16[128,1024]{1,0:T(8,128)(2,1)} %bitcast.27, bf16[128,256]{1,0:T(8,128)(2,1)} %bitcast.29, bf16[128,256]{1,0:T(8,128)(2,1)} %bitcast.31), custom_call_target="tpu_custom_call" | custom-call | tf_op jit(solution)/shard_map/pallas_call | solution.py:279
  4.8 0.1 collective-permute-start.1
  4.9 3.0 %collective-permute-start.2 = (bf16[128,256]{1,0:T(8,128)(2,1)S(1)}, bf16[128,256]{1,0:T(8,128)(2,1)S(1)}, u32[]{:S(2)}, u32[]{:S(2)}) collective-permute-start(bf16[128,256]{1,0:T(8,128)(2,1)S(1)} %get-tuple-element.25), channel_id=1, source_target_pairs={{0,16},{8,24},{16,0},{24,8},{1,17},{9,25},{17,1},{25,9},{2,18},{10... | collective-permute-start | bytes 196616 | tf_op jit(solution)/shard_map/ppermute | solution.py:264
  7.9 1.3 %collective-permute-start.3 = (bf16[128,256]{1,0:T(8,128)(2,1)S(1)}, bf16[128,256]{1,0:T(8,128)(2,1)S(1)}, u32[]{:S(2)}, u32[]{:S(2)}) collective-permute-start(bf16[128,256]{1,0:T(8,128)(2,1)S(1)} %get-tuple-element.26), channel_id=1, source_target_pairs={{0,24},{8,16},{16,8},{24,0},{1,25},{9,17},{17,9},{25,1},{2,26},{10... | collective-permute-start | bytes 196616 | tf_op jit(solution)/shard_map/ppermute | solution.py:264
  9.3 0.0 copy-start.1
  9.3 0.0 copy-start.2
  9.3 0.0 copy-start.4
  9.3 1.2 %shard_map.157 = (bf16[128,1280]{1,0:T(8,128)(2,1)S(1)}, bf16[256,512]{1,0:T(8,128)(2,1)S(1)}, f32[1,64]{1,0:T(1,128)S(1)}, f32[1,64]{1,0:T(1,128)S(1)}) custom-call(bf16[128,1024]{1,0:T(8,128)(2,1)} %bitcast.26, bf16[128,1024]{1,0:T(8,128)(2,1)} %bitcast.28, bf16[128,256]{1,0:T(8,128)(2,1)} %bitcast.30, bf16[128,256]{1,0:T(8,128)(2,1)} %bitcast.32, ...), custom_call_target="tpu_custom_call" | custom-call | tf_op jit(solution)/shard_map/pallas_call | solution.py:279
  10.5 0.0 copy-start.3
  10.5 13.8 %collective-permute-done.2.refs_2_ = bf16[128,256]{1,0:T(8,128)(2,1)S(1)} collective-permute-done((bf16[128,256]{1,0:T(8,128)(2,1)S(1)}, bf16[128,256]{1,0:T(8,128)(2,1)S(1)}, u32[]{:S(2)}, u32[]{:S(2)}) %collective-permute-start.2) | collective-permute-done | bytes 65568 | tf_op jit(solution)/shard_map/ppermute | solution.py:264
  24.3 3.6 %collective-permute-done.3.refs_3_ = bf16[128,256]{1,0:T(8,128)(2,1)S(1)} collective-permute-done((bf16[128,256]{1,0:T(8,128)(2,1)S(1)}, bf16[128,256]{1,0:T(8,128)(2,1)S(1)}, u32[]{:S(2)}, u32[]{:S(2)}) %collective-permute-start.3) | collective-permute-done | bytes 65568 | tf_op jit(solution)/shard_map/ppermute | solution.py:264
  27.9 0.0 collective-permute-done.1.refs_1_
  27.9 0.0 copy-done.1
  27.9 0.0 copy-done.2
  27.9 0.0 copy-done.4
  27.9 0.0 copy-done.3
  27.9 0.0 copy-start
  27.9 6.6 %shard_map.159 = (bf16[128,512]{1,0:T(8,128)(2,1)S(1)}, bf16[128,512]{1,0:T(8,128)(2,1)S(1)}, f32[256,256]{1,0:T(8,128)S(1)}, bf16[256,256]{1,0:T(8,128)(2,1)S(1)}) custom-call(bf16[128,1280]{1,0:T(8,128)(2,1)S(1)} %get-tuple-element.23.refs_0_, bf16[128,1280]{1,0:T(8,128)(2,1)S(1)} %collective-permute-done.1.refs_1_, ...), custom_call_target="tpu_custom_call" | custom-call | flops 671088640 | tf_op jit(solution)/shard_map/pallas_call | solution.py:243
  34.5 0.1 collective-permute-start.4
  34.6 0.0 collective-permute-done.mate_ref
  34.6 0.0 copy-done
  34.6 0.3 shard_map.156.x_ref
  34.9 6.2 %collective-permute-done.4.pf_ref = bf16[256,256]{1,0:T(8,128)(2,1)S(1)} collective-permute-done((bf16[256,256]{1,0:T(8,128)(2,1)S(1)}, bf16[256,256]{1,0:T(8,128)(2,1)S(1)}, u32[]{:S(2)}, u32[]{:S(2)}) %collective-permute-start.4) | collective-permute-done | bytes 131104 | tf_op jit(solution)/shard_map/ppermute | solution.py:264
  41.1 0.5 shard_map.160
  41.6 0.1 collective-permute-start.14
  41.7 1.6 %collective-permute-start.10 = (bf16[256,512]{1,0:T(8,128)(2,1)S(1)}, bf16[256,512]{1,0:T(8,128)(2,1)S(1)}, u32[]{:S(2)}, u32[]{:S(2)}) collective-permute-start(bf16[256,512]{1,0:T(8,128)(2,1)S(1)} %get-tuple-element.35.rest_0_), channel_id=1, source_target_pairs={{0,4},{1,5},{2,6},{3,7},{4,0},{5,1},{6,2},{7,3},{8,12},{9,13},{10,... | collective-permute-start | bytes 786440 | tf_op jit(solution)/shard_map/ppermute | solution.py:264
  43.3 0.3 collective-permute-start.11
  43.6 2.5 %collective-permute-start.12 = (bf16[256,512]{1,0:T(8,128)(2,1)S(1)}, bf16[256,512]{1,0:T(8,128)(2,1)S(1)}, u32[]{:S(2)}, u32[]{:S(2)}) collective-permute-start(bf16[256,512]{1,0:T(8,128)(2,1)S(1)} %get-tuple-element.35.rest_0_), channel_id=1, source_target_pairs={{0,6},{1,7},{2,4},{3,5},{4,2},{5,3},{6,0},{7,1},{8,14},{9,15},{10,... | collective-permute-start | bytes 786440 | tf_op jit(solution)/shard_map/ppermute | solution.py:264
  46.0 0.0 collective-permute-done.14
  46.0 0.1 fusion.3
  46.1 0.6 collective-permute-start.15
  46.7 0.5 collective-permute-start.16
  47.2 9.4 %collective-permute-done.10.rest_4_ = bf16[256,512]{1,0:T(8,128)(2,1)S(1)} collective-permute-done((bf16[256,512]{1,0:T(8,128)(2,1)S(1)}, bf16[256,512]{1,0:T(8,128)(2,1)S(1)}, u32[]{:S(2)}, u32[]{:S(2)}) %collective-permute-start.10) | collective-permute-done | bytes 262176 | tf_op jit(solution)/shard_map/ppermute | solution.py:264
  56.6 2.5 %collective-permute-start.17 = (bf16[256,256]{1,0:T(8,128)(2,1)S(1)}, bf16[256,256]{1,0:T(8,128)(2,1)S(1)}, u32[]{:S(2)}, u32[]{:S(2)}) collective-permute-start(bf16[256,256]{1,0:T(8,128)(2,1)S(1)} %get-tuple-element.43), channel_id=1, source_target_pairs={{0,6},{1,7},{2,4},{3,5},{4,2},{5,3},{6,0},{7,1},{8,14},{9,15},{10,... | collective-permute-start | bytes 393224 | tf_op jit(solution)/shard_map/ppermute | solution.py:264
  59.0 5.0 %collective-permute-done.11.rest_5_ = bf16[256,512]{1,0:T(8,128)(2,1)S(1)} collective-permute-done((bf16[256,512]{1,0:T(8,128)(2,1)S(1)}, bf16[256,512]{1,0:T(8,128)(2,1)S(1)}, u32[]{:S(2)}, u32[]{:S(2)}) %collective-permute-start.11) | collective-permute-done | bytes 262176 | tf_op jit(solution)/shard_map/ppermute | solution.py:264
  64.0 2.8 %collective-permute-start.13 = (bf16[256,512]{1,0:T(8,128)(2,1)S(1)}, bf16[256,512]{1,0:T(8,128)(2,1)S(1)}, u32[]{:S(2)}, u32[]{:S(2)}) collective-permute-start(bf16[256,512]{1,0:T(8,128)(2,1)S(1)} %get-tuple-element.35.rest_0_), channel_id=1, source_target_pairs={{0,7},{1,6},{2,5},{3,4},{4,3},{5,2},{6,1},{7,0},{8,15},{9,14},{10,... | collective-permute-start | bytes 786440 | tf_op jit(solution)/shard_map/ppermute | solution.py:264
  66.9 0.0 collective-permute-done.12.rest_6_
  66.9 0.0 collective-permute-start.7
  66.9 0.0 collective-permute-done.15
  66.9 0.6 collective-permute-start.8
  67.5 0.0 collective-permute-done.16
  67.5 1.3 %collective-permute-start.9 = (bf16[256,512]{1,0:T(8,128)(2,1)S(1)}, bf16[256,512]{1,0:T(8,128)(2,1)S(1)}, u32[]{:S(2)}, u32[]{:S(2)}) collective-permute-start(bf16[256,512]{1,0:T(8,128)(2,1)S(1)} %get-tuple-element.35.rest_0_), channel_id=1, source_target_pairs={{0,3},{1,2},{2,1},{3,0},{4,7},{5,6},{6,5},{7,4},{8,11},{9,10},{10,... | collective-permute-start | bytes 786440 | tf_op jit(solution)/shard_map/ppermute | solution.py:264
  68.7 0.0 collective-permute-done.17
  68.7 0.0 collective-permute-start.6
  68.8 0.1 fusion.2.own_ref
  68.8 4.7 %collective-permute-done.13.rest_7_ = bf16[256,512]{1,0:T(8,128)(2,1)S(1)} collective-permute-done((bf16[256,512]{1,0:T(8,128)(2,1)S(1)}, bf16[256,512]{1,0:T(8,128)(2,1)S(1)}, u32[]{:S(2)}, u32[]{:S(2)}) %collective-permute-start.13) | collective-permute-done | bytes 262176 | tf_op jit(solution)/shard_map/ppermute | solution.py:264
  73.6 0.0 collective-permute-start.18
  73.6 0.0 collective-permute-done.7.rest_1_
  73.6 3.0 %collective-permute-start.19 = (bf16[256,256]{1,0:T(8,128)(2,1)S(1)}, bf16[256,256]{1,0:T(8,128)(2,1)S(1)}, u32[]{:S(2)}, u32[]{:S(2)}) collective-permute-start(bf16[256,256]{1,0:T(8,128)(2,1)S(1)} %fusion.2.own_ref), channel_id=1, source_target_pairs={{0,16},{8,24},{16,0},{24,8},{1,17},{9,25},{17,1},{25,9},{2,18},{10... | collective-permute-start | bytes 393224 | tf_op jit(solution)/shard_map/ppermute | solution.py:264
  76.5 3.6 %collective-permute-done.8.rest_2_ = bf16[256,512]{1,0:T(8,128)(2,1)S(1)} collective-permute-done((bf16[256,512]{1,0:T(8,128)(2,1)S(1)}, bf16[256,512]{1,0:T(8,128)(2,1)S(1)}, u32[]{:S(2)}, u32[]{:S(2)}) %collective-permute-start.8) | collective-permute-done | bytes 262176 | tf_op jit(solution)/shard_map/ppermute | solution.py:264
  80.2 2.4 %collective-permute-start.20 = (bf16[256,256]{1,0:T(8,128)(2,1)S(1)}, bf16[256,256]{1,0:T(8,128)(2,1)S(1)}, u32[]{:S(2)}, u32[]{:S(2)}) collective-permute-start(bf16[256,256]{1,0:T(8,128)(2,1)S(1)} %fusion.2.own_ref), channel_id=1, source_target_pairs={{0,24},{8,16},{16,8},{24,0},{1,25},{9,17},{17,9},{25,1},{2,26},{10... | collective-permute-start | bytes 393224 | tf_op jit(solution)/shard_map/ppermute | solution.py:264
  82.6 1.1 %collective-permute-done.9.rest_3_ = bf16[256,512]{1,0:T(8,128)(2,1)S(1)} collective-permute-done((bf16[256,512]{1,0:T(8,128)(2,1)S(1)}, bf16[256,512]{1,0:T(8,128)(2,1)S(1)}, u32[]{:S(2)}, u32[]{:S(2)}) %collective-permute-start.9) | collective-permute-done | bytes 262176 | tf_op jit(solution)/shard_map/ppermute | solution.py:264
  83.7 0.0 collective-permute-start.5
  83.7 0.0 collective-permute-done.6.dqm_ref
  83.7 4.8 %collective-permute-done.5.pm_ref = bf16[128,256]{1,0:T(8,128)(2,1)S(1)} collective-permute-done((bf16[128,256]{1,0:T(8,128)(2,1)S(1)}, bf16[128,256]{1,0:T(8,128)(2,1)S(1)}, u32[]{:S(2)}, u32[]{:S(2)}) %collective-permute-start.5) | collective-permute-done | bytes 65568 | tf_op jit(solution)/shard_map/ppermute | solution.py:264
  88.6 1.7 %shard_map.161 = (bf16[128,2048]{1,0:T(8,128)(2,1)}, bf16[128,1024]{1,0:T(8,128)(2,1)}) custom-call(bf16[128,256]{1,0:T(8,128)(2,1)S(1)} %get-tuple-element.31.p_ref, bf16[128,256]{1,0:T(8,128)(2,1)S(1)} %collective-permute-done.5.pm_ref, bf16[128,512]{1,0:T(8,128)(2,1)S(1)} %get-tuple-element.33.dq_ref, ...), custom_call_target="tpu_custom_call" | custom-call | flops 268435456 | tf_op jit(solution)/shard_map/pallas_call | solution.py:243
  90.2 0.0 collective-permute-done.18.mate_ref
  90.2 0.0 collective-permute-done.19.far_ref
  90.2 0.0 collective-permute-done.20.far_mate_ref
  90.2 0.9 join_weight_grads.1
Async XLA Ops:
  0.6 34.0 %collective-permute-start = (bf16[128,2048]{1,0:T(8,128)(2,1)}, bf16[128,2048]{1,0:T(8,128)(2,1)S(1)}, u32[]{:S(2)}, u32[]{:S(2)}) collective-permute-start(bf16[128,2048]{1,0:T(8,128)(2,1)} %bitcast.23), channel_id=1, source_target_pairs={{0,8},{8,0},{16,24},{24,16},{1,9},{9,1},{17,25},{25,17},{2,10},{10... | collective-permute-start | bytes 1572872 | tf_op jit(solution)/shard_map/ppermute | solution.py:264
  4.8 23.1 %collective-permute-start.1 = (bf16[128,1280]{1,0:T(8,128)(2,1)S(1)}, bf16[128,1280]{1,0:T(8,128)(2,1)S(1)}, u32[]{:S(2)}, u32[]{:S(2)}) collective-permute-start(bf16[128,1280]{1,0:T(8,128)(2,1)S(1)} %get-tuple-element.24), channel_id=1, source_target_pairs={{0,8},{8,0},{16,24},{24,16},{1,9},{9,1},{17,25},{25,17},{2,10},{10... | collective-permute-start | bytes 983048 | tf_op jit(solution)/shard_map/ppermute | solution.py:264
  4.9 19.4 %collective-permute-start.2 = (bf16[128,256]{1,0:T(8,128)(2,1)S(1)}, bf16[128,256]{1,0:T(8,128)(2,1)S(1)}, u32[]{:S(2)}, u32[]{:S(2)}) collective-permute-start(bf16[128,256]{1,0:T(8,128)(2,1)S(1)} %get-tuple-element.25), channel_id=1, source_target_pairs={{0,16},{8,24},{16,0},{24,8},{1,17},{9,25},{17,1},{25,9},{2,18},{10... | collective-permute-start | bytes 196616 | tf_op jit(solution)/shard_map/ppermute | solution.py:264
  7.9 20.0 %collective-permute-start.3 = (bf16[128,256]{1,0:T(8,128)(2,1)S(1)}, bf16[128,256]{1,0:T(8,128)(2,1)S(1)}, u32[]{:S(2)}, u32[]{:S(2)}) collective-permute-start(bf16[128,256]{1,0:T(8,128)(2,1)S(1)} %get-tuple-element.26), channel_id=1, source_target_pairs={{0,24},{8,16},{16,8},{24,0},{1,25},{9,17},{17,9},{25,1},{2,26},{10... | collective-permute-start | bytes 196616 | tf_op jit(solution)/shard_map/ppermute | solution.py:264
  9.3 18.7 %copy-start.1 = (f32[64,128]{1,0:T(8,128)S(1)}, f32[64,128]{1,0:T(8,128)}, u32[]{:S(2)}) copy-start(f32[64,128]{1,0:T(8,128)} %constant.10.clone.refs_8_) | copy-start | bytes 98308
  9.3 18.7 %copy-start.2 = (f32[64,128]{1,0:T(8,128)S(1)}, f32[64,128]{1,0:T(8,128)}, u32[]{:S(2)}) copy-start(f32[64,128]{1,0:T(8,128)} %constant.11.clone.refs_9_) | copy-start | bytes 98308
  9.3 18.7 %copy-start.4 = (f32[8,128]{1,0:T(8,128)S(1)}, f32[8,128]{1,0:T(8,128)}, u32[]{:S(2)}) copy-start(f32[8,128]{1,0:T(8,128)} %constant.9.clone.refs_7_) | copy-start | bytes 12292
  10.5 17.5 %copy-start.3 = (f32[8,128]{1,0:T(8,128)S(1)}, f32[8,128]{1,0:T(8,128)}, u32[]{:S(2)}) copy-start(f32[8,128]{1,0:T(8,128)} %constant.8.clone.refs_6_) | copy-start | bytes 12292
  27.9 6.7 %copy-start = (bf16[1,128,2048]{2,1,0:T(8,128)(2,1)S(1)}, bf16[1,128,2048]{2,1,0:T(8,128)(2,1)}, u32[]{:S(2)}) copy-start(bf16[1,128,2048]{2,1,0:T(8,128)(2,1)} %param.13) | copy-start | bytes 1572868
  34.5 6.6 %collective-permute-start.4 = (bf16[256,256]{1,0:T(8,128)(2,1)S(1)}, bf16[256,256]{1,0:T(8,128)(2,1)S(1)}, u32[]{:S(2)}, u32[]{:S(2)}) collective-permute-start(bf16[256,256]{1,0:T(8,128)(2,1)S(1)} %get-tuple-element.30), channel_id=1, source_target_pairs={{0,16},{8,24},{16,0},{24,8},{1,17},{9,25},{17,1},{25,9},{2,18},{10... | collective-permute-start | bytes 393224 | tf_op jit(solution)/shard_map/ppermute | solution.py:264
  41.6 4.4 %collective-permute-start.14 = (bf16[4,256,256]{2,1,0:T(8,128)(2,1)S(1)}, bf16[4,256,256]{2,1,0:T(8,128)(2,1)S(1)}, u32[]{:S(2)}, u32[]{:S(2)}) collective-permute-start(bf16[4,256,256]{2,1,0:T(8,128)(2,1)S(1)} %get-tuple-element.39), channel_id=1, source_target_pairs={{0,1},{1,0},{2,3},{3,2},{4,5},{5,4},{6,7},{7,6},{8,9},{9,8},{10,11... | collective-permute-start | bytes 1572872 | tf_op jit(solution)/shard_map/ppermute | solution.py:264
  41.7 14.9 %collective-permute-start.10 = (bf16[256,512]{1,0:T(8,128)(2,1)S(1)}, bf16[256,512]{1,0:T(8,128)(2,1)S(1)}, u32[]{:S(2)}, u32[]{:S(2)}) collective-permute-start(bf16[256,512]{1,0:T(8,128)(2,1)S(1)} %get-tuple-element.35.rest_0_), channel_id=1, source_target_pairs={{0,4},{1,5},{2,6},{3,7},{4,0},{5,1},{6,2},{7,3},{8,12},{9,13},{10,... | collective-permute-start | bytes 786440 | tf_op jit(solution)/shard_map/ppermute | solution.py:264
  43.3 20.7 %collective-permute-start.11 = (bf16[256,512]{1,0:T(8,128)(2,1)S(1)}, bf16[256,512]{1,0:T(8,128)(2,1)S(1)}, u32[]{:S(2)}, u32[]{:S(2)}) collective-permute-start(bf16[256,512]{1,0:T(8,128)(2,1)S(1)} %get-tuple-element.35.rest_0_), channel_id=1, source_target_pairs={{0,5},{1,4},{2,7},{3,6},{4,1},{5,0},{6,3},{7,2},{8,13},{9,12},{10,... | collective-permute-start | bytes 786440 | tf_op jit(solution)/shard_map/ppermute | solution.py:264
  43.6 23.3 %collective-permute-start.12 = (bf16[256,512]{1,0:T(8,128)(2,1)S(1)}, bf16[256,512]{1,0:T(8,128)(2,1)S(1)}, u32[]{:S(2)}, u32[]{:S(2)}) collective-permute-start(bf16[256,512]{1,0:T(8,128)(2,1)S(1)} %get-tuple-element.35.rest_0_), channel_id=1, source_target_pairs={{0,6},{1,7},{2,4},{3,5},{4,2},{5,3},{6,0},{7,1},{8,14},{9,15},{10,... | collective-permute-start | bytes 786440 | tf_op jit(solution)/shard_map/ppermute | solution.py:264
  46.1 20.8 %collective-permute-start.15 = (bf16[256,256]{1,0:T(8,128)(2,1)S(1)}, bf16[256,256]{1,0:T(8,128)(2,1)S(1)}, u32[]{:S(2)}, u32[]{:S(2)}) collective-permute-start(bf16[256,256]{1,0:T(8,128)(2,1)S(1)} %get-tuple-element.42), channel_id=1, source_target_pairs={{0,2},{1,3},{2,0},{3,1},{4,6},{5,7},{6,4},{7,5},{8,10},{9,11},{10,... | collective-permute-start | bytes 393224 | tf_op jit(solution)/shard_map/ppermute | solution.py:264
  46.7 20.8 %collective-permute-start.16 = (bf16[256,256]{1,0:T(8,128)(2,1)S(1)}, bf16[256,256]{1,0:T(8,128)(2,1)S(1)}, u32[]{:S(2)}, u32[]{:S(2)}) collective-permute-start(bf16[256,256]{1,0:T(8,128)(2,1)S(1)} %get-tuple-element.44), channel_id=1, source_target_pairs={{0,4},{1,5},{2,6},{3,7},{4,0},{5,1},{6,2},{7,3},{8,12},{9,13},{10,... | collective-permute-start | bytes 393224 | tf_op jit(solution)/shard_map/ppermute | solution.py:264
  56.6 12.2 %collective-permute-start.17 = (bf16[256,256]{1,0:T(8,128)(2,1)S(1)}, bf16[256,256]{1,0:T(8,128)(2,1)S(1)}, u32[]{:S(2)}, u32[]{:S(2)}) collective-permute-start(bf16[256,256]{1,0:T(8,128)(2,1)S(1)} %get-tuple-element.43), channel_id=1, source_target_pairs={{0,6},{1,7},{2,4},{3,5},{4,2},{5,3},{6,0},{7,1},{8,14},{9,15},{10,... | collective-permute-start | bytes 393224 | tf_op jit(solution)/shard_map/ppermute | solution.py:264
  64.0 9.5 %collective-permute-start.13 = (bf16[256,512]{1,0:T(8,128)(2,1)S(1)}, bf16[256,512]{1,0:T(8,128)(2,1)S(1)}, u32[]{:S(2)}, u32[]{:S(2)}) collective-permute-start(bf16[256,512]{1,0:T(8,128)(2,1)S(1)} %get-tuple-element.35.rest_0_), channel_id=1, source_target_pairs={{0,7},{1,6},{2,5},{3,4},{4,3},{5,2},{6,1},{7,0},{8,15},{9,14},{10,... | collective-permute-start | bytes 786440 | tf_op jit(solution)/shard_map/ppermute | solution.py:264
  66.9 6.7 %collective-permute-start.7 = (bf16[256,512]{1,0:T(8,128)(2,1)S(1)}, bf16[256,512]{1,0:T(8,128)(2,1)S(1)}, u32[]{:S(2)}, u32[]{:S(2)}) collective-permute-start(bf16[256,512]{1,0:T(8,128)(2,1)S(1)} %get-tuple-element.35.rest_0_), channel_id=1, source_target_pairs={{0,1},{1,0},{2,3},{3,2},{4,5},{5,4},{6,7},{7,6},{8,9},{9,8},{10,11... | collective-permute-start | bytes 786440 | tf_op jit(solution)/shard_map/ppermute | solution.py:264
  66.9 13.3 %collective-permute-start.8 = (bf16[256,512]{1,0:T(8,128)(2,1)S(1)}, bf16[256,512]{1,0:T(8,128)(2,1)S(1)}, u32[]{:S(2)}, u32[]{:S(2)}) collective-permute-start(bf16[256,512]{1,0:T(8,128)(2,1)S(1)} %get-tuple-element.35.rest_0_), channel_id=1, source_target_pairs={{0,2},{1,3},{2,0},{3,1},{4,6},{5,7},{6,4},{7,5},{8,10},{9,11},{10,... | collective-permute-start | bytes 786440 | tf_op jit(solution)/shard_map/ppermute | solution.py:264
  67.5 16.2 %collective-permute-start.9 = (bf16[256,512]{1,0:T(8,128)(2,1)S(1)}, bf16[256,512]{1,0:T(8,128)(2,1)S(1)}, u32[]{:S(2)}, u32[]{:S(2)}) collective-permute-start(bf16[256,512]{1,0:T(8,128)(2,1)S(1)} %get-tuple-element.35.rest_0_), channel_id=1, source_target_pairs={{0,3},{1,2},{2,1},{3,0},{4,7},{5,6},{6,5},{7,4},{8,11},{9,10},{10,... | collective-permute-start | bytes 786440 | tf_op jit(solution)/shard_map/ppermute | solution.py:264
  68.7 15.0 %collective-permute-start.6 = (bf16[128,512]{1,0:T(8,128)(2,1)S(1)}, bf16[128,512]{1,0:T(8,128)(2,1)S(1)}, u32[]{:S(2)}, u32[]{:S(2)}) collective-permute-start(bf16[128,512]{1,0:T(8,128)(2,1)S(1)} %get-tuple-element.34), channel_id=1, source_target_pairs={{0,8},{8,0},{16,24},{24,16},{1,9},{9,1},{17,25},{25,17},{2,10},{10... | collective-permute-start | bytes 393224 | tf_op jit(solution)/shard_map/ppermute | solution.py:264
  73.6 16.7 %collective-permute-start.18 = (bf16[256,256]{1,0:T(8,128)(2,1)S(1)}, bf16[256,256]{1,0:T(8,128)(2,1)S(1)}, u32[]{:S(2)}, u32[]{:S(2)}) collective-permute-start(bf16[256,256]{1,0:T(8,128)(2,1)S(1)} %fusion.2.own_ref), channel_id=1, source_target_pairs={{0,8},{8,0},{16,24},{24,16},{1,9},{9,1},{17,25},{25,17},{2,10},{10... | collective-permute-start | bytes 393224 | tf_op jit(solution)/shard_map/ppermute | solution.py:264
  73.6 16.7 %collective-permute-start.19 = (bf16[256,256]{1,0:T(8,128)(2,1)S(1)}, bf16[256,256]{1,0:T(8,128)(2,1)S(1)}, u32[]{:S(2)}, u32[]{:S(2)}) collective-permute-start(bf16[256,256]{1,0:T(8,128)(2,1)S(1)} %fusion.2.own_ref), channel_id=1, source_target_pairs={{0,16},{8,24},{16,0},{24,8},{1,17},{9,25},{17,1},{25,9},{2,18},{10... | collective-permute-start | bytes 393224 | tf_op jit(solution)/shard_map/ppermute | solution.py:264
  80.2 10.1 %collective-permute-start.20 = (bf16[256,256]{1,0:T(8,128)(2,1)S(1)}, bf16[256,256]{1,0:T(8,128)(2,1)S(1)}, u32[]{:S(2)}, u32[]{:S(2)}) collective-permute-start(bf16[256,256]{1,0:T(8,128)(2,1)S(1)} %fusion.2.own_ref), channel_id=1, source_target_pairs={{0,24},{8,16},{16,8},{24,0},{1,25},{9,17},{17,9},{25,1},{2,26},{10... | collective-permute-start | bytes 393224 | tf_op jit(solution)/shard_map/ppermute | solution.py:264
  83.7 4.8 %collective-permute-start.5 = (bf16[128,256]{1,0:T(8,128)(2,1)S(1)}, bf16[128,256]{1,0:T(8,128)(2,1)S(1)}, u32[]{:S(2)}, u32[]{:S(2)}) collective-permute-start(bf16[128,256]{1,0:T(8,128)(2,1)S(1)} %get-tuple-element.32), channel_id=1, source_target_pairs={{0,8},{8,0},{16,24},{24,16},{1,9},{9,1},{17,25},{25,17},{2,10},{10... | collective-permute-start | bytes 196616 | tf_op jit(solution)/shard_map/ppermute | solution.py:264

commit v4 on v3

--- a/solution.py
+++ b/solution.py
@@ -320,25 +320,26 @@
     )
 
 
-def pack_own(queries, keys, values, out_grad, key_matrix, value_matrix, query_gain, key_gain):
+def pack_own(queries, keys, values, out_grad, key_matrix, value_matrix, small):
     rows, q_all = queries.shape
     q_half, kv_half = q_all // 2, keys.shape[1] // 2
 
-    def body(q_ref, g_ref, k_ref, v_ref, wk_ref, wv_ref, qg_ref, kg_ref, own, weight, qg_out, kg_out):
+    def body(q_ref, g_ref, k_ref, v_ref, wk_ref, wv_ref, *rest):
+        own, weight = rest[len(small) : len(small) + 2]
         bit = lax.axis_index("sp") % 2
         pairs = head_copies((q_ref, g_ref, k_ref, v_ref), own, bit, q_half, kv_half)
         for d in range(2):
             cols = slice(d * kv_half, (d + 1) * kv_half)
             for ref, at in ((wk_ref, 2 * d), (wv_ref, 2 * d + 1)):
                 pairs.append((ref.at[:, cols], weight.at[:, at * kv_half : (at + 1) * kv_half]))
-        return pairs + [(qg_ref, qg_out), (kg_ref, kg_out)]
+        return pairs + list(zip(rest[: len(small)], rest[len(small) + 2 :]))
 
     return copy_call(
         body,
         [held((rows, 2 * q_half + 2 * kv_half)), held((key_matrix.shape[0], 4 * kv_half))]
-        + [held((1, HEAD_CHANNELS), f32)] * 2,
-        10,
-        (queries, out_grad, keys, values, key_matrix, value_matrix, query_gain[None], key_gain[None]),
+        + [held(value.shape, value.dtype) for value in small],
+        8 + len(small),
+        (queries, out_grad, keys, values, key_matrix, value_matrix, *small),
     )
 
 
@@ -366,7 +367,50 @@
     return tables
 
 
-def attention(own, mate, far, far_mate, query_gain, key_gain):
+class Rotation:
+    def __init__(self, row_cos, row_sin, col_cos, col_sin):
+        self.tables = (row_cos, row_sin, col_cos, col_sin)
+        self.pair = 2 * HEAD_CHANNELS
+        lane = lax.broadcasted_iota(jnp.int32, (GRID, self.pair), 1)
+        self.even = lane % 2 == 0
+        self.by_row = lane % HEAD_CHANNELS < HEAD_CHANNELS // 2
+        seg_r = lax.broadcasted_iota(jnp.int32, (2 * self.pair, self.pair), 0)
+        seg_c = lax.broadcasted_iota(jnp.int32, (2 * self.pair, self.pair), 1)
+        same = seg_r // HEAD_CHANNELS % 2 == seg_c // HEAD_CHANNELS
+        self.seg = jnp.where(same, 1.0 / HEAD_CHANNELS, 0.0).astype(bf16)
+
+    def head_mean(self, product_f):
+        high = product_f.astype(bf16)
+        low = (product_f - high.astype(f32)).astype(bf16)
+        return dot(jnp.concatenate([high, low], axis=1), self.seg, 1, 0)
+
+    def swap(self, value):
+        left, right = pltpu.roll(value, self.pair - 1, 1), pltpu.roll(value, 1, 1)
+        return jnp.where(self.even, left, right)
+
+    def angles_of(self, r):
+        row_cos, row_sin, col_cos, col_sin = self.tables
+        cos = jnp.where(self.by_row, row_cos[pl.ds(r, 1), :], col_cos[...])
+        sin = jnp.where(self.by_row, row_sin[pl.ds(r, 1), :], col_sin[...])
+        return cos, sin
+
+    def forward(self, value, gain, cos, sin):
+        inv = lax.rsqrt(self.head_mean(value * value) + norm_eps)
+        normed = value * inv * gain
+        return inv, (normed * cos + self.swap(normed) * sin).astype(bf16)
+
+    def backward(self, value, inv, grad, gain, cos, sin):
+        weighted = (grad * cos - self.swap(grad) * sin) * gain
+        inner = self.head_mean(weighted * value)
+        return inv * (weighted - value * inv * inv * inner)
+
+
+def split_halves(value, upper, half, own_out, far_out):
+    own_out[...] = value[pl.ds(pl.multiple_of(upper * half, half), half), :]
+    far_out[...] = value[pl.ds(pl.multiple_of((1 - upper) * half, half), half), :].astype(bf16)
+
+
+def attention_values(own, mate, far, far_mate, gains, tables):
     rows, width = own.shape
     k_width = far.shape[1] // 2
     q_width = width // 2 - k_width
@@ -376,64 +420,29 @@
     per_group = heads // groups
     half = 2 * rows
     tokens = 4 * rows
-    tables = angle_tables(tokens)
 
     def body(*refs):
-        own_ref, mate_ref, far_ref, far_mate_ref = refs[:4]
-        qg_ref, kg_ref, row_cos, row_sin, col_cos, col_sin = refs[4:10]
-        dq_own, dq_mate, p_own, p_far = refs[10:14]
-        q_tok, kv_tok, qh, gh, kr, vv, q_inv, k_inv, dq_sc, dk_sc, dq_out, p_sc = refs[14:]
+        own_ref, mate_ref, far_ref, far_mate_ref, qg_ref, kg_ref = refs[:6]
+        pv_own, pv_far, probs, qh, gh, kr, vv, q_inv, k_inv, q_tok, kv_tok, dv_sc = refs[10:]
         me = lax.axis_index("sp")
         bit = me % 2
         upper = me // 2
-        q_own = pl.multiple_of(bit * rows, rows)
-        q_mate = pl.multiple_of((1 - bit) * rows, rows)
-
-        q_tok[pl.ds(q_own, rows), :] = own_ref[:, : 2 * q_width]
-        q_tok[pl.ds(q_mate, rows), :] = mate_ref[:, : 2 * q_width]
+        q_tok[pl.ds(pl.multiple_of(bit * rows, rows), rows), :] = own_ref[:, : 2 * q_width]
+        q_tok[pl.ds(pl.multiple_of((1 - bit) * rows, rows), rows), :] = mate_ref[:, : 2 * q_width]
         for k, block in enumerate(
             (own_ref[:, 2 * q_width :], mate_ref[:, 2 * q_width :], far_ref[...], far_mate_ref[...])
         ):
             kv_tok[pl.ds(pl.multiple_of((me ^ k) * rows, rows), rows), :] = block
-        lane = lax.broadcasted_iota(jnp.int32, (GRID, pair), 1)
-        even = lane % 2 == 0
-        by_row = lane % HEAD_CHANNELS < HEAD_CHANNELS // 2
-        seg_r = lax.broadcasted_iota(jnp.int32, (2 * pair, pair), 0) // HEAD_CHANNELS % 2
-        seg_c = lax.broadcasted_iota(jnp.int32, (2 * pair, pair), 1) // HEAD_CHANNELS
-        seg = jnp.where(seg_r == seg_c, 1.0 / HEAD_CHANNELS, 0.0).astype(bf16)
+        turn = Rotation(*refs[6:10])
         q_gain = jnp.concatenate([qg_ref[...], qg_ref[...]], axis=1)
         k_gain = jnp.concatenate([kg_ref[...], kg_ref[...]], axis=1)
-
-        def head_mean(product_f):
-            high = product_f.astype(bf16)
-            low = (product_f - high.astype(f32)).astype(bf16)
-            return dot(jnp.concatenate([high, low], axis=1), seg, 1, 0)
-
-        def swap(value):
-            return jnp.where(even, pltpu.roll(value, pair - 1, 1), pltpu.roll(value, 1, 1))
-
-        def angles_of(r):
-            cos = jnp.where(by_row, row_cos[pl.ds(r, 1), :], col_cos[...])
-            sin = jnp.where(by_row, row_sin[pl.ds(r, 1), :], col_sin[...])
-            return cos, sin
-
-        def forward(value, gain, cos, sin):
-            inv = lax.rsqrt(head_mean(value * value) + norm_eps)
-            normed = value * inv * gain
-            return inv, (normed * cos + swap(normed) * sin).astype(bf16)
-
-        def backward(value, inv, grad, gain, cos, sin):
-            weighted = (grad * cos - swap(grad) * sin) * gain
-            inner = head_mean(weighted * value)
-            return inv * (weighted - value * inv * inv * inner)
-
         q_rows = half // GRID
         for r in range(tokens // GRID):
             at = slice(r * GRID, (r + 1) * GRID)
-            cos, sin = angles_of(r)
+            cos, sin = turn.angles_of(r)
             for lo in range(0, k_width, pair):
                 part = slice(lo, lo + pair)
-                inv, turned = forward(kv_tok[at, part].astype(f32), k_gain, cos, sin)
+                inv, turned = turn.forward(kv_tok[at, part].astype(f32), k_gain, cos, sin)
                 k_inv[at, part] = inv
                 for u in range(2):
                     g = lo // HEAD_CHANNELS + u
@@ -442,106 +451,139 @@
                     vv[g, at, :] = kv_tok[at, begin : begin + HEAD_CHANNELS]
         for r in range(q_rows):
             at = slice(r * GRID, (r + 1) * GRID)
-            cos, sin = angles_of(upper * q_rows + r)
+            cos, sin = turn.angles_of(upper * q_rows + r)
             for lo in range(0, q_width, pair):
                 part = slice(lo, lo + pair)
-                inv, turned = forward(q_tok[at, part].astype(f32), q_gain, cos, sin)
+                inv, turned = turn.forward(q_tok[at, part].astype(f32), q_gain, cos, sin)
                 q_inv[at, part] = inv
                 grad = q_tok[at, q_width + lo : q_width + lo + pair]
                 for u in range(2):
                     lanes = slice(u * HEAD_CHANNELS, (u + 1) * HEAD_CHANNELS)
                     qh[lo // HEAD_CHANNELS + u, at, :] = turned[:, lanes]
                     gh[lo // HEAD_CHANNELS + u, at, :] = grad[:, lanes]
-
+        for g in range(groups):
+            key_rot = kr[g]
+            for h in range(g * per_group, (g + 1) * per_group):
+                scores = dot(key_rot, qh[h], 1, 1)
+                top = jnp.max(scores, axis=0, keepdims=True)
+                expo = jnp.exp((scores - top) * score_scale)
+                prob = expo * (1.0 / jnp.sum(expo, axis=0, keepdims=True))
+                probs[h] = prob
+                dv = dot(prob.astype(bf16), gh[h], 1, 0)
+                value_acc = dv if h == g * per_group else value_acc + dv
+            dv_sc[:, g * HEAD_CHANNELS : (g + 1) * HEAD_CHANNELS] = value_acc
+        split_halves(dv_sc, upper, half, pv_own, pv_far)
+
+    outs = kernel_call(
+        body,
+        [
+            held((half, k_width), f32),
+            held((half, k_width)),
+            held((heads, tokens, half), f32),
+            held((heads, half, HEAD_CHANNELS)),
+            held((heads, half, HEAD_CHANNELS)),
+            held((groups, tokens, HEAD_CHANNELS)),
+            held((groups, tokens, HEAD_CHANNELS)),
+            held((half, q_width), f32),
+            held((tokens, k_width), f32),
+            held((half, 2 * q_width)),
+            held((tokens, 2 * k_width)),
+        ],
+        [pltpu.VMEM((tokens, k_width), f32)],
+        (own, mate, far, far_mate, *gains, *tables),
+        flops=4 * heads * half * tokens * HEAD_CHANNELS,
+        limit=20 * MIB,
+    )
+    return outs[0], outs[1], outs[2:]
+
+
+def attention_keys(state, gains, tables):
+    probs, _, _, kr, _, q_inv, k_inv, _, _ = state
+    heads, tokens, half = probs.shape
+    rows = half // 2
+    groups = kr.shape[0]
+    per_group = heads // groups
+    q_width, k_width = q_inv.shape[1], k_inv.shape[1]
+    pair = 2 * HEAD_CHANNELS
+
+    def body(*refs):
+        probs, qh, gh, kr, vv, q_inv, k_inv, q_tok, kv_tok, qg_ref, kg_ref = refs[:11]
+        dq_own, dq_mate, pk_own, pk_far, dq_sc, dk_sc, dq_out, p_sc = refs[15:]
+        me = lax.axis_index("sp")
+        bit = me % 2
+        upper = me // 2
+        turn = Rotation(*refs[11:15])
+        q_gain = jnp.concatenate([qg_ref[...], qg_ref[...]], axis=1)
+        k_gain = jnp.concatenate([kg_ref[...], kg_ref[...]], axis=1)
+        q_rows = half // GRID
         for g in range(groups):
             key_rot = kr[g]
             value_in = vv[g]
             for h in range(g * per_group, (g + 1) * per_group):
-                query = qh[h]
-                grad = gh[h]
-                scores = dot(key_rot, query, 1, 1)
-                top = jnp.max(scores, axis=0, keepdims=True)
-                expo = jnp.exp((scores - top) * score_scale)
-                prob = expo * (1.0 / jnp.sum(expo, axis=0, keepdims=True))
-                prob_grad = dot(value_in, grad, 1, 1)
+                prob = probs[h]
+                prob_grad = dot(value_in, gh[h], 1, 1)
                 row_dot = jnp.sum(prob * prob_grad, axis=0, keepdims=True)
                 score_grad = (prob * (prob_grad - row_dot)).astype(bf16)
-                dv = dot(prob.astype(bf16), grad, 1, 0)
-                dk = dot(score_grad, query, 1, 0)
+                dk = dot(score_grad, qh[h], 1, 0)
                 dq_t = dot(key_rot, score_grad, 0, 0)
                 dq_sc[:, h * HEAD_CHANNELS : (h + 1) * HEAD_CHANNELS] = dq_t.T * score_scale
-                first = h == g * per_group
-                key_acc = dk if first else key_acc + dk
-                value_acc = dv if first else value_acc + dv
-            lo = g * HEAD_CHANNELS
-            dk_sc[:, lo : lo + HEAD_CHANNELS] = key_acc * score_scale
-            p_sc[:, k_width + lo : k_width + lo + HEAD_CHANNELS] = value_acc
-
+                key_acc = dk if h == g * per_group else key_acc + dk
+            dk_sc[:, g * HEAD_CHANNELS : (g + 1) * HEAD_CHANNELS] = key_acc * score_scale
         for r in range(tokens // GRID):
             at = slice(r * GRID, (r + 1) * GRID)
-            cos, sin = angles_of(r)
+            cos, sin = turn.angles_of(r)
             for lo in range(0, k_width, pair):
                 part = slice(lo, lo + pair)
                 value = kv_tok[at, part].astype(f32)
-                p_sc[at, part] = backward(value, k_inv[at, part], dk_sc[at, part], k_gain, cos, sin)
-        p_own[...] = p_sc[pl.ds(pl.multiple_of(upper * half, half), half), :]
-        p_far[...] = p_sc[pl.ds(pl.multiple_of((1 - upper) * half, half), half), :].astype(bf16)
+                p_sc[at, part] = turn.backward(
+                    value, k_inv[at, part], dk_sc[at, part], k_gain, cos, sin
+                )
+        split_halves(p_sc, upper, half, pk_own, pk_far)
         for r in range(q_rows):
             at = slice(r * GRID, (r + 1) * GRID)
-            cos, sin = angles_of(upper * q_rows + r)
+            cos, sin = turn.angles_of(upper * q_rows + r)
             for lo in range(0, q_width, pair):
                 part = slice(lo, lo + pair)
                 value = q_tok[at, part].astype(f32)
-                result = backward(value, q_inv[at, part], dq_sc[at, part], q_gain, cos, sin)
+                result = turn.backward(value, q_inv[at, part], dq_sc[at, part], q_gain, cos, sin)
                 dq_out[at, part] = result.astype(bf16)
-        dq_own[...] = dq_out[pl.ds(q_own, rows), :]
-        dq_mate[...] = dq_out[pl.ds(q_mate, rows), :]
+        dq_own[...] = dq_out[pl.ds(pl.multiple_of(bit * rows, rows), rows), :]
+        dq_mate[...] = dq_out[pl.ds(pl.multiple_of((1 - bit) * rows, rows), rows), :]
 
     return kernel_call(
         body,
-        [held((rows, q_width))] * 2 + [held((half, 2 * k_width), f32), held((half, 2 * k_width))],
+        [held((rows, q_width))] * 2 + [held((half, k_width), f32), held((half, k_width))],
         [
-            pltpu.VMEM((half, 2 * q_width), bf16),
-            pltpu.VMEM((tokens, 2 * k_width), bf16),
-            pltpu.VMEM((heads, half, HEAD_CHANNELS), bf16),
-            pltpu.VMEM((heads, half, HEAD_CHANNELS), bf16),
-            pltpu.VMEM((groups, tokens, HEAD_CHANNELS), bf16),
-            pltpu.VMEM((groups, tokens, HEAD_CHANNELS), bf16),
-            pltpu.VMEM((half, q_width), f32),
-            pltpu.VMEM((tokens, k_width), f32),
             pltpu.VMEM((half, q_width), f32),
             pltpu.VMEM((tokens, k_width), f32),
             pltpu.VMEM((half, q_width), bf16),
-            pltpu.VMEM((tokens, 2 * k_width), f32),
+            pltpu.VMEM((tokens, k_width), f32),
         ],
-        (
-            own,
-            mate,
-            far,
-            far_mate,
-            query_gain,
-            key_gain,
-            *[jnp.asarray(table) for table in tables],
-        ),
-        flops=10 * heads * half * tokens * HEAD_CHANNELS,
-        limit=32 * MIB,
-    )
-
-
-def weight_partials(turned, p_own, p_far, dp_count):
+        (*state, *gains, *tables),
+        flops=6 * heads * half * tokens * HEAD_CHANNELS,
+        limit=20 * MIB,
+    )
+
+
+def weight_partials(turned, p_own, p_far, extra, dp_count):
     feats, half = turned.shape
     rows, cols = half // 2, p_own.shape[1]
     share = feats // dp_count
     chips = dp_count // 2
 
-    def body(x_ref, po_ref, pf_ref, mine_out, mate_out, own_out, send_out, p_sc):
+    def body(x_ref, po_ref, pf_ref, *rest):
+        mine_out, mate_out, own_out, send_out, p_sc = rest[len(extra) :]
         bit = lax.axis_index("sp") % 2
         mine = lax.axis_index("dp")
         p_sc[...] = (po_ref[...] + pf_ref[...].astype(f32)).astype(bf16)
         p_mine = p_sc[pl.ds(pl.multiple_of(bit * rows, rows), rows), :]
         p_mate = p_sc[pl.ds(pl.multiple_of((1 - bit) * rows, rows), rows), :]
         mine_out[...] = p_mine
-        mate_out[...] = p_mate
+        mate_out[:, :cols] = p_mate
+        lo = cols
+        for ref in rest[: len(extra)]:
+            mate_out[:, lo : lo + ref.shape[1]] = ref[...]
+            lo += ref.shape[1]
         p_all = jnp.concatenate([p_mine, p_mate], axis=0)
         for out, flip in ((send_out, 1), (own_out, 0)):
             for m in range(chips):
@@ -550,69 +592,75 @@
 
     return kernel_call(
         body,
-        [held((rows, cols))] * 2 + [held((chips, share, cols))] * 2,
+        [held((rows, cols)), held((rows, cols + sum(value.shape[1] for value in extra)))]
+        + [held((chips, share, cols))] * 2,
         [pltpu.VMEM((half, cols), bf16)],
-        (turned, p_own, p_far),
+        (turned, p_own, p_far, *extra),
         flops=2 * feats * half * cols,
     )
 
 
-def sum_over_devices(own, sent):
-    received = swap_with(sent, "dp", 1)
-    chips = own.shape[0]
-    paired = [own[m].astype(f32) + received[m].astype(f32) for m in range(chips)]
-    total = paired[0]
-    for m in range(1, chips):
-        total = total + swap_with(paired[m].astype(bf16), "dp", 2 * m).astype(f32)
-    return total.astype(bf16)
-
-
-def join_weight_grads(own, mate, far, far_mate):
+def sum_cores(own, received):
+    chips, share, cols = own.shape
+
+    def body(own_ref, got_ref, first, *rest):
+        first[...] = own_ref[0].astype(f32) + got_ref[0].astype(f32)
+        for m, out in enumerate(rest, 1):
+            out[...] = (own_ref[m].astype(f32) + got_ref[m].astype(f32)).astype(bf16)
+
+    return kernel_call(
+        body, [held((share, cols), f32)] + [held((share, cols))] * (chips - 1), [], (own, received)
+    )
+
+
+def sum_chips(first, received):
+    def body(*refs):
+        total = refs[0][...]
+        for ref in refs[1:-1]:
+            total = total + ref[...].astype(f32)
+        refs[-1][...] = total.astype(bf16)
+
+    return kernel_call(body, [held(first.shape)], [], (first, *received))[0]
+
+
+def join_weight_grad(own, mate, far, far_mate):
     rows, cols = own.shape
-    half = cols // 2
-
-    def body(own_ref, mate_ref, far_ref, far_mate_ref, k_out, v_out, k_sc, v_sc, sems):
+
+    def body(own_ref, mate_ref, far_ref, far_mate_ref, out, scratch, sem):
         even = lax.axis_index("sp") % 2 == 0
         here = own_ref[...].astype(f32) + far_ref[...].astype(f32)
         there = mate_ref[...].astype(f32) + far_mate_ref[...].astype(f32)
-        copies = []
-        for i, (scratch, out, lanes) in enumerate(
-            ((k_sc, k_out, slice(0, half)), (v_sc, v_out, slice(half, cols)))
-        ):
-            scratch[:, :half] = jnp.where(even, here[:, lanes], there[:, lanes])
-            scratch[:, half:] = jnp.where(even, there[:, lanes], here[:, lanes])
-            copy = pltpu.make_async_copy(scratch, out, sems.at[i])
-            copy.start()
-            copies.append(copy)
-        for copy in copies:
-            copy.wait()
+        scratch[:, :cols] = jnp.where(even, here, there)
+        scratch[:, cols:] = jnp.where(even, there, here)
+        copy = pltpu.make_async_copy(scratch, out, sem)
+        copy.start()
+        copy.wait()
 
     return pl.pallas_call(
         body,
-        out_shape=[shape_of((rows, cols), f32)] * 2,
+        out_shape=shape_of((rows, 2 * cols), f32),
         in_specs=[pl.BlockSpec(memory_space=pltpu.VMEM)] * 4,
-        out_specs=[pl.BlockSpec(memory_space=pltpu.HBM)] * 2,
-        scratch_shapes=[pltpu.VMEM((rows, cols), f32)] * 2 + [pltpu.SemaphoreType.DMA((2,))],
+        out_specs=pl.BlockSpec(memory_space=pltpu.HBM),
+        scratch_shapes=[pltpu.VMEM((rows, 2 * cols), f32), pltpu.SemaphoreType.DMA],
         compiler_params=pltpu.CompilerParams(vmem_limit_bytes=4 * MIB),
-        name="join_weight_grads",
     )(*[in_vmem(piece) for piece in (own, mate, far, far_mate)])
 
 
-def token_outputs(p_mine, p_from_mate, weight_pieces, dq_own, dq_from_mate):
-    rows, cols = p_mine.shape
+def token_outputs(k_mine, v_mine, from_mate, weight_pieces, dq_own):
+    rows, cols = k_mine.shape
     q_half = dq_own.shape[1]
     dp_count = len(weight_pieces)
     w_rows = weight_pieces[0].shape[0]
 
-    def body(p_ref, pm_ref, dq_ref, dqm_ref, *rest):
+    def body(k_ref, v_ref, mate_ref, dq_ref, *rest):
         w_refs = rest[:dp_count]
         x_out, q_out, p_buf, out_buf, q_buf = rest[dp_count:]
         bit = lax.axis_index("sp") % 2
         mine = lax.axis_index("dp")
-        p_buf[bit] = p_ref[...]
-        p_buf[1 - bit] = pm_ref[...]
+        p_buf[bit] = jnp.concatenate([k_ref[...], v_ref[...]], axis=1)
+        p_buf[1 - bit] = mate_ref[:, : 2 * cols]
         q_buf[bit] = dq_ref[...]
-        q_buf[1 - bit] = dqm_ref[...]
+        q_buf[1 - bit] = mate_ref[:, 2 * cols :]
         for d in range(2):
             q_out[:, d * q_half : (d + 1) * q_half] = q_buf[d]
         left = jnp.concatenate([p_buf[0], p_buf[1]], axis=1)
@@ -625,12 +673,12 @@
         body,
         [shape_of((rows, dp_count * w_rows)), shape_of((rows, 2 * q_half))],
         [
-            pltpu.VMEM((2, rows, cols), bf16),
+            pltpu.VMEM((2, rows, 2 * cols), bf16),
             pltpu.VMEM((dp_count, rows, w_rows), bf16),
             pltpu.VMEM((2, rows, q_half), bf16),
         ],
-        (p_mine, p_from_mate, dq_own, dq_from_mate, *weight_pieces),
-        flops=4 * rows * dp_count * w_rows * cols,
+        (k_mine, v_mine, from_mate, dq_own, *weight_pieces),
+        flops=8 * rows * dp_count * w_rows * cols,
     )
 
 
@@ -654,28 +702,44 @@
     inputs, queries, keys, values, out_grad, query_gain, key_gain, key_matrix, value_matrix
 ):
     dp_count = lax.axis_size("dp")
+    chips = dp_count // 2
     mate, far, far_mate = pack_heads(queries, keys, values, out_grad)
     mate = swap_with(mate, "sp", 1)
     far = swap_with(far, "sp", 2)
     far_mate = swap_with(far_mate, "sp", 3)
-    own, joined_weight, query_gain, key_gain = pack_own(
-        queries, keys, values, out_grad, key_matrix, value_matrix, query_gain, key_gain
-    )
+    tables = [jnp.asarray(table) for table in angle_tables(4 * inputs.shape[0])]
+    own, joined_weight, *small = pack_own(
+        queries,
+        keys,
+        values,
+        out_grad,
+        key_matrix,
+        value_matrix,
+        [query_gain[None], key_gain[None], *tables],
+    )
+    gains, tables = small[:2], small[2:]
     weight_pieces = [joined_weight] + [
         swap_with(joined_weight, "dp", m) for m in range(1, dp_count)
     ]
     mate_inputs = swap_with(inputs, "sp", 1)
-    dq_own, dq_mate, p_own, p_far = attention(own, mate, far, far_mate, query_gain, key_gain)
-    p_far = swap_with(p_far, "sp", 2)
-    dq_mate = swap_with(dq_mate, "sp", 1)
+    v_own, v_far, state = attention_values(own, mate, far, far_mate, gains, tables)
+    v_far = swap_with(v_far, "sp", 2)
+    dq_own, dq_mate, k_own, k_far = attention_keys(state, gains, tables)
+    k_far = swap_with(k_far, "sp", 2)
     turned = turn_inputs(inputs, mate_inputs)
-    p_mine, p_mate, own, sent = weight_partials(turned, p_own, p_far, dp_count)
-    summed = sum_over_devices(own, sent)
-    p_mate = swap_with(p_mate, "sp", 1)
-    input_grad, query_grad = token_outputs(p_mine, p_mate, weight_pieces, dq_own, dq_mate)
-    key_weight, value_weight = join_weight_grads(
-        summed, *[swap_with(summed, "sp", k) for k in range(1, 4)]
-    )
+
+    def weight_grad(p_own, p_far, extra):
+        mine, there, blocks, sent = weight_partials(turned, p_own, p_far, extra, dp_count)
+        first, *rest = sum_cores(blocks, swap_with(sent, "dp", 1))
+        received = [swap_with(rest[m - 1], "dp", 2 * m) for m in range(1, chips)]
+        total = sum_chips(first, received)
+        others = [swap_with(total, "sp", k) for k in range(1, 4)]
+        return mine, there, join_weight_grad(total, *others)
+
+    v_mine, v_there, value_weight = weight_grad(v_own, v_far, ())
+    k_mine, there, key_weight = weight_grad(k_own, k_far, (v_there, dq_mate))
+    from_mate = swap_with(there, "sp", 1)
+    input_grad, query_grad = token_outputs(k_mine, v_mine, from_mate, weight_pieces, dq_own)
     return input_grad[None], query_grad[None], key_weight, value_weight
 
 

time: 91.3 us -> 108 us (1.18)
  waiting for transfers between devices: 52.4 us -> 59.6 us
  starting transfers between devices: 25.6 us -> 32.6 us
  Pallas kernels: 12.1 us -> 14.2 us
    ppermute x21 -> x28, waiting for transfers between devices: 52.4 us -> 59.6 us  [swap_with(): return lax.ppermute(value, axis, [(i, i ^ k) for i in range(count)])]
    ppermute x21 -> x28, starting transfers between devices: 25.6 us -> 32.6 us  [swap_with(): return lax.ppermute(value, axis, [(i, i ^ k) for i in range(count)])]
    pallas_call x4 -> x10, Pallas kernels: 9.03 us -> 10.4 us  [kernel_call(): pl.pallas_call(body, out_shape=out_shape, in_specs=[vmem] * len(args), ou...]
  transfers between devices with their start and end apart: 21 -> 28, of which waited for: 9 -> 9; matrix products, arithmetic and copies ran while one was open for 0% -> 0% of each run, Pallas kernels for 12% -> 12%
where the time goes in v4:
time: 108 us
  waiting for transfers between devices  59.6 us (55%)
  starting transfers between devices  32.6 us (30%)
  Pallas kernels  14.2 us (13%)
    ppermute x28, waiting for transfers between devices, swap_with(): return lax.ppermute(value, axis, [(i, i ^ k) for i in range(count)])  59.6 us
    ppermute x28, starting transfers between devices, swap_with(): return lax.ppermute(value, axis, [(i, i ^ k) for i in range(count)])  32.6 us
    pallas_call x10, Pallas kernels, kernel_call(): pl.pallas_call(body, out_shape=out_shape, in_specs=[vmem] * len(args), ou...  10.4 us
    pallas_call x2, Pallas kernels, copy_call(): pl.pallas_call(run, out_shape=out_shape, in_specs=[pl.BlockSpec(memory_sp...  2.27 us
  transfers between devices with their start and end apart: 28, of which 9 were waited for; matrix products, arithmetic and copies ran while one was open for 0% of the time, Pallas kernels for 12%

profile of v4, /device:TPU:0, one launch (start us, length us, event | category | flops | bytes accessed | tf_op | source)
XLA Modules:
  0.0 108.1 jit_solution(18349064687960982045)
XLA Ops:
  0.6 3.1 %collective-permute-start = (bf16[128,2048]{1,0:T(8,128)(2,1)}, bf16[128,2048]{1,0:T(8,128)(2,1)S(1)}, u32[]{:S(2)}, u32[]{:S(2)}) collective-permute-start(bf16[128,2048]{1,0:T(8,128)(2,1)} %bitcast.9), channel_id=1, source_target_pairs={{0,8},{8,0},{16,24},{24,16},{1,9},{9,1},{17,25},{25,17},{2,10},{10... | collective-permute-start | bytes 1572872 | tf_op jit(solution)/shard_map/ppermute | solution.py:264
  3.7 1.0 shard_map.158
  4.8 0.1 collective-permute-start.1
  4.9 3.0 %collective-permute-start.2 = (bf16[128,256]{1,0:T(8,128)(2,1)S(1)}, bf16[128,256]{1,0:T(8,128)(2,1)S(1)}, u32[]{:S(2)}, u32[]{:S(2)}) collective-permute-start(bf16[128,256]{1,0:T(8,128)(2,1)S(1)} %get-tuple-element.50), channel_id=1, source_target_pairs={{0,16},{8,24},{16,0},{24,8},{1,17},{9,25},{17,1},{25,9},{2,18},{10... | collective-permute-start | bytes 196616 | tf_op jit(solution)/shard_map/ppermute | solution.py:264
  7.9 1.3 %collective-permute-start.3 = (bf16[128,256]{1,0:T(8,128)(2,1)S(1)}, bf16[128,256]{1,0:T(8,128)(2,1)S(1)}, u32[]{:S(2)}, u32[]{:S(2)}) collective-permute-start(bf16[128,256]{1,0:T(8,128)(2,1)S(1)} %get-tuple-element.51), channel_id=1, source_target_pairs={{0,24},{8,16},{16,8},{24,0},{1,25},{9,17},{17,9},{25,1},{2,26},{10... | collective-permute-start | bytes 196616 | tf_op jit(solution)/shard_map/ppermute | solution.py:264
  9.3 1.2 %shard_map.157 = (bf16[128,1280]{1,0:T(8,128)(2,1)S(1)}, bf16[256,512]{1,0:T(8,128)(2,1)S(1)}, f32[1,64]{1,0:T(1,128)S(1)}, f32[1,64]{1,0:T(1,128)S(1)}, f32[8,1...) custom-call(bf16[128,1024]{1,0:T(8,128)(2,1)} %bitcast.12, ...), custom_call_target="tpu_custom_call" | custom-call | tf_op jit(solution)/shard_map/pallas_call | solution.py:279
  10.5 13.8 %collective-permute-done.2.refs_2_ = bf16[128,256]{1,0:T(8,128)(2,1)S(1)} collective-permute-done((bf16[128,256]{1,0:T(8,128)(2,1)S(1)}, bf16[128,256]{1,0:T(8,128)(2,1)S(1)}, u32[]{:S(2)}, u32[]{:S(2)}) %collective-permute-start.2) | collective-permute-done | bytes 65568 | tf_op jit(solution)/shard_map/ppermute | solution.py:264
  24.3 3.6 %collective-permute-done.3.refs_3_ = bf16[128,256]{1,0:T(8,128)(2,1)S(1)} collective-permute-done((bf16[128,256]{1,0:T(8,128)(2,1)S(1)}, bf16[128,256]{1,0:T(8,128)(2,1)S(1)}, u32[]{:S(2)}, u32[]{:S(2)}) %collective-permute-start.3) | collective-permute-done | bytes 65568 | tf_op jit(solution)/shard_map/ppermute | solution.py:264
  27.9 0.0 collective-permute-done.1.refs_1_
  27.9 3.1 %shard_map.159 = (f32[256,128]{1,0:T(8,128)S(1)}, bf16[256,128]{1,0:T(8,128)(2,1)S(1)}, f32[8,512,256]{2,1,0:T(8,128)S(1)}, bf16[8,256,64]{2,1,0:T(8,128)(2,1)S(...) custom-call(bf16[128,1280]{1,0:T(8,128)(2,1)S(1)} %get-tuple-element, ...), custom_call_target="tpu_custom_call" | custom-call | flops 268435456 | tf_op jit(solution)/shard_map/pallas_call | solution.py:243
  31.1 0.1 collective-permute-start.5
  31.1 0.0 collective-permute-done.mate_ref
  31.2 0.0 copy-start
  31.2 1.0 copy-done
  32.2 0.3 shard_map.156.x_ref
  32.5 3.8 %collective-permute-done.5.pf_ref = bf16[256,128]{1,0:T(8,128)(2,1)S(1)} collective-permute-done((bf16[256,128]{1,0:T(8,128)(2,1)S(1)}, bf16[256,128]{1,0:T(8,128)(2,1)S(1)}, u32[]{:S(2)}, u32[]{:S(2)}) %collective-permute-start.5) | collective-permute-done | bytes 65568 | tf_op jit(solution)/shard_map/ppermute | solution.py:264
  36.3 0.4 shard_map.161
  36.7 0.1 collective-permute-start.21
  36.8 4.2 %shard_map.160 = (bf16[128,512]{1,0:T(8,128)(2,1)S(1)}, bf16[128,512]{1,0:T(8,128)(2,1)S(1)}, f32[256,128]{1,0:T(8,128)S(1)}, bf16[256,128]{1,0:T(8,128)(2,1)S(1)}) custom-call(f32[8,512,256]{2,1,0:T(8,128)S(1)} %get-tuple-element.58.refs_0_, bf16[8,256,64]{2,1,0:T(8,128)(2,1)S(1)} %get-tuple-element.59.refs_1_, ...), custom_call_target="tpu_custom_call" | custom-call | flops 402653184 | tf_op jit(solution)/shard_map/pallas_call | solution.py:243
  41.0 0.1 collective-permute-start.4
  41.1 1.6 %collective-permute-start.10 = (bf16[256,512]{1,0:T(8,128)(2,1)S(1)}, bf16[256,512]{1,0:T(8,128)(2,1)S(1)}, u32[]{:S(2)}, u32[]{:S(2)}) collective-permute-start(bf16[256,512]{1,0:T(8,128)(2,1)S(1)} %get-tuple-element.77.rest_0_), channel_id=1, source_target_pairs={{0,4},{1,5},{2,6},{3,7},{4,0},{5,1},{6,2},{7,3},{8,12},{9,13},{10,... | collective-permute-start | bytes 786440 | tf_op jit(solution)/shard_map/ppermute | solution.py:264
  42.7 4.5 %collective-permute-done.4.pf_ref = bf16[256,128]{1,0:T(8,128)(2,1)S(1)} collective-permute-done((bf16[256,128]{1,0:T(8,128)(2,1)S(1)}, bf16[256,128]{1,0:T(8,128)(2,1)S(1)}, u32[]{:S(2)}, u32[]{:S(2)}) %collective-permute-start.4) | collective-permute-done | bytes 65568 | tf_op jit(solution)/shard_map/ppermute | solution.py:264
  47.2 0.4 shard_map.162
  47.6 0.1 collective-permute-start.14
  47.7 1.6 %collective-permute-start.11 = (bf16[256,512]{1,0:T(8,128)(2,1)S(1)}, bf16[256,512]{1,0:T(8,128)(2,1)S(1)}, u32[]{:S(2)}, u32[]{:S(2)}) collective-permute-start(bf16[256,512]{1,0:T(8,128)(2,1)S(1)} %get-tuple-element.77.rest_0_), channel_id=1, source_target_pairs={{0,5},{1,4},{2,7},{3,6},{4,1},{5,0},{6,3},{7,2},{8,13},{9,12},{10,... | collective-permute-start | bytes 786440 | tf_op jit(solution)/shard_map/ppermute | solution.py:264
  49.3 1.4 %collective-permute-start.12 = (bf16[256,512]{1,0:T(8,128)(2,1)S(1)}, bf16[256,512]{1,0:T(8,128)(2,1)S(1)}, u32[]{:S(2)}, u32[]{:S(2)}) collective-permute-start(bf16[256,512]{1,0:T(8,128)(2,1)S(1)} %get-tuple-element.77.rest_0_), channel_id=1, source_target_pairs={{0,6},{1,7},{2,4},{3,5},{4,2},{5,3},{6,0},{7,1},{8,14},{9,15},{10,... | collective-permute-start | bytes 786440 | tf_op jit(solution)/shard_map/ppermute | solution.py:264
  50.7 0.9 collective-permute-start.13
  51.6 0.1 shard_map.167
  51.7 0.0 collective-permute-done.10.rest_4_
  51.7 1.6 %collective-permute-start.22 = (bf16[256,128]{1,0:T(8,128)(2,1)S(1)}, bf16[256,128]{1,0:T(8,128)(2,1)S(1)}, u32[]{:S(2)}, u32[]{:S(2)}) collective-permute-start(bf16[256,128]{1,0:T(8,128)(2,1)S(1)} %get-tuple-element.89), channel_id=1, source_target_pairs={{0,2},{1,3},{2,0},{3,1},{4,6},{5,7},{6,4},{7,5},{8,10},{9,11},{10,... | collective-permute-start | bytes 196616 | tf_op jit(solution)/shard_map/ppermute | solution.py:264
  53.3 0.0 collective-permute-done.14.got_ref
  53.3 0.5 collective-permute-start.23
  53.8 0.1 shard_map.164
  53.8 13.4 %collective-permute-done.11.rest_5_ = bf16[256,512]{1,0:T(8,128)(2,1)S(1)} collective-permute-done((bf16[256,512]{1,0:T(8,128)(2,1)S(1)}, bf16[256,512]{1,0:T(8,128)(2,1)S(1)}, u32[]{:S(2)}, u32[]{:S(2)}) %collective-permute-start.11) | collective-permute-done | bytes 262176 | tf_op jit(solution)/shard_map/ppermute | solution.py:264
  67.2 0.8 collective-permute-start.7
  68.0 1.5 %collective-permute-start.8 = (bf16[256,512]{1,0:T(8,128)(2,1)S(1)}, bf16[256,512]{1,0:T(8,128)(2,1)S(1)}, u32[]{:S(2)}, u32[]{:S(2)}) collective-permute-start(bf16[256,512]{1,0:T(8,128)(2,1)S(1)} %get-tuple-element.77.rest_0_), channel_id=1, source_target_pairs={{0,2},{1,3},{2,0},{3,1},{4,6},{5,7},{6,4},{7,5},{8,10},{9,11},{10,... | collective-permute-start | bytes 786440 | tf_op jit(solution)/shard_map/ppermute | solution.py:264
  69.5 0.0 collective-permute-done.22.refs_1_
  69.5 2.3 %collective-permute-start.24 = (bf16[256,128]{1,0:T(8,128)(2,1)S(1)}, bf16[256,128]{1,0:T(8,128)(2,1)S(1)}, u32[]{:S(2)}, u32[]{:S(2)}) collective-permute-start(bf16[256,128]{1,0:T(8,128)(2,1)S(1)} %get-tuple-element.91), channel_id=1, source_target_pairs={{0,6},{1,7},{2,4},{3,5},{4,2},{5,3},{6,0},{7,1},{8,14},{9,15},{10,... | collective-permute-start | bytes 196616 | tf_op jit(solution)/shard_map/ppermute | solution.py:264
  71.8 0.0 collective-permute-done.23.refs_2_
  71.8 0.7 collective-permute-start.15
  72.6 12.3 %collective-permute-done.24.refs_3_ = bf16[256,128]{1,0:T(8,128)(2,1)S(1)} collective-permute-done((bf16[256,128]{1,0:T(8,128)(2,1)S(1)}, bf16[256,128]{1,0:T(8,128)(2,1)S(1)}, u32[]{:S(2)}, u32[]{:S(2)}) %collective-permute-start.24) | collective-permute-done | bytes 65568 | tf_op jit(solution)/shard_map/ppermute | solution.py:264
  84.9 0.5 collective-permute-start.16
  85.4 0.0 collective-permute-done.15.refs_1_
  85.4 1.0 collective-permute-start.6
  86.4 2.7 %collective-permute-done.16.refs_2_ = bf16[256,128]{1,0:T(8,128)(2,1)S(1)} collective-permute-done((bf16[256,128]{1,0:T(8,128)(2,1)S(1)}, bf16[256,128]{1,0:T(8,128)(2,1)S(1)}, u32[]{:S(2)}, u32[]{:S(2)}) %collective-permute-start.16) | collective-permute-done | bytes 65568 | tf_op jit(solution)/shard_map/ppermute | solution.py:264
  89.2 1.4 %collective-permute-start.17 = (bf16[256,128]{1,0:T(8,128)(2,1)S(1)}, bf16[256,128]{1,0:T(8,128)(2,1)S(1)}, u32[]{:S(2)}, u32[]{:S(2)}) collective-permute-start(bf16[256,128]{1,0:T(8,128)(2,1)S(1)} %get-tuple-element.85), channel_id=1, source_target_pairs={{0,6},{1,7},{2,4},{3,5},{4,2},{5,3},{6,0},{7,1},{8,14},{9,15},{10,... | collective-permute-start | bytes 196616 | tf_op jit(solution)/shard_map/ppermute | solution.py:264
  90.7 3.7 %collective-permute-done.17.refs_3_ = bf16[256,128]{1,0:T(8,128)(2,1)S(1)} collective-permute-done((bf16[256,128]{1,0:T(8,128)(2,1)S(1)}, bf16[256,128]{1,0:T(8,128)(2,1)S(1)}, u32[]{:S(2)}, u32[]{:S(2)}) %collective-permute-start.17) | collective-permute-done | bytes 65568 | tf_op jit(solution)/shard_map/ppermute | solution.py:264
  94.4 1.0 collective-permute-start.25
  95.4 0.0 collective-permute-done.7.rest_1_
  95.4 1.5 %collective-permute-start.26 = (bf16[256,128]{1,0:T(8,128)(2,1)S(1)}, bf16[256,128]{1,0:T(8,128)(2,1)S(1)}, u32[]{:S(2)}, u32[]{:S(2)}) collective-permute-start(bf16[256,128]{1,0:T(8,128)(2,1)S(1)} %shard_map.168.own_ref), channel_id=1, source_target_pairs={{0,16},{8,24},{16,0},{24,8},{1,17},{9,25},{17,1},{25,9},{2,18},{10... | collective-permute-start | bytes 196616 | tf_op jit(solution)/shard_map/ppermute | solution.py:264
  96.9 0.0 collective-permute-done.8.rest_2_
  96.9 1.9 %collective-permute-start.27 = (bf16[256,128]{1,0:T(8,128)(2,1)S(1)}, bf16[256,128]{1,0:T(8,128)(2,1)S(1)}, u32[]{:S(2)}, u32[]{:S(2)}) collective-permute-start(bf16[256,128]{1,0:T(8,128)(2,1)S(1)} %shard_map.168.own_ref), channel_id=1, source_target_pairs={{0,24},{8,16},{16,8},{24,0},{1,25},{9,17},{17,9},{25,1},{2,26},{10... | collective-permute-start | bytes 196616 | tf_op jit(solution)/shard_map/ppermute | solution.py:264
  98.9 0.0 collective-permute-done.9.rest_3_
  98.9 0.1 collective-permute-start.18
  99.0 0.0 collective-permute-done.6.mate_ref
  99.0 2.3 %collective-permute-start.19 = (bf16[256,128]{1,0:T(8,128)(2,1)S(1)}, bf16[256,128]{1,0:T(8,128)(2,1)S(1)}, u32[]{:S(2)}, u32[]{:S(2)}) collective-permute-start(bf16[256,128]{1,0:T(8,128)(2,1)S(1)} %shard_map.165.own_ref), channel_id=1, source_target_pairs={{0,16},{8,24},{16,0},{24,8},{1,17},{9,25},{17,1},{25,9},{2,18},{10... | collective-permute-start | bytes 196616 | tf_op jit(solution)/shard_map/ppermute | solution.py:264
  101.3 0.0 collective-permute-done.25.mate_ref
  101.3 1.9 %collective-permute-start.20 = (bf16[256,128]{1,0:T(8,128)(2,1)S(1)}, bf16[256,128]{1,0:T(8,128)(2,1)S(1)}, u32[]{:S(2)}, u32[]{:S(2)}) collective-permute-start(bf16[256,128]{1,0:T(8,128)(2,1)S(1)} %shard_map.165.own_ref), channel_id=1, source_target_pairs={{0,24},{8,16},{16,8},{24,0},{1,25},{9,17},{17,9},{25,1},{2,26},{10... | collective-permute-start | bytes 196616 | tf_op jit(solution)/shard_map/ppermute | solution.py:264
  103.3 1.7 %shard_map.163 = (bf16[128,2048]{1,0:T(8,128)(2,1)}, bf16[128,1024]{1,0:T(8,128)(2,1)}) custom-call(bf16[128,128]{1,0:T(8,128)(2,1)S(1)} %get-tuple-element.73.k_ref, bf16[128,128]{1,0:T(8,128)(2,1)S(1)} %get-tuple-element.74.v_ref, bf16[128,768]{1,0:T(8,128)(2,1)S(1)} %collective-permute-done.6.mate_ref, bf16[128,512]{1,0:T(8,128)(2,1)S(1)} %get-tuple-element.76.dq_ref, ...), custom_call_target="tpu_custom_call" | custom-call | flops 268435456 | tf_op jit(solution)/shard_map/pallas_call | solution.py:243
  104.9 0.0 collective-permute-done.26.far_ref
  104.9 0.0 collective-permute-done.27.far_mate_ref
  104.9 0.8 shard_map.169
  105.7 1.7 %collective-permute-done.20.far_mate_ref = bf16[256,128]{1,0:T(8,128)(2,1)S(1)} collective-permute-done((bf16[256,128]{1,0:T(8,128)(2,1)S(1)}, bf16[256,128]{1,0:T(8,128)(2,1)S(1)}, u32[]{:S(2)}, u32[]{:S(2)}) %collective-permute-start.20) | collective-permute-done | bytes 65568 | tf_op jit(solution)/shard_map/ppermute | solution.py:264
  107.4 0.8 shard_map.166
  (8 shorter events, 0.1 us)
Async XLA Ops:
  0.6 30.5 %collective-permute-start = (bf16[128,2048]{1,0:T(8,128)(2,1)}, bf16[128,2048]{1,0:T(8,128)(2,1)S(1)}, u32[]{:S(2)}, u32[]{:S(2)}) collective-permute-start(bf16[128,2048]{1,0:T(8,128)(2,1)} %bitcast.9), channel_id=1, source_target_pairs={{0,8},{8,0},{16,24},{24,16},{1,9},{9,1},{17,25},{25,17},{2,10},{10... | collective-permute-start | bytes 1572872 | tf_op jit(solution)/shard_map/ppermute | solution.py:264
  4.8 23.1 %collective-permute-start.1 = (bf16[128,1280]{1,0:T(8,128)(2,1)S(1)}, bf16[128,1280]{1,0:T(8,128)(2,1)S(1)}, u32[]{:S(2)}, u32[]{:S(2)}) collective-permute-start(bf16[128,1280]{1,0:T(8,128)(2,1)S(1)} %get-tuple-element.49), channel_id=1, source_target_pairs={{0,8},{8,0},{16,24},{24,16},{1,9},{9,1},{17,25},{25,17},{2,10},{10... | collective-permute-start | bytes 983048 | tf_op jit(solution)/shard_map/ppermute | solution.py:264
  4.9 19.4 %collective-permute-start.2 = (bf16[128,256]{1,0:T(8,128)(2,1)S(1)}, bf16[128,256]{1,0:T(8,128)(2,1)S(1)}, u32[]{:S(2)}, u32[]{:S(2)}) collective-permute-start(bf16[128,256]{1,0:T(8,128)(2,1)S(1)} %get-tuple-element.50), channel_id=1, source_target_pairs={{0,16},{8,24},{16,0},{24,8},{1,17},{9,25},{17,1},{25,9},{2,18},{10... | collective-permute-start | bytes 196616 | tf_op jit(solution)/shard_map/ppermute | solution.py:264
  7.9 20.0 %collective-permute-start.3 = (bf16[128,256]{1,0:T(8,128)(2,1)S(1)}, bf16[128,256]{1,0:T(8,128)(2,1)S(1)}, u32[]{:S(2)}, u32[]{:S(2)}) collective-permute-start(bf16[128,256]{1,0:T(8,128)(2,1)S(1)} %get-tuple-element.51), channel_id=1, source_target_pairs={{0,24},{8,16},{16,8},{24,0},{1,25},{9,17},{17,9},{25,1},{2,26},{10... | collective-permute-start | bytes 196616 | tf_op jit(solution)/shard_map/ppermute | solution.py:264
  31.1 5.2 %collective-permute-start.5 = (bf16[256,128]{1,0:T(8,128)(2,1)S(1)}, bf16[256,128]{1,0:T(8,128)(2,1)S(1)}, u32[]{:S(2)}, u32[]{:S(2)}) collective-permute-start(bf16[256,128]{1,0:T(8,128)(2,1)S(1)} %get-tuple-element.70), channel_id=1, source_target_pairs={{0,16},{8,24},{16,0},{24,8},{1,17},{9,25},{17,1},{25,9},{2,18},{10... | collective-permute-start | bytes 196616 | tf_op jit(solution)/shard_map/ppermute | solution.py:264
  31.2 1.0 copy-start
  36.7 14.0 %collective-permute-start.21 = (bf16[4,256,128]{2,1,0:T(8,128)(2,1)S(1)}, bf16[4,256,128]{2,1,0:T(8,128)(2,1)S(1)}, u32[]{:S(2)}, u32[]{:S(2)}) collective-permute-start(bf16[4,256,128]{2,1,0:T(8,128)(2,1)S(1)} %get-tuple-element.87), channel_id=1, source_target_pairs={{0,1},{1,0},{2,3},{3,2},{4,5},{5,4},{6,7},{7,6},{8,9},{9,8},{10,11... | collective-permute-start | bytes 786440 | tf_op jit(solution)/shard_map/ppermute | solution.py:264
  41.0 6.2 %collective-permute-start.4 = (bf16[256,128]{1,0:T(8,128)(2,1)S(1)}, bf16[256,128]{1,0:T(8,128)(2,1)S(1)}, u32[]{:S(2)}, u32[]{:S(2)}) collective-permute-start(bf16[256,128]{1,0:T(8,128)(2,1)S(1)} %get-tuple-element.68), channel_id=1, source_target_pairs={{0,16},{8,24},{16,0},{24,8},{1,17},{9,25},{17,1},{25,9},{2,18},{10... | collective-permute-start | bytes 196616 | tf_op jit(solution)/shard_map/ppermute | solution.py:264
  41.1 10.6 %collective-permute-start.10 = (bf16[256,512]{1,0:T(8,128)(2,1)S(1)}, bf16[256,512]{1,0:T(8,128)(2,1)S(1)}, u32[]{:S(2)}, u32[]{:S(2)}) collective-permute-start(bf16[256,512]{1,0:T(8,128)(2,1)S(1)} %get-tuple-element.77.rest_0_), channel_id=1, source_target_pairs={{0,4},{1,5},{2,6},{3,7},{4,0},{5,1},{6,2},{7,3},{8,12},{9,13},{10,... | collective-permute-start | bytes 786440 | tf_op jit(solution)/shard_map/ppermute | solution.py:264
  47.6 5.7 %collective-permute-start.14 = (bf16[4,256,128]{2,1,0:T(8,128)(2,1)S(1)}, bf16[4,256,128]{2,1,0:T(8,128)(2,1)S(1)}, u32[]{:S(2)}, u32[]{:S(2)}) collective-permute-start(bf16[4,256,128]{2,1,0:T(8,128)(2,1)S(1)} %get-tuple-element.81), channel_id=1, source_target_pairs={{0,1},{1,0},{2,3},{3,2},{4,5},{5,4},{6,7},{7,6},{8,9},{9,8},{10,11... | collective-permute-start | bytes 786440 | tf_op jit(solution)/shard_map/ppermute | solution.py:264
  47.7 19.5 %collective-permute-start.11 = (bf16[256,512]{1,0:T(8,128)(2,1)S(1)}, bf16[256,512]{1,0:T(8,128)(2,1)S(1)}, u32[]{:S(2)}, u32[]{:S(2)}) collective-permute-start(bf16[256,512]{1,0:T(8,128)(2,1)S(1)} %get-tuple-element.77.rest_0_), channel_id=1, source_target_pairs={{0,5},{1,4},{2,7},{3,6},{4,1},{5,0},{6,3},{7,2},{8,13},{9,12},{10,... | collective-permute-start | bytes 786440 | tf_op jit(solution)/shard_map/ppermute | solution.py:264
  49.3 18.7 %collective-permute-start.12 = (bf16[256,512]{1,0:T(8,128)(2,1)S(1)}, bf16[256,512]{1,0:T(8,128)(2,1)S(1)}, u32[]{:S(2)}, u32[]{:S(2)}) collective-permute-start(bf16[256,512]{1,0:T(8,128)(2,1)S(1)} %get-tuple-element.77.rest_0_), channel_id=1, source_target_pairs={{0,6},{1,7},{2,4},{3,5},{4,2},{5,3},{6,0},{7,1},{8,14},{9,15},{10,... | collective-permute-start | bytes 786440 | tf_op jit(solution)/shard_map/ppermute | solution.py:264
  50.7 18.8 %collective-permute-start.13 = (bf16[256,512]{1,0:T(8,128)(2,1)S(1)}, bf16[256,512]{1,0:T(8,128)(2,1)S(1)}, u32[]{:S(2)}, u32[]{:S(2)}) collective-permute-start(bf16[256,512]{1,0:T(8,128)(2,1)S(1)} %get-tuple-element.77.rest_0_), channel_id=1, source_target_pairs={{0,7},{1,6},{2,5},{3,4},{4,3},{5,2},{6,1},{7,0},{8,15},{9,14},{10,... | collective-permute-start | bytes 786440 | tf_op jit(solution)/shard_map/ppermute | solution.py:264
  51.7 17.8 %collective-permute-start.22 = (bf16[256,128]{1,0:T(8,128)(2,1)S(1)}, bf16[256,128]{1,0:T(8,128)(2,1)S(1)}, u32[]{:S(2)}, u32[]{:S(2)}) collective-permute-start(bf16[256,128]{1,0:T(8,128)(2,1)S(1)} %get-tuple-element.89), channel_id=1, source_target_pairs={{0,2},{1,3},{2,0},{3,1},{4,6},{5,7},{6,4},{7,5},{8,10},{9,11},{10,... | collective-permute-start | bytes 196616 | tf_op jit(solution)/shard_map/ppermute | solution.py:264
  53.3 18.6 %collective-permute-start.23 = (bf16[256,128]{1,0:T(8,128)(2,1)S(1)}, bf16[256,128]{1,0:T(8,128)(2,1)S(1)}, u32[]{:S(2)}, u32[]{:S(2)}) collective-permute-start(bf16[256,128]{1,0:T(8,128)(2,1)S(1)} %get-tuple-element.90), channel_id=1, source_target_pairs={{0,4},{1,5},{2,6},{3,7},{4,0},{5,1},{6,2},{7,3},{8,12},{9,13},{10,... | collective-permute-start | bytes 196616 | tf_op jit(solution)/shard_map/ppermute | solution.py:264
  67.2 28.2 %collective-permute-start.7 = (bf16[256,512]{1,0:T(8,128)(2,1)S(1)}, bf16[256,512]{1,0:T(8,128)(2,1)S(1)}, u32[]{:S(2)}, u32[]{:S(2)}) collective-permute-start(bf16[256,512]{1,0:T(8,128)(2,1)S(1)} %get-tuple-element.77.rest_0_), channel_id=1, source_target_pairs={{0,1},{1,0},{2,3},{3,2},{4,5},{5,4},{6,7},{7,6},{8,9},{9,8},{10,11... | collective-permute-start | bytes 786440 | tf_op jit(solution)/shard_map/ppermute | solution.py:264
  68.0 28.9 %collective-permute-start.8 = (bf16[256,512]{1,0:T(8,128)(2,1)S(1)}, bf16[256,512]{1,0:T(8,128)(2,1)S(1)}, u32[]{:S(2)}, u32[]{:S(2)}) collective-permute-start(bf16[256,512]{1,0:T(8,128)(2,1)S(1)} %get-tuple-element.77.rest_0_), channel_id=1, source_target_pairs={{0,2},{1,3},{2,0},{3,1},{4,6},{5,7},{6,4},{7,5},{8,10},{9,11},{10,... | collective-permute-start | bytes 786440 | tf_op jit(solution)/shard_map/ppermute | solution.py:264
  69.5 29.3 %collective-permute-start.9 = (bf16[256,512]{1,0:T(8,128)(2,1)S(1)}, bf16[256,512]{1,0:T(8,128)(2,1)S(1)}, u32[]{:S(2)}, u32[]{:S(2)}) collective-permute-start(bf16[256,512]{1,0:T(8,128)(2,1)S(1)} %get-tuple-element.77.rest_0_), channel_id=1, source_target_pairs={{0,3},{1,2},{2,1},{3,0},{4,7},{5,6},{6,5},{7,4},{8,11},{9,10},{10,... | collective-permute-start | bytes 786440 | tf_op jit(solution)/shard_map/ppermute | solution.py:264
  69.5 15.4 %collective-permute-start.24 = (bf16[256,128]{1,0:T(8,128)(2,1)S(1)}, bf16[256,128]{1,0:T(8,128)(2,1)S(1)}, u32[]{:S(2)}, u32[]{:S(2)}) collective-permute-start(bf16[256,128]{1,0:T(8,128)(2,1)S(1)} %get-tuple-element.91), channel_id=1, source_target_pairs={{0,6},{1,7},{2,4},{3,5},{4,2},{5,3},{6,0},{7,1},{8,14},{9,15},{10,... | collective-permute-start | bytes 196616 | tf_op jit(solution)/shard_map/ppermute | solution.py:264
  71.8 13.6 %collective-permute-start.15 = (bf16[256,128]{1,0:T(8,128)(2,1)S(1)}, bf16[256,128]{1,0:T(8,128)(2,1)S(1)}, u32[]{:S(2)}, u32[]{:S(2)}) collective-permute-start(bf16[256,128]{1,0:T(8,128)(2,1)S(1)} %get-tuple-element.83), channel_id=1, source_target_pairs={{0,2},{1,3},{2,0},{3,1},{4,6},{5,7},{6,4},{7,5},{8,10},{9,11},{10,... | collective-permute-start | bytes 196616 | tf_op jit(solution)/shard_map/ppermute | solution.py:264
  84.9 4.3 %collective-permute-start.16 = (bf16[256,128]{1,0:T(8,128)(2,1)S(1)}, bf16[256,128]{1,0:T(8,128)(2,1)S(1)}, u32[]{:S(2)}, u32[]{:S(2)}) collective-permute-start(bf16[256,128]{1,0:T(8,128)(2,1)S(1)} %get-tuple-element.84), channel_id=1, source_target_pairs={{0,4},{1,5},{2,6},{3,7},{4,0},{5,1},{6,2},{7,3},{8,12},{9,13},{10,... | collective-permute-start | bytes 196616 | tf_op jit(solution)/shard_map/ppermute | solution.py:264
  85.4 13.5 %collective-permute-start.6 = (bf16[128,768]{1,0:T(8,128)(2,1)S(1)}, bf16[128,768]{1,0:T(8,128)(2,1)S(1)}, u32[]{:S(2)}, u32[]{:S(2)}) collective-permute-start(bf16[128,768]{1,0:T(8,128)(2,1)S(1)} %get-tuple-element.75), channel_id=1, source_target_pairs={{0,8},{8,0},{16,24},{24,16},{1,9},{9,1},{17,25},{25,17},{2,10},{10... | collective-permute-start | bytes 589832 | tf_op jit(solution)/shard_map/ppermute | solution.py:264
  89.2 5.2 %collective-permute-start.17 = (bf16[256,128]{1,0:T(8,128)(2,1)S(1)}, bf16[256,128]{1,0:T(8,128)(2,1)S(1)}, u32[]{:S(2)}, u32[]{:S(2)}) collective-permute-start(bf16[256,128]{1,0:T(8,128)(2,1)S(1)} %get-tuple-element.85), channel_id=1, source_target_pairs={{0,6},{1,7},{2,4},{3,5},{4,2},{5,3},{6,0},{7,1},{8,14},{9,15},{10,... | collective-permute-start | bytes 196616 | tf_op jit(solution)/shard_map/ppermute | solution.py:264
  94.4 7.0 %collective-permute-start.25 = (bf16[256,128]{1,0:T(8,128)(2,1)S(1)}, bf16[256,128]{1,0:T(8,128)(2,1)S(1)}, u32[]{:S(2)}, u32[]{:S(2)}) collective-permute-start(bf16[256,128]{1,0:T(8,128)(2,1)S(1)} %shard_map.168.own_ref), channel_id=1, source_target_pairs={{0,8},{8,0},{16,24},{24,16},{1,9},{9,1},{17,25},{25,17},{2,10},{10... | collective-permute-start | bytes 196616 | tf_op jit(solution)/shard_map/ppermute | solution.py:264
  95.4 9.5 %collective-permute-start.26 = (bf16[256,128]{1,0:T(8,128)(2,1)S(1)}, bf16[256,128]{1,0:T(8,128)(2,1)S(1)}, u32[]{:S(2)}, u32[]{:S(2)}) collective-permute-start(bf16[256,128]{1,0:T(8,128)(2,1)S(1)} %shard_map.168.own_ref), channel_id=1, source_target_pairs={{0,16},{8,24},{16,0},{24,8},{1,17},{9,25},{17,1},{25,9},{2,18},{10... | collective-permute-start | bytes 196616 | tf_op jit(solution)/shard_map/ppermute | solution.py:264
  96.9 8.0 %collective-permute-start.27 = (bf16[256,128]{1,0:T(8,128)(2,1)S(1)}, bf16[256,128]{1,0:T(8,128)(2,1)S(1)}, u32[]{:S(2)}, u32[]{:S(2)}) collective-permute-start(bf16[256,128]{1,0:T(8,128)(2,1)S(1)} %shard_map.168.own_ref), channel_id=1, source_target_pairs={{0,24},{8,16},{16,8},{24,0},{1,25},{9,17},{17,9},{25,1},{2,26},{10... | collective-permute-start | bytes 196616 | tf_op jit(solution)/shard_map/ppermute | solution.py:264
  98.9 6.8 %collective-permute-start.18 = (bf16[256,128]{1,0:T(8,128)(2,1)S(1)}, bf16[256,128]{1,0:T(8,128)(2,1)S(1)}, u32[]{:S(2)}, u32[]{:S(2)}) collective-permute-start(bf16[256,128]{1,0:T(8,128)(2,1)S(1)} %shard_map.165.own_ref), channel_id=1, source_target_pairs={{0,8},{8,0},{16,24},{24,16},{1,9},{9,1},{17,25},{25,17},{2,10},{10... | collective-permute-start | bytes 196616 | tf_op jit(solution)/shard_map/ppermute | solution.py:264
  99.0 6.7 %collective-permute-start.19 = (bf16[256,128]{1,0:T(8,128)(2,1)S(1)}, bf16[256,128]{1,0:T(8,128)(2,1)S(1)}, u32[]{:S(2)}, u32[]{:S(2)}) collective-permute-start(bf16[256,128]{1,0:T(8,128)(2,1)S(1)} %shard_map.165.own_ref), channel_id=1, source_target_pairs={{0,16},{8,24},{16,0},{24,8},{1,17},{9,25},{17,1},{25,9},{2,18},{10... | collective-permute-start | bytes 196616 | tf_op jit(solution)/shard_map/ppermute | solution.py:264
  101.3 6.1 %collective-permute-start.20 = (bf16[256,128]{1,0:T(8,128)(2,1)S(1)}, bf16[256,128]{1,0:T(8,128)(2,1)S(1)}, u32[]{:S(2)}, u32[]{:S(2)}) collective-permute-start(bf16[256,128]{1,0:T(8,128)(2,1)S(1)} %shard_map.165.own_ref), channel_id=1, source_target_pairs={{0,24},{8,16},{16,8},{24,0},{1,25},{9,17},{17,9},{25,1},{2,26},{10... | collective-permute-start | bytes 196616 | tf_op jit(solution)/shard_map/ppermute | solution.py:264

commit v5 on v4

--- a/solution.py
+++ b/solution.py
@@ -343,14 +343,11 @@
     )
 
 
-def turn_inputs(own, mate):
-    rows, width = own.shape
-
-    def body(own_ref, mate_ref, out):
-        out[:, :rows] = own_ref[...].T
-        out[:, rows:] = mate_ref[...].T
-
-    return kernel_call(body, [held((width, 2 * rows))], [], (own, mate))[0]
+def turn_inputs(token_in):
+    def body(x_ref, out):
+        out[...] = x_ref[...].T
+
+    return kernel_call(body, [held(token_in.shape[::-1])], [], (token_in,))[0]
 
 
 def angle_tables(token_length):
@@ -565,13 +562,13 @@
     )
 
 
-def weight_partials(turned, p_own, p_far, extra, dp_count):
-    feats, half = turned.shape
-    rows, cols = half // 2, p_own.shape[1]
+def weight_partials(turned, turned_mate, p_own, p_far, extra, dp_count):
+    feats, rows = turned.shape
+    half, cols = p_own.shape
     share = feats // dp_count
     chips = dp_count // 2
 
-    def body(x_ref, po_ref, pf_ref, *rest):
+    def body(x_ref, xm_ref, po_ref, pf_ref, *rest):
         mine_out, mate_out, own_out, send_out, p_sc = rest[len(extra) :]
         bit = lax.axis_index("sp") % 2
         mine = lax.axis_index("dp")
@@ -588,14 +585,16 @@
         for out, flip in ((send_out, 1), (own_out, 0)):
             for m in range(chips):
                 start = pl.multiple_of((mine ^ (2 * m + flip)) * share, share)
-                out[m] = dot(x_ref[pl.ds(start, share), :], p_all, 1, 0).astype(bf16)
+                at = pl.ds(start, share)
+                x_all = jnp.concatenate([x_ref[at, :], xm_ref[at, :]], axis=1)
+                out[m] = dot(x_all, p_all, 1, 0).astype(bf16)
 
     return kernel_call(
         body,
         [held((rows, cols)), held((rows, cols + sum(value.shape[1] for value in extra)))]
         + [held((chips, share, cols))] * 2,
         [pltpu.VMEM((half, cols), bf16)],
-        (turned, p_own, p_far, *extra),
+        (turned, turned_mate, p_own, p_far, *extra),
         flops=2 * feats * half * cols,
     )
 
@@ -626,22 +625,26 @@
 def join_weight_grad(own, mate, far, far_mate):
     rows, cols = own.shape
 
-    def body(own_ref, mate_ref, far_ref, far_mate_ref, out, scratch, sem):
+    def body(own_ref, mate_ref, far_ref, far_mate_ref, out, scratch, sems):
         even = lax.axis_index("sp") % 2 == 0
-        here = own_ref[...].astype(f32) + far_ref[...].astype(f32)
-        there = mate_ref[...].astype(f32) + far_mate_ref[...].astype(f32)
-        scratch[:, :cols] = jnp.where(even, here, there)
-        scratch[:, cols:] = jnp.where(even, there, here)
-        copy = pltpu.make_async_copy(scratch, out, sem)
-        copy.start()
-        copy.wait()
+        copies = []
+        for i in range(2):
+            at = slice(i * rows // 2, (i + 1) * rows // 2)
+            here = own_ref[at, :].astype(f32) + far_ref[at, :].astype(f32)
+            there = mate_ref[at, :].astype(f32) + far_mate_ref[at, :].astype(f32)
+            scratch[at, :cols] = jnp.where(even, here, there)
+            scratch[at, cols:] = jnp.where(even, there, here)
+            copies.append(pltpu.make_async_copy(scratch.at[at, :], out.at[at, :], sems.at[i]))
+            copies[-1].start()
+        for copy in copies:
+            copy.wait()
 
     return pl.pallas_call(
         body,
         out_shape=shape_of((rows, 2 * cols), f32),
         in_specs=[pl.BlockSpec(memory_space=pltpu.VMEM)] * 4,
         out_specs=pl.BlockSpec(memory_space=pltpu.HBM),
-        scratch_shapes=[pltpu.VMEM((rows, 2 * cols), f32), pltpu.SemaphoreType.DMA],
+        scratch_shapes=[pltpu.VMEM((rows, 2 * cols), f32), pltpu.SemaphoreType.DMA((2,))],
         compiler_params=pltpu.CompilerParams(vmem_limit_bytes=4 * MIB),
     )(*[in_vmem(piece) for piece in (own, mate, far, far_mate)])
 
@@ -726,10 +729,13 @@
     v_far = swap_with(v_far, "sp", 2)
     dq_own, dq_mate, k_own, k_far = attention_keys(state, gains, tables)
     k_far = swap_with(k_far, "sp", 2)
-    turned = turn_inputs(inputs, mate_inputs)
+    turned = turn_inputs(inputs)
+    turned_mate = turn_inputs(mate_inputs)
 
     def weight_grad(p_own, p_far, extra):
-        mine, there, blocks, sent = weight_partials(turned, p_own, p_far, extra, dp_count)
+        mine, there, blocks, sent = weight_partials(
+            turned, turned_mate, p_own, p_far, extra, dp_count
+        )
         first, *rest = sum_cores(blocks, swap_with(sent, "dp", 1))
         received = [swap_with(rest[m - 1], "dp", 2 * m) for m in range(1, chips)]
         total = sum_chips(first, received)

time: 108 us -> 108 us (level)
    pallas_call x10 -> x11, Pallas kernels: 10.4 us -> 10.5 us  [kernel_call(): pl.pallas_call(body, out_shape=out_shape, in_specs=[vmem] * len(args), ou...]
where the time goes in v5:
time: 108 us
  waiting for transfers between devices  59.5 us (55%)
  starting transfers between devices  32.6 us (30%)
  Pallas kernels  14.2 us (13%)
    ppermute x28, waiting for transfers between devices, swap_with(): return lax.ppermute(value, axis, [(i, i ^ k) for i in range(count)])  59.5 us
    ppermute x28, starting transfers between devices, swap_with(): return lax.ppermute(value, axis, [(i, i ^ k) for i in range(count)])  32.6 us
    pallas_call x11, Pallas kernels, kernel_call(): pl.pallas_call(body, out_shape=out_shape, in_specs=[vmem] * len(args), ou...  10.5 us
    pallas_call x2, Pallas kernels, copy_call(): pl.pallas_call(run, out_shape=out_shape, in_specs=[pl.BlockSpec(memory_sp...  2.27 us
  transfers between devices with their start and end apart: 28, of which 9 were waited for; matrix products, arithmetic and copies ran while one was open for 0% of the time, Pallas kernels for 12%

profile of v5, /device:TPU:0, one launch (start us, length us, event | category | flops | bytes accessed | tf_op | source)
XLA Modules:
  0.0 108.1 jit_solution(3479353419992032637)
XLA Ops:
  0.6 3.1 %collective-permute-start = (bf16[128,2048]{1,0:T(8,128)(2,1)}, bf16[128,2048]{1,0:T(8,128)(2,1)S(1)}, u32[]{:S(2)}, u32[]{:S(2)}) collective-permute-start(bf16[128,2048]{1,0:T(8,128)(2,1)} %bitcast.9), channel_id=1, source_target_pairs={{0,8},{8,0},{16,24},{24,16},{1,9},{9,1},{17,25},{25,17},{2,10},{10... | collective-permute-start | bytes 1572872 | tf_op jit(solution)/shard_map/ppermute | solution.py:264
  3.7 1.0 shard_map.159
  4.8 0.1 collective-permute-start.1
  4.9 3.0 %collective-permute-start.2 = (bf16[128,256]{1,0:T(8,128)(2,1)S(1)}, bf16[128,256]{1,0:T(8,128)(2,1)S(1)}, u32[]{:S(2)}, u32[]{:S(2)}) collective-permute-start(bf16[128,256]{1,0:T(8,128)(2,1)S(1)} %get-tuple-element.50), channel_id=1, source_target_pairs={{0,16},{8,24},{16,0},{24,8},{1,17},{9,25},{17,1},{25,9},{2,18},{10... | collective-permute-start | bytes 196616 | tf_op jit(solution)/shard_map/ppermute | solution.py:264
  7.9 1.3 %collective-permute-start.3 = (bf16[128,256]{1,0:T(8,128)(2,1)S(1)}, bf16[128,256]{1,0:T(8,128)(2,1)S(1)}, u32[]{:S(2)}, u32[]{:S(2)}) collective-permute-start(bf16[128,256]{1,0:T(8,128)(2,1)S(1)} %get-tuple-element.51), channel_id=1, source_target_pairs={{0,24},{8,16},{16,8},{24,0},{1,25},{9,17},{17,9},{25,1},{2,26},{10... | collective-permute-start | bytes 196616 | tf_op jit(solution)/shard_map/ppermute | solution.py:264
  9.3 1.2 %shard_map.158 = (bf16[128,1280]{1,0:T(8,128)(2,1)S(1)}, bf16[256,512]{1,0:T(8,128)(2,1)S(1)}, f32[1,64]{1,0:T(1,128)S(1)}, f32[1,64]{1,0:T(1,128)S(1)}, f32[8,1...) custom-call(bf16[128,1024]{1,0:T(8,128)(2,1)} %bitcast.12, ...), custom_call_target="tpu_custom_call" | custom-call | tf_op jit(solution)/shard_map/pallas_call | solution.py:279
  10.5 13.8 %collective-permute-done.2.refs_2_ = bf16[128,256]{1,0:T(8,128)(2,1)S(1)} collective-permute-done((bf16[128,256]{1,0:T(8,128)(2,1)S(1)}, bf16[128,256]{1,0:T(8,128)(2,1)S(1)}, u32[]{:S(2)}, u32[]{:S(2)}) %collective-permute-start.2) | collective-permute-done | bytes 65568 | tf_op jit(solution)/shard_map/ppermute | solution.py:264
  24.3 3.6 %collective-permute-done.3.refs_3_ = bf16[128,256]{1,0:T(8,128)(2,1)S(1)} collective-permute-done((bf16[128,256]{1,0:T(8,128)(2,1)S(1)}, bf16[128,256]{1,0:T(8,128)(2,1)S(1)}, u32[]{:S(2)}, u32[]{:S(2)}) %collective-permute-start.3) | collective-permute-done | bytes 65568 | tf_op jit(solution)/shard_map/ppermute | solution.py:264
  27.9 0.0 collective-permute-done.1.refs_1_
  27.9 3.1 %shard_map.160 = (f32[256,128]{1,0:T(8,128)S(1)}, bf16[256,128]{1,0:T(8,128)(2,1)S(1)}, f32[8,512,256]{2,1,0:T(8,128)S(1)}, bf16[8,256,64]{2,1,0:T(8,128)(2,1)S(...) custom-call(bf16[128,1280]{1,0:T(8,128)(2,1)S(1)} %get-tuple-element, ...), custom_call_target="tpu_custom_call" | custom-call | flops 268435456 | tf_op jit(solution)/shard_map/pallas_call | solution.py:243
  31.1 0.1 collective-permute-start.5
  31.1 0.0 copy-start
  31.2 1.0 copy-done
  32.2 0.2 shard_map.156.x_ref
  32.4 0.0 collective-permute-done.x_ref
  32.4 0.2 shard_map.157.xm_ref
  32.6 3.7 %collective-permute-done.5.pf_ref = bf16[256,128]{1,0:T(8,128)(2,1)S(1)} collective-permute-done((bf16[256,128]{1,0:T(8,128)(2,1)S(1)}, bf16[256,128]{1,0:T(8,128)(2,1)S(1)}, u32[]{:S(2)}, u32[]{:S(2)}) %collective-permute-start.5) | collective-permute-done | bytes 65568 | tf_op jit(solution)/shard_map/ppermute | solution.py:264
  36.3 0.4 shard_map.162
  36.7 0.1 collective-permute-start.21
  36.8 4.2 %shard_map.161 = (bf16[128,512]{1,0:T(8,128)(2,1)S(1)}, bf16[128,512]{1,0:T(8,128)(2,1)S(1)}, f32[256,128]{1,0:T(8,128)S(1)}, bf16[256,128]{1,0:T(8,128)(2,1)S(1)}) custom-call(f32[8,512,256]{2,1,0:T(8,128)S(1)} %get-tuple-element.58.refs_0_, bf16[8,256,64]{2,1,0:T(8,128)(2,1)S(1)} %get-tuple-element.59.refs_1_, ...), custom_call_target="tpu_custom_call" | custom-call | flops 402653184 | tf_op jit(solution)/shard_map/pallas_call | solution.py:243
  41.0 0.1 collective-permute-start.4
  41.1 1.6 %collective-permute-start.10 = (bf16[256,512]{1,0:T(8,128)(2,1)S(1)}, bf16[256,512]{1,0:T(8,128)(2,1)S(1)}, u32[]{:S(2)}, u32[]{:S(2)}) collective-permute-start(bf16[256,512]{1,0:T(8,128)(2,1)S(1)} %get-tuple-element.77.rest_0_), channel_id=1, source_target_pairs={{0,4},{1,5},{2,6},{3,7},{4,0},{5,1},{6,2},{7,3},{8,12},{9,13},{10,... | collective-permute-start | bytes 786440 | tf_op jit(solution)/shard_map/ppermute | solution.py:264
  42.7 4.5 %collective-permute-done.4.pf_ref = bf16[256,128]{1,0:T(8,128)(2,1)S(1)} collective-permute-done((bf16[256,128]{1,0:T(8,128)(2,1)S(1)}, bf16[256,128]{1,0:T(8,128)(2,1)S(1)}, u32[]{:S(2)}, u32[]{:S(2)}) %collective-permute-start.4) | collective-permute-done | bytes 65568 | tf_op jit(solution)/shard_map/ppermute | solution.py:264
  47.2 0.5 shard_map.163
  47.6 0.1 collective-permute-start.14
  47.8 1.6 %collective-permute-start.11 = (bf16[256,512]{1,0:T(8,128)(2,1)S(1)}, bf16[256,512]{1,0:T(8,128)(2,1)S(1)}, u32[]{:S(2)}, u32[]{:S(2)}) collective-permute-start(bf16[256,512]{1,0:T(8,128)(2,1)S(1)} %get-tuple-element.77.rest_0_), channel_id=1, source_target_pairs={{0,5},{1,4},{2,7},{3,6},{4,1},{5,0},{6,3},{7,2},{8,13},{9,12},{10,... | collective-permute-start | bytes 786440 | tf_op jit(solution)/shard_map/ppermute | solution.py:264
  49.3 1.4 %collective-permute-start.12 = (bf16[256,512]{1,0:T(8,128)(2,1)S(1)}, bf16[256,512]{1,0:T(8,128)(2,1)S(1)}, u32[]{:S(2)}, u32[]{:S(2)}) collective-permute-start(bf16[256,512]{1,0:T(8,128)(2,1)S(1)} %get-tuple-element.77.rest_0_), channel_id=1, source_target_pairs={{0,6},{1,7},{2,4},{3,5},{4,2},{5,3},{6,0},{7,1},{8,14},{9,15},{10,... | collective-permute-start | bytes 786440 | tf_op jit(solution)/shard_map/ppermute | solution.py:264
  50.8 0.0 collective-permute-done.21.got_ref
  50.8 0.9 collective-permute-start.13
  51.6 0.1 shard_map.168
  51.7 0.0 collective-permute-done.10.rest_4_
  51.7 1.6 %collective-permute-start.22 = (bf16[256,128]{1,0:T(8,128)(2,1)S(1)}, bf16[256,128]{1,0:T(8,128)(2,1)S(1)}, u32[]{:S(2)}, u32[]{:S(2)}) collective-permute-start(bf16[256,128]{1,0:T(8,128)(2,1)S(1)} %get-tuple-element.89), channel_id=1, source_target_pairs={{0,2},{1,3},{2,0},{3,1},{4,6},{5,7},{6,4},{7,5},{8,10},{9,11},{10,... | collective-permute-start | bytes 196616 | tf_op jit(solution)/shard_map/ppermute | solution.py:264
  53.3 0.5 collective-permute-start.23
  53.8 0.1 shard_map.165
  53.9 13.4 %collective-permute-done.11.rest_5_ = bf16[256,512]{1,0:T(8,128)(2,1)S(1)} collective-permute-done((bf16[256,512]{1,0:T(8,128)(2,1)S(1)}, bf16[256,512]{1,0:T(8,128)(2,1)S(1)}, u32[]{:S(2)}, u32[]{:S(2)}) %collective-permute-start.11) | collective-permute-done | bytes 262176 | tf_op jit(solution)/shard_map/ppermute | solution.py:264
  67.2 0.8 collective-permute-start.7
  68.0 0.0 collective-permute-done.12.rest_6_
  68.0 1.5 %collective-permute-start.8 = (bf16[256,512]{1,0:T(8,128)(2,1)S(1)}, bf16[256,512]{1,0:T(8,128)(2,1)S(1)}, u32[]{:S(2)}, u32[]{:S(2)}) collective-permute-start(bf16[256,512]{1,0:T(8,128)(2,1)S(1)} %get-tuple-element.77.rest_0_), channel_id=1, source_target_pairs={{0,2},{1,3},{2,0},{3,1},{4,6},{5,7},{6,4},{7,5},{8,10},{9,11},{10,... | collective-permute-start | bytes 786440 | tf_op jit(solution)/shard_map/ppermute | solution.py:264
  69.5 0.0 collective-permute-done.13.rest_7_
  69.5 0.0 collective-permute-start.9
  69.5 0.0 collective-permute-done.22.refs_1_
  69.5 2.3 %collective-permute-start.24 = (bf16[256,128]{1,0:T(8,128)(2,1)S(1)}, bf16[256,128]{1,0:T(8,128)(2,1)S(1)}, u32[]{:S(2)}, u32[]{:S(2)}) collective-permute-start(bf16[256,128]{1,0:T(8,128)(2,1)S(1)} %get-tuple-element.91), channel_id=1, source_target_pairs={{0,6},{1,7},{2,4},{3,5},{4,2},{5,3},{6,0},{7,1},{8,14},{9,15},{10,... | collective-permute-start | bytes 196616 | tf_op jit(solution)/shard_map/ppermute | solution.py:264
  71.8 0.7 collective-permute-start.15
  72.6 12.3 %collective-permute-done.24.refs_3_ = bf16[256,128]{1,0:T(8,128)(2,1)S(1)} collective-permute-done((bf16[256,128]{1,0:T(8,128)(2,1)S(1)}, bf16[256,128]{1,0:T(8,128)(2,1)S(1)}, u32[]{:S(2)}, u32[]{:S(2)}) %collective-permute-start.24) | collective-permute-done | bytes 65568 | tf_op jit(solution)/shard_map/ppermute | solution.py:264
  84.9 0.5 collective-permute-start.16
  85.5 1.0 collective-permute-start.6
  86.5 2.7 %collective-permute-done.16.refs_2_ = bf16[256,128]{1,0:T(8,128)(2,1)S(1)} collective-permute-done((bf16[256,128]{1,0:T(8,128)(2,1)S(1)}, bf16[256,128]{1,0:T(8,128)(2,1)S(1)}, u32[]{:S(2)}, u32[]{:S(2)}) %collective-permute-start.16) | collective-permute-done | bytes 65568 | tf_op jit(solution)/shard_map/ppermute | solution.py:264
  89.2 1.4 %collective-permute-start.17 = (bf16[256,128]{1,0:T(8,128)(2,1)S(1)}, bf16[256,128]{1,0:T(8,128)(2,1)S(1)}, u32[]{:S(2)}, u32[]{:S(2)}) collective-permute-start(bf16[256,128]{1,0:T(8,128)(2,1)S(1)} %get-tuple-element.85), channel_id=1, source_target_pairs={{0,6},{1,7},{2,4},{3,5},{4,2},{5,3},{6,0},{7,1},{8,14},{9,15},{10,... | collective-permute-start | bytes 196616 | tf_op jit(solution)/shard_map/ppermute | solution.py:264
  90.7 3.7 %collective-permute-done.17.refs_3_ = bf16[256,128]{1,0:T(8,128)(2,1)S(1)} collective-permute-done((bf16[256,128]{1,0:T(8,128)(2,1)S(1)}, bf16[256,128]{1,0:T(8,128)(2,1)S(1)}, u32[]{:S(2)}, u32[]{:S(2)}) %collective-permute-start.17) | collective-permute-done | bytes 65568 | tf_op jit(solution)/shard_map/ppermute | solution.py:264
  94.4 1.0 collective-permute-start.25
  95.4 1.5 %collective-permute-start.26 = (bf16[256,128]{1,0:T(8,128)(2,1)S(1)}, bf16[256,128]{1,0:T(8,128)(2,1)S(1)}, u32[]{:S(2)}, u32[]{:S(2)}) collective-permute-start(bf16[256,128]{1,0:T(8,128)(2,1)S(1)} %shard_map.169.own_ref), channel_id=1, source_target_pairs={{0,16},{8,24},{16,0},{24,8},{1,17},{9,25},{17,1},{25,9},{2,18},{10... | collective-permute-start | bytes 196616 | tf_op jit(solution)/shard_map/ppermute | solution.py:264
  96.9 0.0 collective-permute-done.8.rest_2_
  96.9 1.9 %collective-permute-start.27 = (bf16[256,128]{1,0:T(8,128)(2,1)S(1)}, bf16[256,128]{1,0:T(8,128)(2,1)S(1)}, u32[]{:S(2)}, u32[]{:S(2)}) collective-permute-start(bf16[256,128]{1,0:T(8,128)(2,1)S(1)} %shard_map.169.own_ref), channel_id=1, source_target_pairs={{0,24},{8,16},{16,8},{24,0},{1,25},{9,17},{17,9},{25,1},{2,26},{10... | collective-permute-start | bytes 196616 | tf_op jit(solution)/shard_map/ppermute | solution.py:264
  98.9 0.1 collective-permute-start.18
  99.0 0.0 collective-permute-done.6.mate_ref
  99.0 2.3 %collective-permute-start.19 = (bf16[256,128]{1,0:T(8,128)(2,1)S(1)}, bf16[256,128]{1,0:T(8,128)(2,1)S(1)}, u32[]{:S(2)}, u32[]{:S(2)}) collective-permute-start(bf16[256,128]{1,0:T(8,128)(2,1)S(1)} %shard_map.166.own_ref), channel_id=1, source_target_pairs={{0,16},{8,24},{16,0},{24,8},{1,17},{9,25},{17,1},{25,9},{2,18},{10... | collective-permute-start | bytes 196616 | tf_op jit(solution)/shard_map/ppermute | solution.py:264
  101.3 0.0 collective-permute-done.25.mate_ref
  101.3 1.9 %collective-permute-start.20 = (bf16[256,128]{1,0:T(8,128)(2,1)S(1)}, bf16[256,128]{1,0:T(8,128)(2,1)S(1)}, u32[]{:S(2)}, u32[]{:S(2)}) collective-permute-start(bf16[256,128]{1,0:T(8,128)(2,1)S(1)} %shard_map.166.own_ref), channel_id=1, source_target_pairs={{0,24},{8,16},{16,8},{24,0},{1,25},{9,17},{17,9},{25,1},{2,26},{10... | collective-permute-start | bytes 196616 | tf_op jit(solution)/shard_map/ppermute | solution.py:264
  103.3 1.7 %shard_map.164 = (bf16[128,2048]{1,0:T(8,128)(2,1)}, bf16[128,1024]{1,0:T(8,128)(2,1)}) custom-call(bf16[128,128]{1,0:T(8,128)(2,1)S(1)} %get-tuple-element.73.k_ref, bf16[128,128]{1,0:T(8,128)(2,1)S(1)} %get-tuple-element.74.v_ref, bf16[128,768]{1,0:T(8,128)(2,1)S(1)} %collective-permute-done.6.mate_ref, bf16[128,512]{1,0:T(8,128)(2,1)S(1)} %get-tuple-element.76.dq_ref, ...), custom_call_target="tpu_custom_call" | custom-call | flops 268435456 | tf_op jit(solution)/shard_map/pallas_call | solution.py:243
  104.9 0.0 collective-permute-done.26.far_ref
  104.9 0.7 shard_map.170
  105.7 0.0 collective-permute-done.19.far_ref
  105.7 1.7 %collective-permute-done.20.far_mate_ref = bf16[256,128]{1,0:T(8,128)(2,1)S(1)} collective-permute-done((bf16[256,128]{1,0:T(8,128)(2,1)S(1)}, bf16[256,128]{1,0:T(8,128)(2,1)S(1)}, u32[]{:S(2)}, u32[]{:S(2)}) %collective-permute-start.20) | collective-permute-done | bytes 65568 | tf_op jit(solution)/shard_map/ppermute | solution.py:264
  107.4 0.7 shard_map.167
  (9 shorter events, 0.1 us)
Async XLA Ops:
  0.6 31.8 %collective-permute-start = (bf16[128,2048]{1,0:T(8,128)(2,1)}, bf16[128,2048]{1,0:T(8,128)(2,1)S(1)}, u32[]{:S(2)}, u32[]{:S(2)}) collective-permute-start(bf16[128,2048]{1,0:T(8,128)(2,1)} %bitcast.9), channel_id=1, source_target_pairs={{0,8},{8,0},{16,24},{24,16},{1,9},{9,1},{17,25},{25,17},{2,10},{10... | collective-permute-start | bytes 1572872 | tf_op jit(solution)/shard_map/ppermute | solution.py:264
  4.8 23.1 %collective-permute-start.1 = (bf16[128,1280]{1,0:T(8,128)(2,1)S(1)}, bf16[128,1280]{1,0:T(8,128)(2,1)S(1)}, u32[]{:S(2)}, u32[]{:S(2)}) collective-permute-start(bf16[128,1280]{1,0:T(8,128)(2,1)S(1)} %get-tuple-element.49), channel_id=1, source_target_pairs={{0,8},{8,0},{16,24},{24,16},{1,9},{9,1},{17,25},{25,17},{2,10},{10... | collective-permute-start | bytes 983048 | tf_op jit(solution)/shard_map/ppermute | solution.py:264
  4.9 19.4 %collective-permute-start.2 = (bf16[128,256]{1,0:T(8,128)(2,1)S(1)}, bf16[128,256]{1,0:T(8,128)(2,1)S(1)}, u32[]{:S(2)}, u32[]{:S(2)}) collective-permute-start(bf16[128,256]{1,0:T(8,128)(2,1)S(1)} %get-tuple-element.50), channel_id=1, source_target_pairs={{0,16},{8,24},{16,0},{24,8},{1,17},{9,25},{17,1},{25,9},{2,18},{10... | collective-permute-start | bytes 196616 | tf_op jit(solution)/shard_map/ppermute | solution.py:264
  7.9 20.0 %collective-permute-start.3 = (bf16[128,256]{1,0:T(8,128)(2,1)S(1)}, bf16[128,256]{1,0:T(8,128)(2,1)S(1)}, u32[]{:S(2)}, u32[]{:S(2)}) collective-permute-start(bf16[128,256]{1,0:T(8,128)(2,1)S(1)} %get-tuple-element.51), channel_id=1, source_target_pairs={{0,24},{8,16},{16,8},{24,0},{1,25},{9,17},{17,9},{25,1},{2,26},{10... | collective-permute-start | bytes 196616 | tf_op jit(solution)/shard_map/ppermute | solution.py:264
  31.1 5.2 %collective-permute-start.5 = (bf16[256,128]{1,0:T(8,128)(2,1)S(1)}, bf16[256,128]{1,0:T(8,128)(2,1)S(1)}, u32[]{:S(2)}, u32[]{:S(2)}) collective-permute-start(bf16[256,128]{1,0:T(8,128)(2,1)S(1)} %get-tuple-element.70), channel_id=1, source_target_pairs={{0,16},{8,24},{16,0},{24,8},{1,17},{9,25},{17,1},{25,9},{2,18},{10... | collective-permute-start | bytes 196616 | tf_op jit(solution)/shard_map/ppermute | solution.py:264
  31.1 1.0 copy-start
  36.7 14.0 %collective-permute-start.21 = (bf16[4,256,128]{2,1,0:T(8,128)(2,1)S(1)}, bf16[4,256,128]{2,1,0:T(8,128)(2,1)S(1)}, u32[]{:S(2)}, u32[]{:S(2)}) collective-permute-start(bf16[4,256,128]{2,1,0:T(8,128)(2,1)S(1)} %get-tuple-element.87), channel_id=1, source_target_pairs={{0,1},{1,0},{2,3},{3,2},{4,5},{5,4},{6,7},{7,6},{8,9},{9,8},{10,11... | collective-permute-start | bytes 786440 | tf_op jit(solution)/shard_map/ppermute | solution.py:264
  41.0 6.2 %collective-permute-start.4 = (bf16[256,128]{1,0:T(8,128)(2,1)S(1)}, bf16[256,128]{1,0:T(8,128)(2,1)S(1)}, u32[]{:S(2)}, u32[]{:S(2)}) collective-permute-start(bf16[256,128]{1,0:T(8,128)(2,1)S(1)} %get-tuple-element.68), channel_id=1, source_target_pairs={{0,16},{8,24},{16,0},{24,8},{1,17},{9,25},{17,1},{25,9},{2,18},{10... | collective-permute-start | bytes 196616 | tf_op jit(solution)/shard_map/ppermute | solution.py:264
  41.1 10.6 %collective-permute-start.10 = (bf16[256,512]{1,0:T(8,128)(2,1)S(1)}, bf16[256,512]{1,0:T(8,128)(2,1)S(1)}, u32[]{:S(2)}, u32[]{:S(2)}) collective-permute-start(bf16[256,512]{1,0:T(8,128)(2,1)S(1)} %get-tuple-element.77.rest_0_), channel_id=1, source_target_pairs={{0,4},{1,5},{2,6},{3,7},{4,0},{5,1},{6,2},{7,3},{8,12},{9,13},{10,... | collective-permute-start | bytes 786440 | tf_op jit(solution)/shard_map/ppermute | solution.py:264
  47.6 5.7 %collective-permute-start.14 = (bf16[4,256,128]{2,1,0:T(8,128)(2,1)S(1)}, bf16[4,256,128]{2,1,0:T(8,128)(2,1)S(1)}, u32[]{:S(2)}, u32[]{:S(2)}) collective-permute-start(bf16[4,256,128]{2,1,0:T(8,128)(2,1)S(1)} %get-tuple-element.81), channel_id=1, source_target_pairs={{0,1},{1,0},{2,3},{3,2},{4,5},{5,4},{6,7},{7,6},{8,9},{9,8},{10,11... | collective-permute-start | bytes 786440 | tf_op jit(solution)/shard_map/ppermute | solution.py:264
  47.8 19.5 %collective-permute-start.11 = (bf16[256,512]{1,0:T(8,128)(2,1)S(1)}, bf16[256,512]{1,0:T(8,128)(2,1)S(1)}, u32[]{:S(2)}, u32[]{:S(2)}) collective-permute-start(bf16[256,512]{1,0:T(8,128)(2,1)S(1)} %get-tuple-element.77.rest_0_), channel_id=1, source_target_pairs={{0,5},{1,4},{2,7},{3,6},{4,1},{5,0},{6,3},{7,2},{8,13},{9,12},{10,... | collective-permute-start | bytes 786440 | tf_op jit(solution)/shard_map/ppermute | solution.py:264
  49.3 18.7 %collective-permute-start.12 = (bf16[256,512]{1,0:T(8,128)(2,1)S(1)}, bf16[256,512]{1,0:T(8,128)(2,1)S(1)}, u32[]{:S(2)}, u32[]{:S(2)}) collective-permute-start(bf16[256,512]{1,0:T(8,128)(2,1)S(1)} %get-tuple-element.77.rest_0_), channel_id=1, source_target_pairs={{0,6},{1,7},{2,4},{3,5},{4,2},{5,3},{6,0},{7,1},{8,14},{9,15},{10,... | collective-permute-start | bytes 786440 | tf_op jit(solution)/shard_map/ppermute | solution.py:264
  50.8 18.8 %collective-permute-start.13 = (bf16[256,512]{1,0:T(8,128)(2,1)S(1)}, bf16[256,512]{1,0:T(8,128)(2,1)S(1)}, u32[]{:S(2)}, u32[]{:S(2)}) collective-permute-start(bf16[256,512]{1,0:T(8,128)(2,1)S(1)} %get-tuple-element.77.rest_0_), channel_id=1, source_target_pairs={{0,7},{1,6},{2,5},{3,4},{4,3},{5,2},{6,1},{7,0},{8,15},{9,14},{10,... | collective-permute-start | bytes 786440 | tf_op jit(solution)/shard_map/ppermute | solution.py:264
  51.7 17.8 %collective-permute-start.22 = (bf16[256,128]{1,0:T(8,128)(2,1)S(1)}, bf16[256,128]{1,0:T(8,128)(2,1)S(1)}, u32[]{:S(2)}, u32[]{:S(2)}) collective-permute-start(bf16[256,128]{1,0:T(8,128)(2,1)S(1)} %get-tuple-element.89), channel_id=1, source_target_pairs={{0,2},{1,3},{2,0},{3,1},{4,6},{5,7},{6,4},{7,5},{8,10},{9,11},{10,... | collective-permute-start | bytes 196616 | tf_op jit(solution)/shard_map/ppermute | solution.py:264
  53.3 18.6 %collective-permute-start.23 = (bf16[256,128]{1,0:T(8,128)(2,1)S(1)}, bf16[256,128]{1,0:T(8,128)(2,1)S(1)}, u32[]{:S(2)}, u32[]{:S(2)}) collective-permute-start(bf16[256,128]{1,0:T(8,128)(2,1)S(1)} %get-tuple-element.90), channel_id=1, source_target_pairs={{0,4},{1,5},{2,6},{3,7},{4,0},{5,1},{6,2},{7,3},{8,12},{9,13},{10,... | collective-permute-start | bytes 196616 | tf_op jit(solution)/shard_map/ppermute | solution.py:264
  67.2 28.2 %collective-permute-start.7 = (bf16[256,512]{1,0:T(8,128)(2,1)S(1)}, bf16[256,512]{1,0:T(8,128)(2,1)S(1)}, u32[]{:S(2)}, u32[]{:S(2)}) collective-permute-start(bf16[256,512]{1,0:T(8,128)(2,1)S(1)} %get-tuple-element.77.rest_0_), channel_id=1, source_target_pairs={{0,1},{1,0},{2,3},{3,2},{4,5},{5,4},{6,7},{7,6},{8,9},{9,8},{10,11... | collective-permute-start | bytes 786440 | tf_op jit(solution)/shard_map/ppermute | solution.py:264
  68.0 28.9 %collective-permute-start.8 = (bf16[256,512]{1,0:T(8,128)(2,1)S(1)}, bf16[256,512]{1,0:T(8,128)(2,1)S(1)}, u32[]{:S(2)}, u32[]{:S(2)}) collective-permute-start(bf16[256,512]{1,0:T(8,128)(2,1)S(1)} %get-tuple-element.77.rest_0_), channel_id=1, source_target_pairs={{0,2},{1,3},{2,0},{3,1},{4,6},{5,7},{6,4},{7,5},{8,10},{9,11},{10,... | collective-permute-start | bytes 786440 | tf_op jit(solution)/shard_map/ppermute | solution.py:264
  69.5 29.3 %collective-permute-start.9 = (bf16[256,512]{1,0:T(8,128)(2,1)S(1)}, bf16[256,512]{1,0:T(8,128)(2,1)S(1)}, u32[]{:S(2)}, u32[]{:S(2)}) collective-permute-start(bf16[256,512]{1,0:T(8,128)(2,1)S(1)} %get-tuple-element.77.rest_0_), channel_id=1, source_target_pairs={{0,3},{1,2},{2,1},{3,0},{4,7},{5,6},{6,5},{7,4},{8,11},{9,10},{10,... | collective-permute-start | bytes 786440 | tf_op jit(solution)/shard_map/ppermute | solution.py:264
  69.5 15.4 %collective-permute-start.24 = (bf16[256,128]{1,0:T(8,128)(2,1)S(1)}, bf16[256,128]{1,0:T(8,128)(2,1)S(1)}, u32[]{:S(2)}, u32[]{:S(2)}) collective-permute-start(bf16[256,128]{1,0:T(8,128)(2,1)S(1)} %get-tuple-element.91), channel_id=1, source_target_pairs={{0,6},{1,7},{2,4},{3,5},{4,2},{5,3},{6,0},{7,1},{8,14},{9,15},{10,... | collective-permute-start | bytes 196616 | tf_op jit(solution)/shard_map/ppermute | solution.py:264
  71.8 13.6 %collective-permute-start.15 = (bf16[256,128]{1,0:T(8,128)(2,1)S(1)}, bf16[256,128]{1,0:T(8,128)(2,1)S(1)}, u32[]{:S(2)}, u32[]{:S(2)}) collective-permute-start(bf16[256,128]{1,0:T(8,128)(2,1)S(1)} %get-tuple-element.83), channel_id=1, source_target_pairs={{0,2},{1,3},{2,0},{3,1},{4,6},{5,7},{6,4},{7,5},{8,10},{9,11},{10,... | collective-permute-start | bytes 196616 | tf_op jit(solution)/shard_map/ppermute | solution.py:264
  84.9 4.3 %collective-permute-start.16 = (bf16[256,128]{1,0:T(8,128)(2,1)S(1)}, bf16[256,128]{1,0:T(8,128)(2,1)S(1)}, u32[]{:S(2)}, u32[]{:S(2)}) collective-permute-start(bf16[256,128]{1,0:T(8,128)(2,1)S(1)} %get-tuple-element.84), channel_id=1, source_target_pairs={{0,4},{1,5},{2,6},{3,7},{4,0},{5,1},{6,2},{7,3},{8,12},{9,13},{10,... | collective-permute-start | bytes 196616 | tf_op jit(solution)/shard_map/ppermute | solution.py:264
  85.5 13.5 %collective-permute-start.6 = (bf16[128,768]{1,0:T(8,128)(2,1)S(1)}, bf16[128,768]{1,0:T(8,128)(2,1)S(1)}, u32[]{:S(2)}, u32[]{:S(2)}) collective-permute-start(bf16[128,768]{1,0:T(8,128)(2,1)S(1)} %get-tuple-element.75), channel_id=1, source_target_pairs={{0,8},{8,0},{16,24},{24,16},{1,9},{9,1},{17,25},{25,17},{2,10},{10... | collective-permute-start | bytes 589832 | tf_op jit(solution)/shard_map/ppermute | solution.py:264
  89.2 5.2 %collective-permute-start.17 = (bf16[256,128]{1,0:T(8,128)(2,1)S(1)}, bf16[256,128]{1,0:T(8,128)(2,1)S(1)}, u32[]{:S(2)}, u32[]{:S(2)}) collective-permute-start(bf16[256,128]{1,0:T(8,128)(2,1)S(1)} %get-tuple-element.85), channel_id=1, source_target_pairs={{0,6},{1,7},{2,4},{3,5},{4,2},{5,3},{6,0},{7,1},{8,14},{9,15},{10,... | collective-permute-start | bytes 196616 | tf_op jit(solution)/shard_map/ppermute | solution.py:264
  94.4 7.0 %collective-permute-start.25 = (bf16[256,128]{1,0:T(8,128)(2,1)S(1)}, bf16[256,128]{1,0:T(8,128)(2,1)S(1)}, u32[]{:S(2)}, u32[]{:S(2)}) collective-permute-start(bf16[256,128]{1,0:T(8,128)(2,1)S(1)} %shard_map.169.own_ref), channel_id=1, source_target_pairs={{0,8},{8,0},{16,24},{24,16},{1,9},{9,1},{17,25},{25,17},{2,10},{10... | collective-permute-start | bytes 196616 | tf_op jit(solution)/shard_map/ppermute | solution.py:264
  95.4 9.5 %collective-permute-start.26 = (bf16[256,128]{1,0:T(8,128)(2,1)S(1)}, bf16[256,128]{1,0:T(8,128)(2,1)S(1)}, u32[]{:S(2)}, u32[]{:S(2)}) collective-permute-start(bf16[256,128]{1,0:T(8,128)(2,1)S(1)} %shard_map.169.own_ref), channel_id=1, source_target_pairs={{0,16},{8,24},{16,0},{24,8},{1,17},{9,25},{17,1},{25,9},{2,18},{10... | collective-permute-start | bytes 196616 | tf_op jit(solution)/shard_map/ppermute | solution.py:264
  96.9 8.0 %collective-permute-start.27 = (bf16[256,128]{1,0:T(8,128)(2,1)S(1)}, bf16[256,128]{1,0:T(8,128)(2,1)S(1)}, u32[]{:S(2)}, u32[]{:S(2)}) collective-permute-start(bf16[256,128]{1,0:T(8,128)(2,1)S(1)} %shard_map.169.own_ref), channel_id=1, source_target_pairs={{0,24},{8,16},{16,8},{24,0},{1,25},{9,17},{17,9},{25,1},{2,26},{10... | collective-permute-start | bytes 196616 | tf_op jit(solution)/shard_map/ppermute | solution.py:264
  98.9 6.8 %collective-permute-start.18 = (bf16[256,128]{1,0:T(8,128)(2,1)S(1)}, bf16[256,128]{1,0:T(8,128)(2,1)S(1)}, u32[]{:S(2)}, u32[]{:S(2)}) collective-permute-start(bf16[256,128]{1,0:T(8,128)(2,1)S(1)} %shard_map.166.own_ref), channel_id=1, source_target_pairs={{0,8},{8,0},{16,24},{24,16},{1,9},{9,1},{17,25},{25,17},{2,10},{10... | collective-permute-start | bytes 196616 | tf_op jit(solution)/shard_map/ppermute | solution.py:264
  99.0 6.7 %collective-permute-start.19 = (bf16[256,128]{1,0:T(8,128)(2,1)S(1)}, bf16[256,128]{1,0:T(8,128)(2,1)S(1)}, u32[]{:S(2)}, u32[]{:S(2)}) collective-permute-start(bf16[256,128]{1,0:T(8,128)(2,1)S(1)} %shard_map.166.own_ref), channel_id=1, source_target_pairs={{0,16},{8,24},{16,0},{24,8},{1,17},{9,25},{17,1},{25,9},{2,18},{10... | collective-permute-start | bytes 196616 | tf_op jit(solution)/shard_map/ppermute | solution.py:264
  101.3 6.1 %collective-permute-start.20 = (bf16[256,128]{1,0:T(8,128)(2,1)S(1)}, bf16[256,128]{1,0:T(8,128)(2,1)S(1)}, u32[]{:S(2)}, u32[]{:S(2)}) collective-permute-start(bf16[256,128]{1,0:T(8,128)(2,1)S(1)} %shard_map.166.own_ref), channel_id=1, source_target_pairs={{0,24},{8,16},{16,8},{24,0},{1,25},{9,17},{17,9},{25,1},{2,26},{10... | collective-permute-start | bytes 196616 | tf_op jit(solution)/shard_map/ppermute | solution.py:264
